TPU v7x, 256 devices: a whole 4x4x8 slice. The times are simulated.
256 devices in a mesh: ep: 16 (over y, x), tp: 16 (over z, core).
Axes of the slice: x: 4, y: 4, z: 8, core: 2. Of those that a mesh axis runs over, the one named last changes fastest.
Arguments:
- q_latent: bfloat16 [12288, 384], P(('ep', 'tp')), may hold values from -6 to 6
- kv_latent: bfloat16 [12288, 256], P(('ep', 'tp')), may hold values from -6 to 6
- rope_key: bfloat16 [12288, 64], P(('ep', 'tp')), may hold values from -6 to 6
- q_latent_gain: float32 [384], replicated, may hold values from 0.1 to 1.9
- kv_latent_gain: float32 [256], replicated, may hold values from 0.1 to 1.9
- w_query: bfloat16 [384, 3072], P(None, 'tp'), may hold values from -0.3125 to 0.3125
- w_key: bfloat16 [256, 2048], P(None, 'tp'), may hold values from -0.375 to 0.375
- w_value: bfloat16 [256, 2048], P(None, 'tp'), may hold values from -0.375 to 0.375
- query_gain: float32 [192], replicated, may hold values from 0.1 to 1.9
- key_gain: float32 [192], replicated, may hold values from 0.1 to 1.9
- w_mix: bfloat16 [2048, 2048], P('tp'), may hold values from -3 to 3
- tokens_b: bfloat16 [12288, 2048], P(('ep', 'tp')), may hold values from -6 to 6
- norm_gain: float32 [2048], replicated, may hold values from 0.1 to 1.9
- expert_ids: int32 [12288, 2], P(('ep', 'tp')), may hold values from 0 to 31, all different within a row; in each aligned block of 48 rows (0 to 47, 48 to 95, ...) at most 4 rows name the same one
- route_weights: float32 [12288, 2], P(('ep', 'tp')), may hold values from 0.05 to 1
- w_gate: bfloat16 [32, 2048, 4096], P('ep', None, 'tp'), may hold values from -0.125 to 0.125
- w_up: bfloat16 [32, 2048, 4096], P('ep', None, 'tp'), may hold values from -0.125 to 0.125
- w_down: bfloat16 [32, 4096, 2048], P('ep', 'tp'), may hold values from -0.09375 to 0.09375
Outputs:
- mix_out: bfloat16 [12288, 2048], P(('ep', 'tp'))
- expert_out: bfloat16 [12288, 2048], P(('ep', 'tp'))
Inputs may be any that keep to these rules, and one draw needn't show every extreme that they name: `expert_ids`: each row names 2 different experts. Within the rows of one device, no expert is named more than 4 times, a bound that some block reaches.
All inputs are finite; a program needn't handle non-finite values.
Results may differ from a plain program's by a relative error of at most 0.018.
Values may be sent and summed in bfloat16 or wider, within the bound.
No kernel may reach another device: no remote copies, remote signals or barrier semaphores. Data moves between devices by JAX's collectives and lax.ppermute only.
A program may use at most 192 MiB of HBM per device.

v0:
```python
import jax
import jax.numpy as jnp
from jax import lax
from jax.sharding import PartitionSpec as P

NOPE_DIM = 128
ROPE_DIM = 64
VALUE_DIM = 128
EXPERTS = 32
TOP_K = 2


EPSILON = 1e-06
THETA = 10000.0


def sent_together(arrays, axis, dim, along):
    both = jnp.concatenate(arrays, axis=along)
    whole, at, outs = (lax.all_gather(both, axis, axis=dim, tiled=True), 0, [])
    for a in arrays:
        outs.append(lax.slice_in_dim(whole, at, at + a.shape[along], axis=along))
        at += a.shape[along]
    return tuple(outs)


def split_up(x, dim, peers):
    before, after = (x.shape[:dim], x.shape[dim + 1 :])
    return jnp.moveaxis(x.reshape(*before, peers, -1, *after), dim, 0)


def one_scatter(arrays, axis, dims):
    peers = lax.axis_size(axis)
    parts = [split_up(a, dim, peers) for a, dim in zip(arrays, dims)]
    lines = jnp.concatenate([b.reshape(peers, -1) for b in parts], axis=1)
    rows = max(16, -(-lines.shape[1] // 1024) * 8)
    lines = jnp.pad(lines, ((0, 0), (0, rows * 128 - lines.shape[1]))).reshape(-1, 128)
    ravelled, at, outs = (lax.psum_scatter(lines, axis, tiled=True).reshape(-1), 0, [])
    for b in parts:
        part = b[0]
        outs.append(ravelled[at : at + part.size].reshape(part.shape))
        at += part.size
    return tuple(outs)


def rms_scale(values, gains):
    return values * lax.rsqrt(jnp.mean(values * values, axis=-1, keepdims=True) + EPSILON) * gains


def rotate(values, positions):
    half_dim = values.shape[-1] // 2
    inverse = THETA ** (-jnp.arange(0, 2 * half_dim, 2, dtype=jnp.float32) / (2 * half_dim))
    angles = positions.astype(jnp.float32)[:, None] * inverse[None, :]
    view_shape = (positions.shape[0],) + (1,) * (values.ndim - 2) + (half_dim,)
    cosine = jnp.cos(angles).reshape(view_shape)
    sine_part = jnp.sin(angles).reshape(view_shape)
    first_half = values[..., :half_dim]
    second = values[..., half_dim:]
    return jnp.concatenate(
        [first_half * cosine - second * sine_part, second * cosine + first_half * sine_part],
        axis=-1,
    )


def attention(q_all, kv_all, rope_all, positions_q, w_query, w_key, w_value, query_gain, key_gain):
    rows_ep = q_all.shape[0]
    heads_dev = w_key.shape[1] // NOPE_DIM
    queries = jnp.dot(q_all, w_query, preferred_element_type=jnp.float32).reshape(
        rows_ep, heads_dev, NOPE_DIM + ROPE_DIM
    )
    queries = rms_scale(queries, query_gain)
    queries = jnp.concatenate(
        [queries[..., :NOPE_DIM], rotate(queries[..., NOPE_DIM:], positions_q)], axis=-1
    ).astype(jnp.bfloat16)
    score_scale = (NOPE_DIM + ROPE_DIM) ** (-0.5)
    latent, shared = sent_together((kv_all, rope_all), "ep", 0, 1)
    key_count = latent.shape[0]
    positions = jnp.arange(key_count, dtype=jnp.int32)
    keys = jnp.dot(latent, w_key, preferred_element_type=jnp.float32).reshape(
        key_count, heads_dev, NOPE_DIM
    )
    shared_rows = shared.astype(jnp.float32)[:, None, :]
    keys = rms_scale(jnp.concatenate([keys, shared_rows], axis=-1), key_gain)
    keys = jnp.concatenate(
        [keys[..., :NOPE_DIM], rotate(keys[..., NOPE_DIM:], positions)], axis=-1
    ).astype(jnp.bfloat16)
    values = jnp.dot(latent, w_value, preferred_element_type=jnp.float32).astype(jnp.bfloat16)
    values = values.reshape(key_count, heads_dev, VALUE_DIM)
    scores = (
        jnp.einsum("qhd,khd->hqk", queries, keys, preferred_element_type=jnp.float32) * score_scale
    )
    probs_f = jnp.exp(scores)
    totals = jnp.sum(probs_f, axis=-1)
    summed = jnp.einsum(
        "hqk,khv->hqv", probs_f.astype(jnp.bfloat16), values, preferred_element_type=jnp.float32
    )
    totals, summed = (totals, summed)
    return (summed / totals[..., None]).astype(jnp.bfloat16)


def expert_terms(pieces, w_gate, w_up, w_down):
    gate_pre = jnp.einsum("tsxcd,xdf->tsxcf", pieces, w_gate, preferred_element_type=jnp.float32)
    up_pre = jnp.einsum("tsxcd,xdf->tsxcf", pieces, w_up, preferred_element_type=jnp.float32)
    hidden = (jax.nn.silu(gate_pre) * up_pre).astype(jnp.bfloat16)
    return jnp.einsum("tsxcf,xfd->tsxcd", hidden, w_down, preferred_element_type=jnp.float32)


def on_device(
    q_latent,
    kv_latent,
    rope_key,
    q_latent_gain,
    kv_latent_gain,
    w_query,
    w_key,
    w_value,
    query_gain,
    key_gain,
    w_mix,
    tokens_b,
    norm_gain,
    expert_ids,
    route_weights,
    w_gate,
    w_up,
    w_down,
):
    tp_count = lax.axis_size("tp")
    ep_count = lax.axis_size("ep")
    local_rows = q_latent.shape[0]
    rows_ep = local_rows * tp_count
    width = tokens_b.shape[1]
    heads_dev = w_key.shape[1] // NOPE_DIM
    q_normed = rms_scale(q_latent.astype(jnp.float32), q_latent_gain).astype(jnp.bfloat16)
    kv_normed = rms_scale(kv_latent.astype(jnp.float32), kv_latent_gain).astype(jnp.bfloat16)
    positions_q = lax.axis_index("ep") * rows_ep + jnp.arange(rows_ep, dtype=jnp.int32)
    mix_weights = w_mix.reshape(heads_dev, VALUE_DIM, width)
    local_b = tokens_b.shape[0]
    capacity = max(2, local_b * TOP_K * 3 // (2 * EXPERTS))
    experts_dev = w_gate.shape[0]
    b_normed = rms_scale(tokens_b.astype(jnp.float32), norm_gain).astype(jnp.bfloat16)
    flat_ids = expert_ids.reshape(-1)
    expert_hot = (flat_ids[:, None] == jnp.arange(EXPERTS, dtype=jnp.int32)[None, :]).astype(
        jnp.int32
    )
    ranks = jnp.sum(expert_hot * (jnp.cumsum(expert_hot, axis=0) - 1), axis=1)
    slots = flat_ids * capacity + ranks
    slot_hot = (slots[:, None] == jnp.arange(EXPERTS * capacity, dtype=jnp.int32)[None, :]).astype(
        jnp.bfloat16
    )
    repeated = jnp.repeat(b_normed, TOP_K, axis=0)
    outgoing = jnp.einsum(
        "as,ad->sd", slot_hot, repeated, preferred_element_type=jnp.float32
    ).astype(jnp.bfloat16)
    outgoing = outgoing.reshape(ep_count, experts_dev * capacity, width)
    arrived = lax.all_to_all(outgoing, "ep", split_axis=0, concat_axis=0, tiled=True)
    arrived = arrived.reshape(1, ep_count, experts_dev, capacity, width)
    q_all, kv_all, rope_all, slots_all = (
        lax.all_gather(q_normed[None], "tp", axis=0, tiled=True),
        lax.all_gather(kv_normed[None], "tp", axis=0, tiled=True),
        lax.all_gather(rope_key[None], "tp", axis=0, tiled=True),
        lax.all_gather(arrived, "tp", axis=0, tiled=True),
    )
    head_out = attention(
        q_all.reshape(rows_ep, -1),
        kv_all.reshape(rows_ep, -1),
        rope_all.reshape(rows_ep, -1),
        positions_q,
        w_query,
        w_key,
        w_value,
        query_gain,
        key_gain,
    )
    mix_term = jnp.einsum("hqv,hvd->qd", head_out, mix_weights, preferred_element_type=jnp.float32)
    mix_term = mix_term.reshape(tp_count, local_rows, width)
    expert_term = expert_terms(slots_all, w_gate, w_up, w_down)
    mix_sum, expert_sum = tuple(
        (
            part.astype(jnp.float32)
            for part in one_scatter(
                (mix_term.astype(jnp.bfloat16), expert_term.astype(jnp.bfloat16)), "tp", (0, 0)
            )
        )
    )
    mix_out = mix_sum[0].astype(jnp.bfloat16)
    expert_done = expert_sum[0].astype(jnp.bfloat16)
    returning = expert_done.reshape(ep_count, experts_dev * capacity, width)
    returned = lax.all_to_all(returning, "ep", split_axis=0, concat_axis=0, tiled=True).reshape(
        EXPERTS * capacity, width
    )
    gathered_back = jnp.dot(slot_hot, returned, preferred_element_type=jnp.float32).reshape(
        local_b, TOP_K, width
    )
    expert_out = jnp.sum(gathered_back * route_weights[:, :, None], axis=1).astype(jnp.bfloat16)
    return (mix_out, expert_out)


def solution(mesh):
    in_specs = (
        P(("ep", "tp"), None),
        P(("ep", "tp"), None),
        P(("ep", "tp"), None),
        P(),
        P(),
        P(None, "tp"),
        P(None, "tp"),
        P(None, "tp"),
        P(),
        P(),
        P("tp", None),
        P(("ep", "tp"), None),
        P(),
        P(("ep", "tp"), None),
        P(("ep", "tp"), None),
        P("ep", None, "tp"),
        P("ep", None, "tp"),
        P("ep", "tp", None),
    )
    out_specs = (P(("ep", "tp"), None), P(("ep", "tp"), None))
    return jax.shard_map(
        on_device, mesh=mesh, in_specs=in_specs, out_specs=out_specs, check_vma=False
    )
```

profile of v0, /device:TPU:2, one launch (start us, length us, event | category | flops | bytes accessed | tf_op | source)
XLA Modules:
  0.0 369.2 jit_solution(14204939258254129752)
XLA Ops:
  9.1 21.0 %all-gather.1 = bf16[768,256]{1,0:T(8,128)(2,1)S(1)} all-gather(bf16[48,256]{1,0:T(8,128)(2,1)S(1)} %fusion.71), channel_id=3, replica_groups=mesh['ep'=16,'tp'=16] {'tp'}, dimensions={0}, use_global_device_ids=true | all-gather | bytes 417792 | tf_op jit(solution)/shard_map/all_gather | solution.py:159
  30.3 15.2 %all-gather.2 = bf16[768,64]{1,0:T(8,128)(2,1)S(1)} all-gather(bf16[48,64]{1,0:T(8,128)(2,1)} %param.20), channel_id=4, replica_groups=mesh['ep'=16,'tp'=16] {'tp'}, dimensions={0}, use_global_device_ids=true | all-gather | bytes 104448 | tf_op jit(solution)/shard_map/all_gather | solution.py:160
  50.4 1.2 fusion.14
  51.6 7.5 %all-to-all-start = ((bf16[16,8,2048]{2,1,0:T(8,128)(2,1)}), bf16[16,8,2048]{2,1,0:T(8,128)(2,1)S(1)}, u32[]{:S(2)}, u32[]{:S(2)}) async-start(bf16[16,8,2048]{2,1,0:T(8,128)(2,1)} %fusion.14), calls=%async_computation | async-start | bytes 1048576 | tf_op jit(solution)/shard_map/all_to_all | solution.py:155
  59.4 17.4 %all-gather = bf16[768,384]{1,0:T(8,128)(2,1)S(1)} all-gather(bf16[48,384]{1,0:T(8,128)(2,1)S(1)} %fusion.68), channel_id=2, replica_groups=mesh['ep'=16,'tp'=16] {'tp'}, dimensions={0}, use_global_device_ids=true | all-gather | bytes 626688 | tf_op jit(solution)/shard_map/all_gather | solution.py:158
  79.0 43.0 %all-gather.6.cloned.1.call-done = bf16[12288,320]{0,1:T(8,128)(2,1)} async-done(((bf16[768,320]{0,1:T(8,128)(2,1)}), bf16[12288,320]{0,1:T(8,128)(2,1)}) %all-gather.6.cloned.1.call-update) | async-done | bytes 7864336 | tf_op jit(solution)/shard_map/all_gather | solution.py:19
  122.0 3.8 %convolution_bitcast_fusion = f32[12288,1,128]{0,2,1:T(8,128)S(1)} fusion(bf16[256,128]{1,0:T(8,128)(2,1)S(1)} %copy-done.6, bf16[12288,320]{0,1:T(8,128)(2,1)} %all-gather.6.cloned.1.call-done), kind=kOutput, calls=%fused_computation.5 | convolution fusion | flops 805306368 | bytes 12648448 | tf_op jit(solution)/shard_map/dot_general | solution.py:78
  125.8 2.9 fusion.36
  130.3 6.3 %convolution_convert_fusion = bf16[12288,128]{1,0:T(8,128)(2,1)} fusion(bf16[256,128]{1,0:T(8,128)(2,1)S(1)} %copy-done.12, bf16[12288,320]{0,1:T(8,128)(2,1)} %all-gather.6.cloned.1.call-done), kind=kOutput, calls=%fused_computation.6 | convolution fusion | flops 806879232 | bytes 9502720 | tf_op jit(solution)/shard_map/dot_general | solution.py:86
  136.7 8.7 %multiply_multiply_fusion = f32[12288,1,192]{0,2,1:T(8,128)} fusion(f32[12288,1,64]{0,2,1:T(8,128)} %copy-done.2, f32[12288,1,128]{0,2,1:T(8,128)} %copy-done.1, f32[192]{0:T(256)S(1)} %copy-done.9, f32[12288]{0:T(1024)S(1)} %add_rsqrt_fusion), kind=kLoop, calls=%fused_computation.9 | loop fusion | flops 7077888 | bytes 18924288 | tf_op jit(solution)/shard_map/mul | solution.py:46
  145.4 9.0 %fusion.46 = (bf16[12288,32]{0,1:T(8,128)(2,1)S(1)}, bf16[12288,32]{0,1:T(8,128)(2,1)}) fusion(f32[12288,1,192]{0,2,1:T(8,128)} %multiply_multiply_fusion, f32[32]{0:T(128)S(1)} %multiply_power_fusion, f32[12288]{0:T(1024)S(1)} %iota_convert_fusion), kind=kLoop, calls=%fused_computation.55 | loop fusion | flops 3538944 | bytes 4767872 | tf_op jit(solution)/shard_map/concatenate | solution.py:83
  154.4 4.9 %fusion.13 = bf16[12288,128]{0,1:T(8,128)(2,1)} fusion(f32[12288,1,192]{0,2,1:T(8,128)} %multiply_multiply_fusion), kind=kLoop, calls=%fused_computation.22 | loop fusion | bytes 6291456 | tf_op jit(solution)/shard_map/concatenate | solution.py:83
  159.4 17.3 %fusion = (f32[768]{0:T(1024)S(1)}, f32[768,12288]{1,0:T(8,128)}) fusion(bf16[12288,32]{0,1:T(8,128)(2,1)} %get-tuple-element.3, bf16[12288,32]{0,1:T(8,128)(2,1)S(1)} %get-tuple-element.2, bf16[12288,128]{0,1:T(8,128)(2,1)} %fusion.13, bf16[768,32]{0,1:T(8,128)(2,1)S(1)} %get-tuple-element.5, bf16[768,32]{0,1:T(8,128)(2,1)S(1)} %get-tuple-element.4, ...), kind=kOutput, calls=%fused_computation.1 | convolution fusion | flops 3657792768 | bytes 42765312 | tf_op jit(solution)/shard_map/qhd,khd->hqk/dot_general | solution.py:89
  176.7 15.4 %fusion.41 = bf16[768,128]{1,0:T(8,128)(2,1)S(1)} fusion(bf16[12288,128]{1,0:T(8,128)(2,1)} %convolution_convert_fusion, f32[768,12288]{1,0:T(8,128)} %get-tuple-element.9, f32[768]{0:T(1024)S(1)} %get-tuple-element.8), kind=kOutput, calls=%fused_computation.52 | convolution fusion | flops 2434990080 | bytes 41094144 | tf_op jit(solution)/shard_map/hqk,khv->hqv/dot_general | solution.py:93
  193.1 3.5 copy.52
  196.6 7.6 %fusion.20 = f32[2,16,16,4,256]{4,2,3,1,0:T(8,128)} fusion(bf16[16,16,2,4,2048]{4,1,3,0,2:T(8,128)(2,1)} %all-gather.8.cloned.1.call-done, bf16[2,2048,256]{2,1,0:T(8,128)(2,1)} %param.34), kind=kOutput, calls=%fused_computation.33 | convolution fusion | flops 2147483648 | bytes 12582912 | tf_op jit(solution)/shard_map/tsxcd,xdf->tsxcf/dot_general | solution.py:102
  204.2 13.5 %convert_bitcast_fusion = bf16[16,16,2,4,2048]{4,1,3,0,2:T(8,128)(2,1)} fusion(bf16[2,256,2048]{2,1,0:T(8,128)(2,1)S(1)} %copy-done, f32[2,16,16,4,256]{4,2,3,1,0:T(8,128)} %fusion.20, bf16[16,16,2,4,2048]{4,1,3,0,2:T(8,128)(2,1)} %all-gather.8.cloned.1.call-done, bf16[2,2048,256]{2,1,0:T(8,128)(2,1)} %param.33), kind=kOutput, calls=%fused_computation.11 | convolution fusion | flops 4302307328 | bytes 23068672 | tf_op jit(solution)/shard_map/tsxcf,xfd->tsxcd/dot_general | solution.py:104
  217.7 11.1 %copy.47 = bf16[16,16,2,4,2048]{4,3,2,1,0:T(4,128)(2,1)} copy(bf16[16,16,2,4,2048]{4,1,3,0,2:T(8,128)(2,1)} %convert_bitcast_fusion) | data formatting | bytes 16777216 | tf_op jit(solution)/shard_map/convert_element_type | solution.py:181
  228.8 10.3 %reshape_reshape.7 = bf16[16,262144]{1,0:T(8,128)(2,1)} reshape(bf16[16,16,2,4,2048]{4,3,2,1,0:T(4,128)(2,1)} %copy.47) | data formatting | bytes 16777216 | tf_op jit(solution)/shard_map/reshape;reshape | solution.py:34
  239.0 12.5 %pad_maximum_fusion = bf16[16,360448]{1,0:T(8,128)(2,1)} fusion(bf16[16,262144]{1,0:T(8,128)(2,1)} %reshape_reshape.7, bf16[16,98304]{1,0:T(8,128)(2,1)} %bitcast.90), kind=kLoop, calls=%fused_computation.7 | loop fusion | flops 23068672 | bytes 23068672 | tf_op jit(solution)/shard_map/concatenate | solution.py:34
  251.5 15.4 %reshape.518 = bf16[45056,128]{1,0:T(8,128)(2,1)} reshape(bf16[16,360448]{1,0:T(8,128)(2,1)} %pad_maximum_fusion) | data formatting | bytes 23068672 | tf_op jit(solution)/shard_map/reshape | solution.py:36
  266.9 76.6 %reduce-scatter.2.cloned.1.call-done = bf16[2816,128]{1,0:T(8,128)(2,1)} async-done(((bf16[45056,128]{1,0:T(8,128)(2,1)}), bf16[2816,128]{1,0:T(8,128)(2,1)}) %reduce-scatter.2.cloned.1.call-update) | async-done | bytes 720912 | tf_op jit(solution)/shard_map/reduce_scatter | solution.py:37
  345.7 7.3 %all-to-all-start.1 = ((bf16[16,8,2048]{2,1,0:T(8,128)(2,1)}), bf16[16,8,2048]{2,1,0:T(8,128)(2,1)S(1)}, u32[]{:S(2)}, u32[]{:S(2)}) async-start(bf16[16,8,2048]{2,1,0:T(8,128)(2,1)} %reshape.520), calls=%async_computation.2 | async-start | bytes 1048576 | tf_op jit(solution)/shard_map/all_to_all | solution.py:188
  354.8 6.9 %all-to-all-done.1 = bf16[16,8,2048]{2,1,0:T(8,128)(2,1)S(1)} async-done(((bf16[16,8,2048]{2,1,0:T(8,128)(2,1)}), bf16[16,8,2048]{2,1,0:T(8,128)(2,1)S(1)}, u32[]{:S(2)}, u32[]{:S(2)}) %all-to-all-start.1) | async-done | bytes 524320 | tf_op jit(solution)/shard_map/all_to_all | solution.py:188
  (74 shorter events, 16.8 us)
Async XLA Ops:
  7.2 197.0 %copy-start = (bf16[2,256,2048]{2,1,0:T(8,128)(2,1)S(1)}, bf16[2,256,2048]{2,1,0:T(8,128)(2,1)}, u32[]{:S(2)}) copy-start(bf16[2,256,2048]{2,1,0:T(8,128)(2,1)} %param.35) | copy-start | bytes 6291460
  7.2 52.0 %copy-start.4 = (bf16[48,384]{1,0:T(8,128)(2,1)S(1)}, bf16[48,384]{1,0:T(8,128)(2,1)}, u32[]{:S(2)}) copy-start(bf16[48,384]{1,0:T(8,128)(2,1)} %param.18) | copy-start | bytes 110596
  7.2 52.1 %copy-start.8 = (f32[384]{0:T(512)S(1)}, f32[384]{0:T(512)}, u32[]{:S(2)}) copy-start(f32[384]{0:T(512)} %param.21) | copy-start | bytes 4612
  7.2 69.6 %copy-start.5 = (bf16[384,192]{0,1:T(8,128)(2,1)S(1)}, bf16[384,192]{0,1:T(8,128)(2,1)}, u32[]{:S(2)}) copy-start(bf16[384,192]{0,1:T(8,128)(2,1)} %param.23) | copy-start | bytes 442372
  7.2 70.0 %copy-start.11 = (f32[192]{0:T(256)S(1)}, f32[192]{0:T(256)}, u32[]{:S(2)}) copy-start(f32[192]{0:T(256)} %param.26) | copy-start | bytes 2308
  7.2 114.7 %all-gather.6.cloned.1.call-start = ((), (), s32[]{:S(2)}) async-start(), calls=%async_computation.3 | async-start | bytes 8355840 | tf_op jit(solution)/shard_map/all_gather | solution.py:19
  30.1 91.8 %copy-start.6 = (bf16[256,128]{1,0:T(8,128)(2,1)S(1)}, bf16[256,128]{1,0:T(8,128)(2,1)}, u32[]{:S(2)}) copy-start(bf16[256,128]{1,0:T(8,128)(2,1)} %param.24) | copy-start | bytes 196612
  51.6 26.2 %all-to-all-start = ((bf16[16,8,2048]{2,1,0:T(8,128)(2,1)}), bf16[16,8,2048]{2,1,0:T(8,128)(2,1)S(1)}, u32[]{:S(2)}, u32[]{:S(2)}) async-start(bf16[16,8,2048]{2,1,0:T(8,128)(2,1)} %fusion.14), calls=%async_computation | async-start | bytes 1048576 | tf_op jit(solution)/shard_map/all_to_all | solution.py:155
  59.1 137.5 %all-gather.8.cloned.1.call-start = ((), (), s32[]{:S(2)}) async-start(), calls=%async_computation.4 | async-start | bytes 8912896 | tf_op jit(solution)/shard_map/all_gather | solution.py:161
  78.9 264.6 %reduce-scatter.2.cloned.1.call-start = ((), (), s32[]{:S(2)}) async-start(), calls=%async_computation.5 | async-start | bytes 12255232 | tf_op jit(solution)/shard_map/reduce_scatter | solution.py:37
  125.8 3.7 copy-start.1
  125.8 4.5 %copy-start.12 = (bf16[256,128]{1,0:T(8,128)(2,1)S(1)}, bf16[256,128]{1,0:T(8,128)(2,1)}, u32[]{:S(2)}) copy-start(bf16[256,128]{1,0:T(8,128)(2,1)} %param.25) | copy-start | bytes 196612
  128.7 1.7 copy-start.2
  130.3 6.3 %copy-start.9 = (f32[192]{0:T(256)S(1)}, f32[192]{0:T(256)}, u32[]{:S(2)}) copy-start(f32[192]{0:T(256)} %param.27) | copy-start | bytes 2308
  176.7 15.5 %copy-start.3 = (bf16[128,2048]{1,0:T(8,128)(2,1)S(1)}, bf16[128,2048]{1,0:T(8,128)(2,1)}, u32[]{:S(2)}) copy-start(bf16[128,2048]{1,0:T(8,128)(2,1)} %param.28) | copy-start | bytes 1572868
  266.9 86.2 %copy-start.7 = (s32[48,2]{0,1:T(2,128)S(1)}, s32[48,2]{0,1:T(2,128)}, u32[]{:S(2)}) copy-start(s32[48,2]{0,1:T(2,128)} %param.31) | copy-start | bytes 1156
  266.9 94.8 %copy-start.10 = (f32[48,2]{0,1:T(2,128)S(1)}, f32[48,2]{0,1:T(2,128)}, u32[]{:S(2)}) copy-start(f32[48,2]{0,1:T(2,128)} %param.32) | copy-start | bytes 1156
  345.7 16.0 %all-to-all-start.1 = ((bf16[16,8,2048]{2,1,0:T(8,128)(2,1)}), bf16[16,8,2048]{2,1,0:T(8,128)(2,1)S(1)}, u32[]{:S(2)}, u32[]{:S(2)}) async-start(bf16[16,8,2048]{2,1,0:T(8,128)(2,1)} %reshape.520), calls=%async_computation.2 | async-start | bytes 1048576 | tf_op jit(solution)/shard_map/all_to_all | solution.py:188
Sparse Core Ops, SparseCore 0:
  46.7 75.2 all-gather.5
  123.8 55.5 all-gather.7
  267.1 76.4 reduce-scatter.1
where the time goes:
time: 370 us; the launch traced here: 369 us
  waiting for transfers between devices  127 us (34%)
  matrix products  67.6 us (18%)
  blocking collectives  53.7 us (15%)
  local copies, waits for them, and re-layouts  52.7 us (14%)
  other arithmetic  39.8 us (11%)
  starting transfers between devices  14.9 us (4%)
  between operations  14.1 us (4%)
    reduce_scatter x1, waiting for transfers between devices, one_scatter(): lax.psum_scatter(lines, axis, tiled=True).reshape(-1)  76.6 us
    all_gather x1, waiting for transfers between devices, sent_together(): whole, at, outs = (lax.all_gather(both, axis, axis=dim, tiled=True), 0, [])  43 us
    all_gather x1, blocking collectives, on_device(): lax.all_gather(kv_normed[None], 'tp', axis=0, tiled=True)  21 us
    all_gather x1, blocking collectives, on_device(): lax.all_gather(q_normed[None], 'tp', axis=0, tiled=True)  17.4 us
    dot_general x1, matrix products, attention(): jnp.einsum('qhd,khd->hqk', queries, keys, preferred_element_type=jnp.floa...  17.3 us
    dot_general x1, matrix products, attention(): jnp.einsum('hqk,khv->hqv', probs_f.astype(jnp.bfloat16), values, preferre...  15.4 us
    reshape x1, local copies, waits for them, and re-layouts, one_scatter(): jnp.pad(lines, ((0, 0), (0, rows * 128 - lines.shape[1]))).reshape(-1, 128)  15.4 us
    all_gather x1, blocking collectives, on_device(): lax.all_gather(rope_key[None], 'tp', axis=0, tiled=True)  15.2 us
  transfers between devices with their start and end apart: 5, of which 3 were waited for; matrix products, arithmetic and copies ran while one was open for 22% of the time, Pallas kernels for 0%

commit v1 on v0

v1 whole, which is shorter than its diff:
```python
import jax
import jax.numpy as jnp
from jax import lax
from jax.experimental import pallas as pl
from jax.experimental.pallas import tpu as pltpu
from jax.sharding import PartitionSpec as P


NOPE_DIM = 128
ROPE_DIM = 64
VALUE_DIM = 128
HEAD_DIM = NOPE_DIM + ROPE_DIM
EXPERTS = 32
TOP_K = 2
CAP = 4
SIDE = 4
EPSILON = 1e-06
THETA = 10000.0
LANES = 128
LOG2E = 1.4426950408889634

BF16 = jnp.bfloat16
F32 = jnp.float32


def params(mib=56):
    return pltpu.CompilerParams(vmem_limit_bytes=mib * 1024 * 1024)


def rms(values, gains):
    return values * lax.rsqrt(jnp.mean(values * values, axis=-1, keepdims=True) + EPSILON) * gains


def latent_body(q_ref, kv_ref, rope_ref, qg_ref, kvg_ref, out_ref):
    rows = q_ref.shape[0]
    q = rms(q_ref[...].astype(F32), qg_ref[...]).astype(BF16)
    kv = rms(kv_ref[...].astype(F32), kvg_ref[...]).astype(BF16)
    rope = rope_ref[...]
    parts = [p[:, j : j + LANES] for p in (q, kv) for j in range(0, p.shape[1], LANES)]
    parts.append(jnp.concatenate([rope, jnp.zeros_like(rope)], axis=1))
    for n, part in enumerate(parts):
        out_ref[n * rows : (n + 1) * rows, :] = part


def square(row):
    return jnp.broadcast_to(row, (row.shape[1], row.shape[1]))


def slots_of(rows, as_rows):
    count = rows.shape[1]
    line = lax.broadcasted_iota(jnp.int32, (count, count), 0)
    lane = lax.broadcasted_iota(jnp.int32, (count, count), 1)
    ids = [square(rows[k : k + 1, :].astype(F32)) for k in range(TOP_K)]
    outs = []
    for k in range(TOP_K):
        if as_rows:
            same = sum(jnp.where((p.T == ids[k]) & (line < lane), 1.0, 0.0) for p in ids)
            picked = ids[k][:1, :] * CAP + jnp.sum(same, axis=0, keepdims=True)
        else:
            mine = ids[k].T
            same = sum(jnp.where((p == mine) & (lane < line), 1.0, 0.0) for p in ids)
            picked = mine[:, :1] * CAP + jnp.sum(same, axis=1, keepdims=True)
        outs.append(picked.astype(jnp.int32))
    return outs


def dispatch_body(tok_ref, gain_ref, rows_ref, out_ref):
    normed = rms(tok_ref[...].astype(F32), gain_ref[...]).astype(BF16)
    first, second = slots_of(rows_ref[...], True)
    shape = (out_ref.shape[0], normed.shape[0])
    slot = lax.broadcasted_iota(jnp.int32, shape, 0)
    hot = jnp.where((slot == first) | (slot == second), 1.0, 0.0).astype(BF16)
    out_ref[...] = jnp.dot(hot, normed, preferred_element_type=F32).astype(BF16)


def collect_body(back_ref, rows_ref, weight_ref, out_ref):
    first, second = slots_of(rows_ref[...], False)
    count = out_ref.shape[0]
    slot = lax.broadcasted_iota(jnp.int32, (count, back_ref.shape[0]), 1)
    weights = [square(weight_ref[k : k + 1, :]).T[:, :1] for k in range(TOP_K)]
    mixed = jnp.where(slot == first, weights[0], 0.0) + jnp.where(slot == second, weights[1], 0.0)
    high = mixed.astype(BF16)
    rest = mixed - high.astype(F32)
    low = rest.astype(BF16)
    last = (rest - low.astype(F32)).astype(BF16)
    back = back_ref[...]
    total = jnp.dot(high, back, preferred_element_type=F32)
    total += jnp.dot(low, back, preferred_element_type=F32)
    total += jnp.dot(last, back, preferred_element_type=F32)
    out_ref[...] = total.astype(BF16)


def turned(values, cosine, sine):
    half = values.shape[-1] // 2
    swapped = jnp.concatenate([values[:, half:], values[:, :half]], axis=1)
    return values * cosine + swapped * sine


def project_body(
    lat_ref, wq_ref, wk_ref, wv_ref, qg_ref, kg_ref, cos_ref, sin_ref, q_ref, kv_ref, lat_q, lat_kv
):
    groups, height, _ = lat_ref.shape
    q_parts = lat_q.shape[1] // LANES
    kv_parts = lat_kv.shape[1] // LANES
    own = height // (q_parts + kv_parts + 1)
    half = groups * own // 2
    for j in range(q_parts + kv_parts):
        piece = lat_ref[:, j * own : (j + 1) * own, :].reshape(2 * half, LANES)
        dst, col = (lat_q, j) if j < q_parts else (lat_kv, j - q_parts)
        dst[:, col * LANES : (col + 1) * LANES] = piece
    rope = lat_ref[:, (q_parts + kv_parts) * own :, :].reshape(2 * half, LANES)[:, :ROPE_DIM]
    rope = rope.astype(F32)
    cosine, sine = cos_ref[...], sin_ref[...]
    queries = jnp.dot(lat_q[...], wq_ref[...], preferred_element_type=F32)
    scale = HEAD_DIM**-0.5 * LOG2E
    queries = rms(queries, qg_ref[...] * scale)
    q_ref[: 2 * half, :] = queries[:, :NOPE_DIM].astype(BF16)
    q_rope = turned(queries[:, NOPE_DIM:], cosine, sine).astype(BF16)
    q_ref[2 * half :, :] = jnp.concatenate([q_rope[:half], q_rope[half:]], axis=1)
    latent = lat_kv[...]
    keys = jnp.dot(latent, wk_ref[...], preferred_element_type=F32)
    square = jnp.sum(keys * keys, axis=-1, keepdims=True) + jnp.sum(
        rope * rope, axis=-1, keepdims=True
    )
    factor = lax.rsqrt(square / HEAD_DIM + EPSILON)
    gains = kg_ref[...]
    kv_ref[: 2 * half, :] = (keys * factor * gains[:, :NOPE_DIM]).astype(BF16)
    kv_ref[2 * half : 4 * half, :] = jnp.dot(
        latent, wv_ref[...], preferred_element_type=F32
    ).astype(BF16)
    k_rope = turned(rope * factor * gains[:, NOPE_DIM:], cosine, sine).astype(BF16)
    kv_ref[4 * half :, :] = jnp.concatenate([k_rope[:half], k_rope[half:]], axis=1)


def attend_body(*refs):
    q_refs, kv_refs, out_refs = refs[:SIDE], refs[SIDE : 2 * SIDE], refs[2 * SIDE : 3 * SIDE]
    qs, ks, vs, acc_ref = refs[3 * SIDE :]
    rows = qs.shape[0] // SIDE
    half = rows // 2
    zero = jnp.zeros((half, ROPE_DIM), BF16)
    ones = jnp.ones((rows, LANES), BF16)
    for b in range(SIDE):
        at = b * rows
        for src, dst, off in ((q_refs[b], qs, rows), (kv_refs[b], ks, 2 * rows)):
            dst[at : at + rows, :NOPE_DIM] = src[:rows, :]
            packed = src[off : off + half, :]
            dst[at : at + half, NOPE_DIM:] = jnp.concatenate([packed[:, :ROPE_DIM], zero], axis=1)
            dst[at + half : at + rows, NOPE_DIM:] = jnp.concatenate(
                [packed[:, ROPE_DIM:], zero], axis=1
            )
        vs[at : at + rows, :VALUE_DIM] = kv_refs[b][rows : 2 * rows, :]
        vs[at : at + rows, VALUE_DIM:] = ones

    def block(i, carry):
        here = pl.ds(pl.multiple_of(i * rows, rows), rows)
        q = qs[here, :]
        acc = None
        for b in range(SIDE):
            there = slice(b * rows, (b + 1) * rows)
            scores = lax.dot_general(
                q, ks[there, :], (((1,), (1,)), ((), ())), preferred_element_type=F32
            )
            probs = jnp.exp2(scores).astype(BF16)
            term = jnp.dot(probs, vs[there, :], preferred_element_type=F32)
            acc = term if acc is None else acc + term
        acc_ref[here, :] = acc
        return carry

    lax.fori_loop(0, SIDE, block, 0)
    for b in range(SIDE):
        at = b * rows
        out_refs[b][:rows, :] = acc_ref[at : at + rows, :VALUE_DIM].astype(BF16)
        for j in range(rows // LANES):
            total = acc_ref[at + j * LANES : at + (j + 1) * LANES, VALUE_DIM:].T[0:1, :]
            high = total.astype(BF16)
            low = (total - high.astype(F32)).astype(BF16)
            out_refs[b][rows + j : rows + j + 1, :] = high
            out_refs[b][rows + 8 + j : rows + 8 + j + 1, :] = low


def mix_body(*refs):
    parts = refs[:SIDE]
    w_ref, _, out_ref, head_ref, term_ref, sems = refs[SIDE:]
    rows = head_ref.shape[0]
    owners, span, _ = out_ref.shape
    own = rows // owners
    count = rows // LANES
    total = sum(p[rows : rows + 8, :].astype(F32) + p[rows + 8 : rows + 16, :].astype(F32) for p in parts)
    inverse = 1.0 / total
    for j in range(count):
        there = slice(j * LANES, (j + 1) * LANES)
        scale = jnp.broadcast_to(inverse[j : j + 1, :], (LANES, LANES)).T
        head = sum(p[there, :].astype(F32) for p in parts)
        head_ref[there, :] = (head * scale).astype(BF16)
    copies = []
    step = owners // 4
    for c in range(4):
        there = slice(c * step * own, (c + 1) * step * own)
        term_ref[there, :] = jnp.dot(
            head_ref[there, :], w_ref[...], preferred_element_type=F32
        ).astype(BF16)
        for i in range(c * step, (c + 1) * step):
            copy = pltpu.make_async_copy(
                term_ref.at[pl.ds(i * own, own), :],
                out_ref.at[i, pl.ds(span - own, own), :],
                sems.at[i],
            )
            copy.start()
            copies.append(copy)
    for copy in copies:
        copy.wait()


def expert_body(x_ref, gate_ref, up_ref, down_ref, out_ref):
    groups, _, rows, width = x_ref.shape
    x = x_ref[...].reshape(groups * rows, width)
    gate = jnp.dot(x, gate_ref[0], preferred_element_type=F32)
    up = jnp.dot(x, up_ref[0], preferred_element_type=F32)
    hidden = (gate / (1.0 + jnp.exp(-gate)) * up).astype(BF16)
    out = jnp.dot(hidden, down_ref[0], preferred_element_type=F32).astype(BF16)
    out_ref[...] = out.reshape(groups, rows, width)


def shift(axis_x, axis_y):
    return [
        (y * SIDE + x, ((y + axis_y) % SIDE) * SIDE + (x + axis_x) % SIDE)
        for y in range(SIDE)
        for x in range(SIDE)
    ]


def on_device(
    q_latent,
    kv_latent,
    rope_key,
    q_latent_gain,
    kv_latent_gain,
    w_query,
    w_key,
    w_value,
    query_gain,
    key_gain,
    w_mix,
    tokens_b,
    norm_gain,
    expert_ids,
    route_weights,
    w_gate,
    w_up,
    w_down,
):
    tp_count = lax.axis_size("tp")
    ep_count = lax.axis_size("ep")
    own = q_latent.shape[0]
    rows = own * tp_count
    width = tokens_b.shape[1]
    experts_dev = w_gate.shape[0]
    slots = EXPERTS * CAP

    height = own * ((q_latent.shape[1] + kv_latent.shape[1]) // LANES + 1)
    latent = pl.pallas_call(
        latent_body,
        out_shape=jax.ShapeDtypeStruct((height, LANES), BF16),
        compiler_params=params(),
        name="latents",
    )(q_latent, kv_latent, rope_key, q_latent_gain[None], kv_latent_gain[None])

    latent, tokens_b = lax.optimization_barrier((latent, tokens_b))
    id_rows = expert_ids.T
    outgoing = pl.pallas_call(
        dispatch_body,
        out_shape=jax.ShapeDtypeStruct((slots, width), BF16),
        compiler_params=params(),
        name="dispatch",
    )(tokens_b, norm_gain[None], id_rows)

    latents = lax.all_gather(latent, "tp", axis=0)

    arrived = lax.all_to_all(outgoing.reshape(ep_count, slots // ep_count, width), "ep", 0, 0)
    arrived = arrived.reshape(slots, width)
    at = jnp.arange(slots, dtype=jnp.int32)
    moved = (at % (slots // experts_dev)) // CAP * (experts_dev * CAP) + at // (
        slots // experts_dev
    ) * CAP + at % CAP
    turn = (moved[:, None] == at[None, :]).astype(BF16)
    grouped = jnp.dot(turn, arrived, preferred_element_type=F32).astype(BF16)
    everyone = lax.all_gather(grouped, "tp", axis=0, tiled=True)
    everyone = everyone.reshape(tp_count, experts_dev, slots // experts_dev, width)

    positions = lax.axis_index("ep") * rows + jnp.arange(rows, dtype=jnp.int32)
    inverse = THETA ** (-jnp.arange(0, ROPE_DIM, 2, dtype=F32) / ROPE_DIM)
    angles = positions.astype(F32)[:, None] * inverse[None, :]
    cosine, sine = jnp.cos(angles), jnp.sin(angles)
    cosine = jnp.concatenate([cosine, cosine], axis=1)
    sine = jnp.concatenate([-sine, sine], axis=1)

    q_own, kv_own = pl.pallas_call(
        project_body,
        out_shape=(
            jax.ShapeDtypeStruct((rows + rows // 2, LANES), BF16),
            jax.ShapeDtypeStruct((2 * rows + rows // 2, LANES), BF16),
        ),
        scratch_shapes=[
            pltpu.VMEM((rows, q_latent.shape[1]), BF16),
            pltpu.VMEM((rows, kv_latent.shape[1]), BF16),
        ],
        compiler_params=params(),
        name="project",
    )(latents, w_query, w_key, w_value, query_gain[None], key_gain[None], cosine, sine)

    kv_all = [kv_own] + [lax.ppermute(kv_own, "ep", shift(d, 0)) for d in (1, 3, 2)]
    q_all = [q_own] + [lax.ppermute(q_own, "ep", shift(0, d)) for d in (1, 3, 2)]
    partial = pl.pallas_call(
        attend_body,
        out_shape=[jax.ShapeDtypeStruct((rows + 16, LANES), BF16)] * SIDE,
        scratch_shapes=[pltpu.VMEM((SIDE * rows, 2 * LANES), BF16)] * 3
        + [pltpu.VMEM((SIDE * rows, 2 * LANES), F32)],
        compiler_params=params(),
        name="attend",
    )(*q_all, *kv_all)
    parts = [partial[0]] + [
        lax.ppermute(p, "ep", shift(0, -d)) for p, d in zip(partial[1:], (1, 3, 2))
    ]

    span = slots + own
    share = slots // experts_dev
    step = tp_count // 2
    hidden = w_gate.shape[2]
    terms = pl.pallas_call(
        expert_body,
        out_shape=jax.ShapeDtypeStruct((tp_count, span, width), BF16),
        grid=(experts_dev, tp_count // step),
        in_specs=[
            pl.BlockSpec((step, 1, share, width), lambda x, j: (j, x, 0, 0)),
            pl.BlockSpec((1, width, hidden), lambda x, j: (x, 0, 0)),
            pl.BlockSpec((1, width, hidden), lambda x, j: (x, 0, 0)),
            pl.BlockSpec((1, hidden, width), lambda x, j: (x, 0, 0)),
        ],
        out_specs=pl.BlockSpec((step, share, width), lambda x, j: (j, x, 0)),
        compiler_params=params(),
        name="experts",
    )(everyone, w_gate, w_up, w_down)

    terms = pl.pallas_call(
        mix_body,
        out_shape=jax.ShapeDtypeStruct((tp_count, span, width), BF16),
        in_specs=[pl.BlockSpec(memory_space=pltpu.VMEM)] * (SIDE + 1)
        + [pl.BlockSpec(memory_space=pl.ANY)],
        out_specs=pl.BlockSpec(memory_space=pl.ANY),
        scratch_shapes=[
            pltpu.VMEM((rows, VALUE_DIM), BF16),
            pltpu.VMEM((rows, width), BF16),
            pltpu.SemaphoreType.DMA((tp_count,)),
        ],
        input_output_aliases={SIDE + 1: 0},
        compiler_params=params(),
        name="mix",
    )(*parts, w_mix, terms)

    summed = lax.psum_scatter(
        terms.reshape(tp_count * span, width), "tp", scatter_dimension=0, tiled=True
    )
    mix_out = summed[slots:]
    done = jnp.dot(turn.T, summed[:slots], preferred_element_type=F32).astype(BF16)
    returned = lax.all_to_all(done.reshape(ep_count, slots // ep_count, width), "ep", 0, 0)
    expert_out = pl.pallas_call(
        collect_body,
        out_shape=jax.ShapeDtypeStruct((own, width), BF16),
        compiler_params=params(),
        name="collect",
    )(returned.reshape(slots, width), id_rows, route_weights.T)
    return (mix_out, expert_out)


def solution(mesh):
    in_specs = (
        P(("ep", "tp"), None),
        P(("ep", "tp"), None),
        P(("ep", "tp"), None),
        P(),
        P(),
        P(None, "tp"),
        P(None, "tp"),
        P(None, "tp"),
        P(),
        P(),
        P("tp", None),
        P(("ep", "tp"), None),
        P(),
        P(("ep", "tp"), None),
        P(("ep", "tp"), None),
        P("ep", None, "tp"),
        P("ep", None, "tp"),
        P("ep", "tp", None),
    )
    out_specs = (P(("ep", "tp"), None), P(("ep", "tp"), None))

    return jax.shard_map(
        on_device, mesh=mesh, in_specs=in_specs, out_specs=out_specs, check_vma=False
    )
```

time: 370 us -> 230 us (0.62)
  matrix products: 67.6 us -> 3.39 us
  blocking collectives: 53.7 us -> 0 us
  local copies, waits for them, and re-layouts: 52.7 us -> 6.75 us
  Pallas kernels: 0 us -> 45.6 us
  other arithmetic: 39.8 us -> 2.66 us
  starting transfers between devices: 14.9 us -> 28.1 us
    dot_general x10 -> x2, matrix products: 67.6 us -> 3.39 us  [the longest x1 2.25 us: on_device(): jnp.dot(turn.T, summed[:slots], preferred_element_type=F32).astype(BF16)]
    all_gather x3 -> x0, blocking collectives: 53.7 us -> none  [the longest x1 21 us: on_device(): lax.all_gather(kv_normed[None], 'tp', axis=0, tiled=True)]
    pallas_call x0 -> x7, Pallas kernels: none -> 45.6 us  [the longest x1 17.4 us: on_device(): pl.pallas_call(attend_body, out_shape=[jax.ShapeDtypeStruct((rows + 16, L...]
    all_gather x2, waiting for transfers between devices: 43 us -> 18.5 us  [the longest x1 17.3 us: on_device(): latents = lax.all_gather(latent, 'tp', axis=0)]
    concatenate x5 -> x1, other arithmetic: 25.6 us -> 1.18 us  [on_device(): cosine = jnp.concatenate([cosine, cosine], axis=1)]
    ppermute x0 -> x9, waiting for transfers between devices: none -> 17.9 us  [the longest x3 10 us: on_device(): lax.ppermute(q_own, 'ep', shift(0, d))]
    reshape x5 -> x0, local copies, waits for them, and re-layouts: 17.5 us -> none  [the longest x1 15.4 us: one_scatter(): jnp.pad(lines, ((0, 0), (0, rows * 128 - lines.shape[1]))).reshape(-1, 128)]
    ppermute x0 -> x9, starting transfers between devices: none -> 13.2 us  [the longest x3 6.44 us: on_device(): lax.ppermute(q_own, 'ep', shift(0, d))]
  transfers between devices with their start and end apart: 5 -> 14, of which waited for: 3 -> 10; matrix products, arithmetic and copies ran while one was open for 22% -> 3% of each run, Pallas kernels for 0% -> 17%
where the time goes in v1:
time: 230 us
  waiting for transfers between devices  129 us (56%)
  Pallas kernels  45.6 us (20%)
  starting transfers between devices  28.1 us (12%)
  between operations  13.8 us (6%)
  local copies, waits for them, and re-layouts  6.75 us (3%)
  matrix products  3.39 us (1%)
  other arithmetic  2.66 us (1%)
    reduce_scatter x1, waiting for transfers between devices, on_device(): lax.psum_scatter(terms.reshape(tp_count * span, width), 'tp', scatter_dim...  75.4 us
    pallas_call x1, Pallas kernels, on_device(): pl.pallas_call(attend_body, out_shape=[jax.ShapeDtypeStruct((rows + 16, L...  17.4 us
    all_gather x1, waiting for transfers between devices, on_device(): latents = lax.all_gather(latent, 'tp', axis=0)  17.3 us
    pallas_call x1, Pallas kernels, on_device(): pl.pallas_call(expert_body, out_shape=jax.ShapeDtypeStruct((tp_count, spa...  13.3 us
    all_to_all x1, waiting for transfers between devices, on_device(): lax.all_to_all(outgoing.reshape(ep_count, slots // ep_count, width), 'ep'...  10.1 us
    ppermute x3, waiting for transfers between devices, on_device(): lax.ppermute(q_own, 'ep', shift(0, d))  10 us
    ppermute x3, waiting for transfers between devices, on_device(): lax.ppermute(kv_own, 'ep', shift(d, 0))  7.91 us
    all_to_all x1, starting transfers between devices, on_device(): lax.all_to_all(outgoing.reshape(ep_count, slots // ep_count, width), 'ep'...  7.48 us
  transfers between devices with their start and end apart: 14, of which 10 were waited for; matrix products, arithmetic and copies ran while one was open for 3% of the time, Pallas kernels for 17%

profile of v1, /device:TPU:2, one launch (start us, length us, event | category | flops | bytes accessed | tf_op | source)
XLA Modules:
  0.0 229.5 jit_solution(7591664234296087186)
XLA Ops:
  8.5 1.5 latents.1
  10.1 2.2 dispatch.1
  12.2 7.5 %all-to-all-start = ((bf16[16,8,2048]{2,1,0:T(8,128)(2,1)}), bf16[16,8,2048]{2,1,0:T(8,128)(2,1)S(1)}, u32[]{:S(2)}, u32[]{:S(2)}) async-start(bf16[16,8,2048]{2,1,0:T(8,128)(2,1)} %bitcast.19), calls=%async_computation | async-start | bytes 1048576 | tf_op jit(solution)/shard_map/all_to_all | solution.py:279
  19.8 10.1 %all-to-all-done = bf16[16,8,2048]{2,1,0:T(8,128)(2,1)S(1)} async-done(((bf16[16,8,2048]{2,1,0:T(8,128)(2,1)}), bf16[16,8,2048]{2,1,0:T(8,128)(2,1)S(1)}, u32[]{:S(2)}, u32[]{:S(2)}) %all-to-all-start) | async-done | bytes 524320 | tf_op jit(solution)/shard_map/all_to_all | solution.py:279
  32.0 1.5 fusion.3
  34.6 17.3 %all-gather.6.cloned.1.call-done = bf16[4608,128]{1,0:T(8,128)(2,1)} async-done(((bf16[288,128]{1,0:T(8,128)(2,1)}), bf16[4608,128]{1,0:T(8,128)(2,1)}) %all-gather.6.cloned.1.call-update) | async-done | bytes 1179664 | tf_op jit(solution)/shard_map/all_gather | solution.py:277
  51.9 5.2 %project.1 = (bf16[1152,128]{1,0:T(8,128)(2,1)}, bf16[1920,128]{1,0:T(8,128)(2,1)}) custom-call(bf16[16,288,128]{2,1,0:T(8,128)(2,1)} %bitcast.20, bf16[384,192]{1,0:T(8,128)(2,1)} %copy.23.wq_ref, bf16[256,128]{1,0:T(8,128)(2,1)} %wk_ref.1, bf16[256,128]{1,0:T(8,128)(2,1)} %wv_ref.1, f32[1,192]{1,0:T(1,128)} %bitcast.25, f32[1,192]{1,0:T(1,128)} %bitcast.26, ...), custom_call_target="tpu_custom_call" | custom-call | tf_op jit(solution)/shard_map/project/pallas_call | solution.py:297
  57.1 3.0 %collective-permute-start.2 = (bf16[1152,128]{1,0:T(8,128)(2,1)}, bf16[1152,128]{1,0:T(8,128)(2,1)S(1)}, u32[]{:S(2)}, u32[]{:S(2)}) collective-permute-start(bf16[1152,128]{1,0:T(8,128)(2,1)} %get-tuple-element.11.refs_0_), channel_id=1, source_target_pairs={{0,128},{16,144},{32,160},{48,176},{64,192},{80,208},{96,224},{112... | collective-permute-start | bytes 884744 | tf_op jit(solution)/shard_map/ppermute | solution.py:312
  60.1 2.1 collective-permute-start.5
  62.2 1.5 collective-permute-start.4
  65.4 2.6 %collective-permute-done.2.refs_3_ = bf16[1152,128]{1,0:T(8,128)(2,1)S(1)} collective-permute-done((bf16[1152,128]{1,0:T(8,128)(2,1)}, bf16[1152,128]{1,0:T(8,128)(2,1)S(1)}, u32[]{:S(2)}, u32[]{:S(2)}) %collective-permute-start.2) | collective-permute-done | bytes 294944 | tf_op jit(solution)/shard_map/ppermute | solution.py:312
  67.9 2.3 collective-permute-start
  70.2 4.1 %collective-permute-done.1.refs_2_ = bf16[1152,128]{1,0:T(8,128)(2,1)S(1)} collective-permute-done((bf16[1152,128]{1,0:T(8,128)(2,1)}, bf16[1152,128]{1,0:T(8,128)(2,1)S(1)}, u32[]{:S(2)}, u32[]{:S(2)}) %collective-permute-start.1) | collective-permute-done | bytes 294944 | tf_op jit(solution)/shard_map/ppermute | solution.py:312
  74.3 3.3 %collective-permute-done.refs_1_ = bf16[1152,128]{1,0:T(8,128)(2,1)S(1)} collective-permute-done((bf16[1152,128]{1,0:T(8,128)(2,1)}, bf16[1152,128]{1,0:T(8,128)(2,1)S(1)}, u32[]{:S(2)}, u32[]{:S(2)}) %collective-permute-start) | collective-permute-done | bytes 294944 | tf_op jit(solution)/shard_map/ppermute | solution.py:312
  77.6 7.8 %collective-permute-done.4.refs_6_ = bf16[1920,128]{1,0:T(8,128)(2,1)S(1)} collective-permute-done((bf16[1920,128]{1,0:T(8,128)(2,1)}, bf16[1920,128]{1,0:T(8,128)(2,1)S(1)}, u32[]{:S(2)}, u32[]{:S(2)}) %collective-permute-start.4) | collective-permute-done | bytes 491552 | tf_op jit(solution)/shard_map/ppermute | solution.py:311
  87.0 17.4 %attend.1 = (bf16[784,128]{1,0:T(8,128)(2,1)}, bf16[784,128]{1,0:T(8,128)(2,1)}, bf16[784,128]{1,0:T(8,128)(2,1)}, bf16[784,128]{1,0:T(8,128)(2,1)}) custom-call(bf16[1152,128]{1,0:T(8,128)(2,1)} %get-tuple-element.11.refs_0_, bf16[1152,128]{1,0:T(8,128)(2,1)} %copy-done.6, bf16[1152,128]{1,0:T(8,128)(2,1)} %copy-done.5, bf16[1152,128]{1,0:T(8,128)(2,1)} %copy-done.4, ...), custom_call_target="tpu_custom_call" | custom-call | tf_op jit(solution)/shard_map/attend/pallas_call | solution.py:313
  108.3 13.3 %experts.1.refs_5_ = bf16[16,176,2048]{2,1,0:T(8,128)(2,1)} custom-call(bf16[16,2,64,2048]{3,2,1,0:T(8,128)(2,1)} %bitcast.17, bf16[2,2048,256]{2,1,0:T(8,128)(2,1)} %gate_ref.1, bf16[2,2048,256]{2,1,0:T(8,128)(2,1)} %up_ref.1, bf16[2,256,2048]{2,1,0:T(8,128)(2,1)} %down_ref.1), custom_call_target="tpu_custom_call" | custom-call | tf_op jit(solution)/shard_map/experts/pallas_call | solution.py:329
  122.4 3.7 %mix.1 = bf16[16,176,2048]{2,1,0:T(8,128)(2,1)} custom-call(bf16[784,128]{1,0:T(8,128)(2,1)} %get-tuple-element.13.refs_0_, bf16[784,128]{1,0:T(8,128)(2,1)} %copy-done.7, bf16[784,128]{1,0:T(8,128)(2,1)} %copy-done.8, bf16[784,128]{1,0:T(8,128)(2,1)} %copy-done.9, bf16[128,2048]{1,0:T(8,128)(2,1)} %refs_4_.1, ...), custom_call_target="tpu_custom_call", output_to_operand_aliasing={{}: (5, {})} | custom-call | tf_op jit(solution)/shard_map/mix/pallas_call | solution.py:344
  126.1 75.4 %reduce-scatter.2.cloned.1.call-done = bf16[176,2048]{1,0:T(8,128)(2,1)} async-done(((bf16[2816,2048]{1,0:T(8,128)(2,1)}), bf16[176,2048]{1,0:T(8,128)(2,1)}) %reduce-scatter.2.cloned.1.call-update) | async-done | bytes 720912 | tf_op jit(solution)/shard_map/reduce_scatter | solution.py:360
  201.5 2.2 fusion
  203.8 7.3 %all-to-all-start.1 = ((bf16[16,8,2048]{2,1,0:T(8,128)(2,1)}), bf16[16,8,2048]{2,1,0:T(8,128)(2,1)S(1)}, u32[]{:S(2)}, u32[]{:S(2)}) async-start(bf16[16,8,2048]{2,1,0:T(8,128)(2,1)} %fusion), calls=%async_computation.2 | async-start | bytes 1048576 | tf_op jit(solution)/shard_map/all_to_all | solution.py:365
  211.0 1.6 slice.8
  212.7 7.2 %all-to-all-done.1 = bf16[16,8,2048]{2,1,0:T(8,128)(2,1)S(1)} async-done(((bf16[16,8,2048]{2,1,0:T(8,128)(2,1)}), bf16[16,8,2048]{2,1,0:T(8,128)(2,1)S(1)}, u32[]{:S(2)}, u32[]{:S(2)}) %all-to-all-start.1) | async-done | bytes 524320 | tf_op jit(solution)/shard_map/all_to_all | solution.py:365
  220.6 2.4 %collect.1 = bf16[48,2048]{1,0:T(8,128)(2,1)} custom-call(bf16[128,2048]{1,0:T(8,128)(2,1)} %bitcast.18, s32[2,48]{1,0:T(2,128)} %bitcast.23, f32[2,48]{1,0:T(2,128)} %bitcast.27), custom_call_target="tpu_custom_call" | custom-call | tf_op jit(solution)/shard_map/collect/pallas_call | solution.py:366
  (46 shorter events, 13.3 us)
Async XLA Ops:
  7.2 23.9 %copy-start.10 = (bf16[384,192]{0,1:T(8,128)(2,1)S(1)}, bf16[384,192]{0,1:T(8,128)(2,1)}, u32[]{:S(2)}) copy-start(bf16[384,192]{0,1:T(8,128)(2,1)} %param.23) | copy-start | bytes 442372
  7.2 44.7 %all-gather.6.cloned.1.call-start = ((), (), s32[]{:S(2)}) async-start(), calls=%async_computation.5 | async-start | bytes 1253376 | tf_op jit(solution)/shard_map/all_gather | solution.py:277
  12.2 17.6 %all-to-all-start = ((bf16[16,8,2048]{2,1,0:T(8,128)(2,1)}), bf16[16,8,2048]{2,1,0:T(8,128)(2,1)S(1)}, u32[]{:S(2)}, u32[]{:S(2)}) async-start(bf16[16,8,2048]{2,1,0:T(8,128)(2,1)} %bitcast.19), calls=%async_computation | async-start | bytes 1048576 | tf_op jit(solution)/shard_map/all_to_all | solution.py:279
  19.7 88.6 %all-gather.4.cloned.1.call-start = ((), (), s32[]{:S(2)}) async-start(), calls=%async_computation.3 | async-start | bytes 8912896 | tf_op jit(solution)/shard_map/all_gather | solution.py:287
  31.1 170.5 %reduce-scatter.2.cloned.1.call-start = ((), (), s32[]{:S(2)}) async-start(), calls=%async_computation.4 | async-start | bytes 12255232 | tf_op jit(solution)/shard_map/reduce_scatter | solution.py:360
  57.1 10.8 %collective-permute-start.2 = (bf16[1152,128]{1,0:T(8,128)(2,1)}, bf16[1152,128]{1,0:T(8,128)(2,1)S(1)}, u32[]{:S(2)}, u32[]{:S(2)}) collective-permute-start(bf16[1152,128]{1,0:T(8,128)(2,1)} %get-tuple-element.11.refs_0_), channel_id=1, source_target_pairs={{0,128},{16,144},{32,160},{48,176},{64,192},{80,208},{96,224},{112... | collective-permute-start | bytes 884744 | tf_op jit(solution)/shard_map/ppermute | solution.py:312
  60.1 17.5 %collective-permute-start.5 = (bf16[1920,128]{1,0:T(8,128)(2,1)}, bf16[1920,128]{1,0:T(8,128)(2,1)S(1)}, u32[]{:S(2)}, u32[]{:S(2)}) collective-permute-start(bf16[1920,128]{1,0:T(8,128)(2,1)} %get-tuple-element.12.refs_4_), channel_id=1, source_target_pairs={{0,32},{16,48},{32,0},{48,16},{64,96},{80,112},{96,64},{112,80},{1... | collective-permute-start | bytes 1474568 | tf_op jit(solution)/shard_map/ppermute | solution.py:311
  62.2 23.2 %collective-permute-start.4 = (bf16[1920,128]{1,0:T(8,128)(2,1)}, bf16[1920,128]{1,0:T(8,128)(2,1)S(1)}, u32[]{:S(2)}, u32[]{:S(2)}) collective-permute-start(bf16[1920,128]{1,0:T(8,128)(2,1)} %get-tuple-element.12.refs_4_), channel_id=1, source_target_pairs={{0,48},{16,0},{32,16},{48,32},{64,112},{80,64},{96,80},{112,96},{1... | collective-permute-start | bytes 1474568 | tf_op jit(solution)/shard_map/ppermute | solution.py:311
  63.7 21.8 %collective-permute-start.3 = (bf16[1920,128]{1,0:T(8,128)(2,1)}, bf16[1920,128]{1,0:T(8,128)(2,1)S(1)}, u32[]{:S(2)}, u32[]{:S(2)}) collective-permute-start(bf16[1920,128]{1,0:T(8,128)(2,1)} %get-tuple-element.12.refs_4_), channel_id=1, source_target_pairs={{0,16},{16,32},{32,48},{48,0},{64,80},{80,96},{96,112},{112,64},{1... | collective-permute-start | bytes 1474568 | tf_op jit(solution)/shard_map/ppermute | solution.py:311
  64.2 10.1 %collective-permute-start.1 = (bf16[1152,128]{1,0:T(8,128)(2,1)}, bf16[1152,128]{1,0:T(8,128)(2,1)S(1)}, u32[]{:S(2)}, u32[]{:S(2)}) collective-permute-start(bf16[1152,128]{1,0:T(8,128)(2,1)} %get-tuple-element.11.refs_0_), channel_id=1, source_target_pairs={{0,192},{16,208},{32,224},{48,240},{64,0},{80,16},{96,32},{112,48}... | collective-permute-start | bytes 884744 | tf_op jit(solution)/shard_map/ppermute | solution.py:312
  67.9 17.6 %copy-start.4 = (bf16[1152,128]{1,0:T(8,128)(2,1)}, bf16[1152,128]{1,0:T(8,128)(2,1)S(1)}, u32[]{:S(2)}) copy-start(bf16[1152,128]{1,0:T(8,128)(2,1)S(1)} %collective-permute-done.2.refs_3_) | copy-start | bytes 884740
  67.9 9.7 %collective-permute-start = (bf16[1152,128]{1,0:T(8,128)(2,1)}, bf16[1152,128]{1,0:T(8,128)(2,1)S(1)}, u32[]{:S(2)}, u32[]{:S(2)}) collective-permute-start(bf16[1152,128]{1,0:T(8,128)(2,1)} %get-tuple-element.11.refs_0_), channel_id=1, source_target_pairs={{0,64},{16,80},{32,96},{48,112},{64,128},{80,144},{96,160},{112,17... | collective-permute-start | bytes 884744 | tf_op jit(solution)/shard_map/ppermute | solution.py:312
  74.3 11.2 %copy-start.5 = (bf16[1152,128]{1,0:T(8,128)(2,1)}, bf16[1152,128]{1,0:T(8,128)(2,1)S(1)}, u32[]{:S(2)}) copy-start(bf16[1152,128]{1,0:T(8,128)(2,1)S(1)} %collective-permute-done.1.refs_2_) | copy-start | bytes 884740
  77.6 7.9 %copy-start.6 = (bf16[1152,128]{1,0:T(8,128)(2,1)}, bf16[1152,128]{1,0:T(8,128)(2,1)S(1)}, u32[]{:S(2)}) copy-start(bf16[1152,128]{1,0:T(8,128)(2,1)S(1)} %collective-permute-done.refs_1_) | copy-start | bytes 884740
  77.6 7.9 %copy-start.1 = (bf16[1920,128]{1,0:T(8,128)(2,1)}, bf16[1920,128]{1,0:T(8,128)(2,1)S(1)}, u32[]{:S(2)}) copy-start(bf16[1920,128]{1,0:T(8,128)(2,1)S(1)} %collective-permute-done.5.refs_7_) | copy-start | bytes 1474564
  85.4 0.8 copy-start.2
  86.2 0.8 copy-start.3
  104.4 17.2 %collective-permute-start.6 = (bf16[784,128]{1,0:T(8,128)(2,1)}, bf16[784,128]{1,0:T(8,128)(2,1)S(1)}, u32[]{:S(2)}, u32[]{:S(2)}) collective-permute-start(bf16[784,128]{1,0:T(8,128)(2,1)} %get-tuple-element.14), channel_id=1, source_target_pairs={{0,192},{16,208},{32,224},{48,240},{64,0},{80,16},{96,32},{112,48}... | collective-permute-start | bytes 602120 | tf_op jit(solution)/shard_map/ppermute | solution.py:322
  105.5 16.0 %collective-permute-start.7 = (bf16[784,128]{1,0:T(8,128)(2,1)}, bf16[784,128]{1,0:T(8,128)(2,1)S(1)}, u32[]{:S(2)}, u32[]{:S(2)}) collective-permute-start(bf16[784,128]{1,0:T(8,128)(2,1)} %get-tuple-element.15), channel_id=1, source_target_pairs={{0,64},{16,80},{32,96},{48,112},{64,128},{80,144},{96,160},{112,17... | collective-permute-start | bytes 602120 | tf_op jit(solution)/shard_map/ppermute | solution.py:322
  106.4 15.2 %collective-permute-start.8 = (bf16[784,128]{1,0:T(8,128)(2,1)}, bf16[784,128]{1,0:T(8,128)(2,1)S(1)}, u32[]{:S(2)}, u32[]{:S(2)}) collective-permute-start(bf16[784,128]{1,0:T(8,128)(2,1)} %get-tuple-element.16), channel_id=1, source_target_pairs={{0,128},{16,144},{32,160},{48,176},{64,192},{80,208},{96,224},{112... | collective-permute-start | bytes 602120 | tf_op jit(solution)/shard_map/ppermute | solution.py:322
  121.6 0.7 copy-start.8
  121.6 0.8 copy-start.9
  203.8 16.1 %all-to-all-start.1 = ((bf16[16,8,2048]{2,1,0:T(8,128)(2,1)}), bf16[16,8,2048]{2,1,0:T(8,128)(2,1)S(1)}, u32[]{:S(2)}, u32[]{:S(2)}) async-start(bf16[16,8,2048]{2,1,0:T(8,128)(2,1)} %fusion), calls=%async_computation.2 | async-start | bytes 1048576 | tf_op jit(solution)/shard_map/all_to_all | solution.py:365
  219.8 0.8 copy-start
  (1 other events, 0.7 us)
Sparse Core Ops, SparseCore 0:
  10.4 41.4 all-gather.5
  53.7 54.5 all-gather.3
  126.2 75.2 reduce-scatter.1

commit v2 on v1

--- a/solution.py
+++ b/solution.py
@@ -18,6 +18,7 @@
 THETA = 10000.0
 LANES = 128
 LOG2E = 1.4426950408889634
+
 
 BF16 = jnp.bfloat16
 F32 = jnp.float32
@@ -97,19 +98,22 @@
 
 
 def project_body(
-    lat_ref, wq_ref, wk_ref, wv_ref, qg_ref, kg_ref, cos_ref, sin_ref, q_ref, kv_ref, lat_q, lat_kv
+    mine_ref, other_ref, wq_ref, wk_ref, wv_ref, qg_ref, kg_ref, cos_ref, sin_ref,
+    q_ref, kv_ref, lat_q, lat_kv,
 ):
-    groups, height, _ = lat_ref.shape
+    groups, height, _ = mine_ref.shape
     q_parts = lat_q.shape[1] // LANES
     kv_parts = lat_kv.shape[1] // LANES
     own = height // (q_parts + kv_parts + 1)
-    half = groups * own // 2
-    for j in range(q_parts + kv_parts):
-        piece = lat_ref[:, j * own : (j + 1) * own, :].reshape(2 * half, LANES)
-        dst, col = (lat_q, j) if j < q_parts else (lat_kv, j - q_parts)
-        dst[:, col * LANES : (col + 1) * LANES] = piece
-    rope = lat_ref[:, (q_parts + kv_parts) * own :, :].reshape(2 * half, LANES)[:, :ROPE_DIM]
-    rope = rope.astype(F32)
+    half = groups * own
+    ropes = []
+    for n, src in enumerate((mine_ref, other_ref)):
+        for j in range(q_parts + kv_parts):
+            piece = src[:, j * own : (j + 1) * own, :].reshape(half, LANES)
+            dst, col = (lat_q, j) if j < q_parts else (lat_kv, j - q_parts)
+            dst[n * half : (n + 1) * half, col * LANES : (col + 1) * LANES] = piece
+        ropes.append(src[:, (q_parts + kv_parts) * own :, :].reshape(half, LANES)[:, :ROPE_DIM])
+    rope = jnp.concatenate(ropes, axis=0).astype(F32)
     cosine, sine = cos_ref[...], sin_ref[...]
     queries = jnp.dot(lat_q[...], wq_ref[...], preferred_element_type=F32)
     scale = HEAD_DIM**-0.5 * LOG2E
@@ -132,30 +136,28 @@
     kv_ref[4 * half :, :] = jnp.concatenate([k_rope[:half], k_rope[half:]], axis=1)
 
 
-def attend_body(*refs):
-    q_refs, kv_refs, out_refs = refs[:SIDE], refs[SIDE : 2 * SIDE], refs[2 * SIDE : 3 * SIDE]
-    qs, ks, vs, acc_ref = refs[3 * SIDE :]
+def attend(q_refs, kv_refs, start, finish, qs, ks, vs):
     rows = qs.shape[0] // SIDE
     half = rows // 2
     zero = jnp.zeros((half, ROPE_DIM), BF16)
     ones = jnp.ones((rows, LANES), BF16)
-    for b in range(SIDE):
+    staged = [(r, qs, b, rows) for b, r in enumerate(q_refs)]
+    staged += [(r, ks, b, 2 * rows) for b, r in enumerate(kv_refs)]
+    for src, dst, b, off in staged:
         at = b * rows
-        for src, dst, off in ((q_refs[b], qs, rows), (kv_refs[b], ks, 2 * rows)):
-            dst[at : at + rows, :NOPE_DIM] = src[:rows, :]
-            packed = src[off : off + half, :]
-            dst[at : at + half, NOPE_DIM:] = jnp.concatenate([packed[:, :ROPE_DIM], zero], axis=1)
-            dst[at + half : at + rows, NOPE_DIM:] = jnp.concatenate(
-                [packed[:, ROPE_DIM:], zero], axis=1
-            )
-        vs[at : at + rows, :VALUE_DIM] = kv_refs[b][rows : 2 * rows, :]
-        vs[at : at + rows, VALUE_DIM:] = ones
+        dst[at : at + rows, :NOPE_DIM] = src[:rows, :]
+        packed = src[off : off + half, :]
+        dst[at : at + half, NOPE_DIM:] = jnp.concatenate([packed[:, :ROPE_DIM], zero], axis=1)
+        dst[at + half : at + rows, NOPE_DIM:] = jnp.concatenate([packed[:, ROPE_DIM:], zero], axis=1)
+    for b, src in enumerate(kv_refs):
+        vs[b * rows : (b + 1) * rows, :VALUE_DIM] = src[rows : 2 * rows, :]
+        vs[b * rows : (b + 1) * rows, VALUE_DIM:] = ones
 
     def block(i, carry):
         here = pl.ds(pl.multiple_of(i * rows, rows), rows)
         q = qs[here, :]
-        acc = None
-        for b in range(SIDE):
+        acc = start(here)
+        for b in range(len(kv_refs)):
             there = slice(b * rows, (b + 1) * rows)
             scores = lax.dot_general(
                 q, ks[there, :], (((1,), (1,)), ((), ())), preferred_element_type=F32
@@ -163,10 +165,30 @@
             probs = jnp.exp2(scores).astype(BF16)
             term = jnp.dot(probs, vs[there, :], preferred_element_type=F32)
             acc = term if acc is None else acc + term
+        finish(here, acc)
+        return carry
+
+    lax.fori_loop(0, SIDE, block, 0)
+
+
+def near_body(*refs):
+    q_refs, kv_refs, (acc_ref, qs, ks, vs) = refs[:SIDE], refs[SIDE:-4], refs[-4:]
+
+    def finish(here, acc):
         acc_ref[here, :] = acc
-        return carry
-
-    lax.fori_loop(0, SIDE, block, 0)
+
+    attend(q_refs, kv_refs, lambda here: None, finish, qs, ks, vs)
+
+
+def far_body(*refs):
+    q_refs, (kv_ref, in_ref), rest = refs[:SIDE], refs[SIDE : SIDE + 2], refs[SIDE + 2 :]
+    out_refs, (qs, ks, vs, acc_ref) = rest[:SIDE], rest[SIDE:]
+    rows = qs.shape[0] // SIDE
+
+    def finish(here, acc):
+        acc_ref[here, :] = acc
+
+    attend(q_refs, (kv_ref,), lambda here: in_ref[here, :], finish, qs, ks, vs)
     for b in range(SIDE):
         at = b * rows
         out_refs[b][:rows, :] = acc_ref[at : at + rows, :VALUE_DIM].astype(BF16)
@@ -178,31 +200,41 @@
             out_refs[b][rows + 8 + j : rows + 8 + j + 1, :] = low
 
 
-def mix_body(*refs):
-    parts = refs[:SIDE]
-    w_ref, _, out_ref, head_ref, term_ref, sems = refs[SIDE:]
-    rows = head_ref.shape[0]
-    owners, span, _ = out_ref.shape
-    own = rows // owners
-    count = rows // LANES
-    total = sum(p[rows : rows + 8, :].astype(F32) + p[rows + 8 : rows + 16, :].astype(F32) for p in parts)
+def stack_body(*refs):
+    for n, ref in enumerate(refs[:-1]):
+        refs[-1][n, :, :] = ref[...]
+
+
+def join_body(*refs):
+    parts, outs = refs[:SIDE], refs[SIDE:]
+    half = outs[0].shape[0]
+    rows = 2 * half
+    total = sum(
+        p[rows : rows + 8, :].astype(F32) + p[rows + 8 : rows + 16, :].astype(F32) for p in parts
+    )
     inverse = 1.0 / total
-    for j in range(count):
+    for j in range(rows // LANES):
         there = slice(j * LANES, (j + 1) * LANES)
         scale = jnp.broadcast_to(inverse[j : j + 1, :], (LANES, LANES)).T
         head = sum(p[there, :].astype(F32) for p in parts)
-        head_ref[there, :] = (head * scale).astype(BF16)
+        at = j * LANES % half
+        outs[j * LANES // half][at : at + LANES, :] = (head * scale).astype(BF16)
+
+
+def mix_body(chip_ref, own_ref, twin_ref, w_own_ref, w_twin_ref, _, out_ref, term_ref, sems):
+    owners, span, _ = out_ref.shape
+    each = own_ref.shape[0] // owners
+    step = owners // 2
     copies = []
-    step = owners // 4
-    for c in range(4):
-        there = slice(c * step * own, (c + 1) * step * own)
-        term_ref[there, :] = jnp.dot(
-            head_ref[there, :], w_ref[...], preferred_element_type=F32
-        ).astype(BF16)
+    for c in range(2):
+        there = slice(c * step * each, (c + 1) * step * each)
+        term = jnp.dot(own_ref[there, :], w_own_ref[...], preferred_element_type=F32)
+        term += jnp.dot(twin_ref[there, :], w_twin_ref[...], preferred_element_type=F32)
+        term_ref[there, :] = term.astype(BF16)
         for i in range(c * step, (c + 1) * step):
             copy = pltpu.make_async_copy(
-                term_ref.at[pl.ds(i * own, own), :],
-                out_ref.at[i, pl.ds(span - own, own), :],
+                term_ref.at[pl.ds(i * each, each), :],
+                out_ref.at[(chip_ref[0] + owners - i) % owners, pl.ds(span - each, each), :],
                 sems.at[i],
             )
             copy.start()
@@ -211,14 +243,19 @@
         copy.wait()
 
 
-def expert_body(x_ref, gate_ref, up_ref, down_ref, out_ref):
-    groups, _, rows, width = x_ref.shape
+def expert_body(core_ref, x_ref, *refs):
+    del core_ref
+    sets, out_ref = (refs[:3], refs[3:6]), refs[6]
+    groups, rows, width = x_ref.shape
     x = x_ref[...].reshape(groups * rows, width)
-    gate = jnp.dot(x, gate_ref[0], preferred_element_type=F32)
-    up = jnp.dot(x, up_ref[0], preferred_element_type=F32)
-    hidden = (gate / (1.0 + jnp.exp(-gate)) * up).astype(BF16)
-    out = jnp.dot(hidden, down_ref[0], preferred_element_type=F32).astype(BF16)
-    out_ref[...] = out.reshape(groups, rows, width)
+    out = None
+    for gate_ref, up_ref, down_ref in sets:
+        gate = jnp.dot(x, gate_ref[...].reshape(width, -1), preferred_element_type=F32)
+        up = jnp.dot(x, up_ref[...].reshape(width, -1), preferred_element_type=F32)
+        hidden = (gate / (1.0 + jnp.exp(-gate)) * up).astype(BF16)
+        term = jnp.dot(hidden, down_ref[...].reshape(-1, width), preferred_element_type=F32)
+        out = term if out is None else out + term
+    out_ref[...] = out.astype(BF16).reshape(groups, rows, width)
 
 
 def shift(axis_x, axis_y):
@@ -251,11 +288,19 @@
 ):
     tp_count = lax.axis_size("tp")
     ep_count = lax.axis_size("ep")
+    chips = tp_count // 2
     own = q_latent.shape[0]
     rows = own * tp_count
+    half = rows // 2
     width = tokens_b.shape[1]
-    experts_dev = w_gate.shape[0]
     slots = EXPERTS * CAP
+    tp_at = lax.axis_index("tp")
+    core, chip = tp_at % 2, tp_at // 2
+    same_core = [[z * 2 + c for z in range(chips)] for c in range(2)]
+    plane = [
+        [e * tp_count + z * 2 + c for e in range(ep_count) for c in range(2)] for z in range(chips)
+    ]
+    swap = [(i, i ^ 1) for i in range(tp_count)]
 
     height = own * ((q_latent.shape[1] + kv_latent.shape[1]) // LANES + 1)
     latent = pl.pallas_call(
@@ -265,7 +310,6 @@
         name="latents",
     )(q_latent, kv_latent, rope_key, q_latent_gain[None], kv_latent_gain[None])
 
-    latent, tokens_b = lax.optimization_barrier((latent, tokens_b))
     id_rows = expert_ids.T
     outgoing = pl.pallas_call(
         dispatch_body,
@@ -274,20 +318,32 @@
         name="dispatch",
     )(tokens_b, norm_gain[None], id_rows)
 
-    latents = lax.all_gather(latent, "tp", axis=0)
-
-    arrived = lax.all_to_all(outgoing.reshape(ep_count, slots // ep_count, width), "ep", 0, 0)
-    arrived = arrived.reshape(slots, width)
-    at = jnp.arange(slots, dtype=jnp.int32)
-    moved = (at % (slots // experts_dev)) // CAP * (experts_dev * CAP) + at // (
-        slots // experts_dev
-    ) * CAP + at % CAP
-    turn = (moved[:, None] == at[None, :]).astype(BF16)
-    grouped = jnp.dot(turn, arrived, preferred_element_type=F32).astype(BF16)
-    everyone = lax.all_gather(grouped, "tp", axis=0, tiled=True)
-    everyone = everyone.reshape(tp_count, experts_dev, slots // experts_dev, width)
-
-    positions = lax.axis_index("ep") * rows + jnp.arange(rows, dtype=jnp.int32)
+    arrived = lax.all_to_all(
+        outgoing.reshape(EXPERTS, CAP, width), ("ep", "tp"), 0, 0, axis_index_groups=plane
+    )
+    everyone = lax.all_gather(
+        arrived.reshape(slots, width), "tp", axis=0, axis_index_groups=same_core
+    )
+
+    mine = [latent] + [
+        lax.ppermute(latent, "tp", [(i, (i + 2 * k) % tp_count) for i in range(tp_count)])
+        for k in range(1, chips)
+    ]
+    mine = pl.pallas_call(
+        stack_body,
+        out_shape=jax.ShapeDtypeStruct((chips, height, LANES), BF16),
+        compiler_params=params(),
+        name="stack",
+    )(*mine)
+    other = lax.ppermute(mine, "tp", swap)
+
+    block = jnp.arange(rows, dtype=jnp.int32) // own
+    side = jnp.where(block < chips, core, 1 - core)
+    positions = (
+        lax.axis_index("ep") * rows
+        + (((chip - block) % chips) * 2 + side) * own
+        + jnp.arange(rows, dtype=jnp.int32) % own
+    )
     inverse = THETA ** (-jnp.arange(0, ROPE_DIM, 2, dtype=F32) / ROPE_DIM)
     angles = positions.astype(F32)[:, None] * inverse[None, :]
     cosine, sine = jnp.cos(angles), jnp.sin(angles)
@@ -306,63 +362,103 @@
         ],
         compiler_params=params(),
         name="project",
-    )(latents, w_query, w_key, w_value, query_gain[None], key_gain[None], cosine, sine)
-
-    kv_all = [kv_own] + [lax.ppermute(kv_own, "ep", shift(d, 0)) for d in (1, 3, 2)]
+    )(mine, other, w_query, w_key, w_value, query_gain[None], key_gain[None], cosine, sine)
+
+    kv_near = [kv_own] + [lax.ppermute(kv_own, "ep", shift(d, 0)) for d in (1, 3)]
     q_all = [q_own] + [lax.ppermute(q_own, "ep", shift(0, d)) for d in (1, 3, 2)]
+    kv_far = lax.ppermute(kv_own, "ep", shift(2, 0))
+    wide = 2 * LANES
+    acc = pl.pallas_call(
+        near_body,
+        out_shape=jax.ShapeDtypeStruct((SIDE * rows, wide), F32),
+        scratch_shapes=[
+            pltpu.VMEM((SIDE * rows, wide), BF16),
+            pltpu.VMEM((3 * rows, wide), BF16),
+            pltpu.VMEM((3 * rows, wide), BF16),
+        ],
+        compiler_params=params(),
+        name="near",
+    )(*q_all, *kv_near)
     partial = pl.pallas_call(
-        attend_body,
+        far_body,
         out_shape=[jax.ShapeDtypeStruct((rows + 16, LANES), BF16)] * SIDE,
-        scratch_shapes=[pltpu.VMEM((SIDE * rows, 2 * LANES), BF16)] * 3
-        + [pltpu.VMEM((SIDE * rows, 2 * LANES), F32)],
-        compiler_params=params(),
-        name="attend",
-    )(*q_all, *kv_all)
+        scratch_shapes=[
+            pltpu.VMEM((SIDE * rows, wide), BF16),
+            pltpu.VMEM((rows, wide), BF16),
+            pltpu.VMEM((rows, wide), BF16),
+            pltpu.VMEM((SIDE * rows, wide), F32),
+        ],
+        compiler_params=params(),
+        name="far",
+    )(*q_all, kv_far, acc)
     parts = [partial[0]] + [
         lax.ppermute(p, "ep", shift(0, -d)) for p, d in zip(partial[1:], (1, 3, 2))
     ]
 
+    twin = [
+        lax.ppermute(lax.dynamic_index_in_dim(w, 1 - core, 0, False), "tp", swap)
+        for w in (w_gate, w_up, w_down)
+    ]
+    mix_twin = lax.ppermute(w_mix, "tp", swap)
+
     span = slots + own
-    share = slots // experts_dev
-    step = tp_count // 2
+    step = chips // 2
     hidden = w_gate.shape[2]
     terms = pl.pallas_call(
         expert_body,
-        out_shape=jax.ShapeDtypeStruct((tp_count, span, width), BF16),
-        grid=(experts_dev, tp_count // step),
-        in_specs=[
-            pl.BlockSpec((step, 1, share, width), lambda x, j: (j, x, 0, 0)),
-            pl.BlockSpec((1, width, hidden), lambda x, j: (x, 0, 0)),
-            pl.BlockSpec((1, width, hidden), lambda x, j: (x, 0, 0)),
-            pl.BlockSpec((1, hidden, width), lambda x, j: (x, 0, 0)),
-        ],
-        out_specs=pl.BlockSpec((step, share, width), lambda x, j: (j, x, 0)),
+        out_shape=jax.ShapeDtypeStruct((chips, span, width), BF16),
+        grid_spec=pltpu.PrefetchScalarGridSpec(
+            num_scalar_prefetch=1,
+            grid=(chips // step,),
+            in_specs=[
+                pl.BlockSpec((step, slots, width), lambda j, c: (j, 0, 0)),
+                pl.BlockSpec((1, width, hidden), lambda j, c: (c[0], 0, 0)),
+                pl.BlockSpec((1, width, hidden), lambda j, c: (c[0], 0, 0)),
+                pl.BlockSpec((1, hidden, width), lambda j, c: (c[0], 0, 0)),
+                pl.BlockSpec((width, hidden), lambda j, c: (0, 0)),
+                pl.BlockSpec((width, hidden), lambda j, c: (0, 0)),
+                pl.BlockSpec((hidden, width), lambda j, c: (0, 0)),
+            ],
+            out_specs=pl.BlockSpec((step, slots, width), lambda j, c: (j, 0, 0)),
+        ),
         compiler_params=params(),
         name="experts",
-    )(everyone, w_gate, w_up, w_down)
-
+    )(core.reshape(1), everyone, w_gate, w_up, w_down, *twin)
+
+    own_head, twin_head = pl.pallas_call(
+        join_body,
+        out_shape=[jax.ShapeDtypeStruct((half, VALUE_DIM), BF16)] * 2,
+        compiler_params=params(),
+        name="join",
+    )(*parts)
+    twin_head = lax.ppermute(twin_head, "tp", swap)
     terms = pl.pallas_call(
         mix_body,
-        out_shape=jax.ShapeDtypeStruct((tp_count, span, width), BF16),
-        in_specs=[pl.BlockSpec(memory_space=pltpu.VMEM)] * (SIDE + 1)
+        out_shape=jax.ShapeDtypeStruct((chips, span, width), BF16),
+        in_specs=[pl.BlockSpec(memory_space=pltpu.SMEM)]
+        + [pl.BlockSpec(memory_space=pltpu.VMEM)] * 4
         + [pl.BlockSpec(memory_space=pl.ANY)],
         out_specs=pl.BlockSpec(memory_space=pl.ANY),
         scratch_shapes=[
-            pltpu.VMEM((rows, VALUE_DIM), BF16),
-            pltpu.VMEM((rows, width), BF16),
-            pltpu.SemaphoreType.DMA((tp_count,)),
+            pltpu.VMEM((half, width), BF16),
+            pltpu.SemaphoreType.DMA((chips,)),
         ],
-        input_output_aliases={SIDE + 1: 0},
+        input_output_aliases={5: 0},
         compiler_params=params(),
         name="mix",
-    )(*parts, w_mix, terms)
+    )(chip.reshape(1), own_head, twin_head, w_mix, mix_twin, terms)
 
     summed = lax.psum_scatter(
-        terms.reshape(tp_count * span, width), "tp", scatter_dimension=0, tiled=True
+        terms.reshape(chips * span, width),
+        "tp",
+        scatter_dimension=0,
+        tiled=True,
+        axis_index_groups=same_core,
     )
     mix_out = summed[slots:]
-    done = jnp.dot(turn.T, summed[:slots], preferred_element_type=F32).astype(BF16)
-    returned = lax.all_to_all(done.reshape(ep_count, slots // ep_count, width), "ep", 0, 0)
+    returned = lax.all_to_all(
+        summed[:slots].reshape(EXPERTS, CAP, width), ("ep", "tp"), 0, 0, axis_index_groups=plane
+    )
     expert_out = pl.pallas_call(
         collect_body,
         out_shape=jax.ShapeDtypeStruct((own, width), BF16),

time: 230 us -> 272 us (1.18)
  blocking collectives: 0 us -> 17.8 us
  local copies, waits for them, and re-layouts: 6.75 us -> 16.3 us
  Pallas kernels: 45.6 us -> 53.1 us
  starting transfers between devices: 28.1 us -> 34.7 us
  matrix products: 3.39 us -> 0 us
    ppermute x3, waiting for transfers between devices: 0.01 us -> 20.4 us  [on_device(): lax.ppermute(p, 'ep', shift(0, -d))]
    ppermute x0 -> x14, starting transfers between devices: none -> 20.1 us  [the longest x7 18.4 us: on_device(): lax.ppermute(latent, 'tp', [(i, (i + 2 * k) % tp_count) for i in range(tp...]
    all_gather x2 -> x1, waiting for transfers between devices: 18.5 us -> 0.02 us  [on_device(): lax.all_gather(arrived.reshape(slots, width), 'tp', axis=0, axis_index_gr...]
    all_to_all x0 -> x1, blocking collectives: none -> 17.8 us  [on_device(): lax.all_to_all(outgoing.reshape(EXPERTS, CAP, width), ('ep', 'tp'), 0, 0,...]
    ppermute x0 -> x14, waiting for transfers between devices: none -> 12.7 us  [the longest x7 12.6 us: on_device(): lax.ppermute(latent, 'tp', [(i, (i + 2 * k) % tp_count) for i in range(tp...]
    all_to_all x2 -> x1, waiting for transfers between devices: 17.3 us -> 8.76 us  [on_device(): lax.all_to_all(summed[:slots].reshape(EXPERTS, CAP, width), ('ep', 'tp'),...]
    pallas_call x3 -> x6, Pallas kernels: 34.3 us -> 41.7 us  [the longest x1 15 us: on_device(): pl.pallas_call(near_body, out_shape=jax.ShapeDtypeStruct((SIDE * rows, wi...]
    all_to_all x2 -> x1, starting transfers between devices: 14.8 us -> 7.41 us  [on_device(): lax.all_to_all(summed[:slots].reshape(EXPERTS, CAP, width), ('ep', 'tp'),...]
  transfers between devices with their start and end apart: 14 -> 25, of which waited for: 10 -> 13; matrix products, arithmetic and copies ran while one was open for 3% -> 3% of each run, Pallas kernels for 17% -> 17%
where the time goes in v2:
time: 272 us; the launch traced here: 269 us
  waiting for transfers between devices  130 us (48%)
  Pallas kernels  53.1 us (20%)
  starting transfers between devices  34.7 us (13%)
  blocking collectives  17.8 us (7%)
  local copies, waits for them, and re-layouts  16.3 us (6%)
  between operations  14.3 us (5%)
    reduce_scatter x1, waiting for transfers between devices, on_device(): lax.psum_scatter(terms.reshape(chips * span, width), 'tp', scatter_dimens...  78.2 us
    ppermute x3, waiting for transfers between devices, on_device(): lax.ppermute(p, 'ep', shift(0, -d))  20.4 us
    ppermute x7, starting transfers between devices, on_device(): lax.ppermute(latent, 'tp', [(i, (i + 2 * k) % tp_count) for i in range(tp...  18.4 us
    all_to_all x1, blocking collectives, on_device(): lax.all_to_all(outgoing.reshape(EXPERTS, CAP, width), ('ep', 'tp'), 0, 0,...  17.8 us
    pallas_call x1, Pallas kernels, on_device(): pl.pallas_call(near_body, out_shape=jax.ShapeDtypeStruct((SIDE * rows, wi...  15 us
    ppermute x7, waiting for transfers between devices, on_device(): lax.ppermute(latent, 'tp', [(i, (i + 2 * k) % tp_count) for i in range(tp...  12.6 us
    pallas_call x1, Pallas kernels, on_device(): pl.pallas_call(expert_body, out_shape=jax.ShapeDtypeStruct((chips, span,...  11.6 us
    ppermute x3, waiting for transfers between devices, on_device(): lax.ppermute(q_own, 'ep', shift(0, d))  9.01 us
  transfers between devices with their start and end apart: 25, of which 13 were waited for; matrix products, arithmetic and copies ran while one was open for 3% of the time, Pallas kernels for 17%

profile of v2, /device:TPU:2, one launch (start us, length us, event | category | flops | bytes accessed | tf_op | source)
XLA Modules:
  0.0 269.2 jit_solution(1855847652259208129)
XLA Ops:
  7.2 2.2 dispatch.1
  10.7 17.8 %all_to_all.10 = bf16[32,4,2048]{2,1,0:T(4,128)(2,1)S(1)} all-to-all(bf16[32,4,2048]{2,1,0:T(4,128)(2,1)S(1)} %reshape.69), channel_id=1, replica_groups={{0,1,16,17,32,33,48,49,64,65,80,81,96,97,112,113,128,129,144,145,160,16..., dimensions={0} | all-to-all | bytes 1048576 | tf_op jit(solution)/shard_map/all_to_all | solution.py:321
  33.5 3.3 %collective-permute-start.1 = (bf16[288,128]{1,0:T(8,128)(2,1)}, bf16[288,128]{1,0:T(8,128)(2,1)S(1)}, u32[]{:S(2)}, u32[]{:S(2)}) collective-permute-start(bf16[288,128]{1,0:T(8,128)(2,1)} %latents.1.refs_0_), channel_id=1, source_target_pairs={{0,4},{1,5},{2,6},{3,7},{4,8},{5,9},{6,10},{7,11},{8,12},{9,13},{1... | collective-permute-start | bytes 221192 | tf_op jit(solution)/shard_map/ppermute | solution.py:329
  36.8 4.0 %collective-permute-start.2 = (bf16[288,128]{1,0:T(8,128)(2,1)}, bf16[288,128]{1,0:T(8,128)(2,1)S(1)}, u32[]{:S(2)}, u32[]{:S(2)}) collective-permute-start(bf16[288,128]{1,0:T(8,128)(2,1)} %latents.1.refs_0_), channel_id=1, source_target_pairs={{0,6},{1,7},{2,8},{3,9},{4,10},{5,11},{6,12},{7,13},{8,14},{9,15},... | collective-permute-start | bytes 221192 | tf_op jit(solution)/shard_map/ppermute | solution.py:329
  41.4 5.0 %collective-permute-start.4 = (bf16[288,128]{1,0:T(8,128)(2,1)}, bf16[288,128]{1,0:T(8,128)(2,1)S(1)}, u32[]{:S(2)}, u32[]{:S(2)}) collective-permute-start(bf16[288,128]{1,0:T(8,128)(2,1)} %latents.1.refs_0_), channel_id=1, source_target_pairs={{0,10},{1,11},{2,12},{3,13},{4,14},{5,15},{6,0},{7,1},{8,2},{9,3},... | collective-permute-start | bytes 221192 | tf_op jit(solution)/shard_map/ppermute | solution.py:329
  46.3 2.7 collective-permute-start.5
  50.8 2.7 %collective-permute-done.2.refs_3_ = bf16[288,128]{1,0:T(8,128)(2,1)S(1)} collective-permute-done((bf16[288,128]{1,0:T(8,128)(2,1)}, bf16[288,128]{1,0:T(8,128)(2,1)S(1)}, u32[]{:S(2)}, u32[]{:S(2)}) %collective-permute-start.2) | collective-permute-done | bytes 73760 | tf_op jit(solution)/shard_map/ppermute | solution.py:329
  53.8 6.5 %collective-permute-done.4.refs_5_ = bf16[288,128]{1,0:T(8,128)(2,1)S(1)} collective-permute-done((bf16[288,128]{1,0:T(8,128)(2,1)}, bf16[288,128]{1,0:T(8,128)(2,1)S(1)}, u32[]{:S(2)}, u32[]{:S(2)}) %collective-permute-start.4) | collective-permute-done | bytes 73760 | tf_op jit(solution)/shard_map/ppermute | solution.py:329
  60.7 2.8 %collective-permute-done.6.refs_7_ = bf16[288,128]{1,0:T(8,128)(2,1)S(1)} collective-permute-done((bf16[288,128]{1,0:T(8,128)(2,1)}, bf16[288,128]{1,0:T(8,128)(2,1)S(1)}, u32[]{:S(2)}, u32[]{:S(2)}) %collective-permute-start.6) | collective-permute-done | bytes 73760 | tf_op jit(solution)/shard_map/ppermute | solution.py:329
  69.6 5.3 %project.1 = (bf16[1152,128]{1,0:T(8,128)(2,1)}, bf16[1920,128]{1,0:T(8,128)(2,1)}) custom-call(bf16[8,288,128]{2,1,0:T(8,128)(2,1)} %stack.1.mine_ref, bf16[8,288,128]{2,1,0:T(8,128)(2,1)} %copy-done.10, bf16[384,192]{1,0:T(8,128)(2,1)} %copy.24.wq_ref, bf16[256,128]{1,0:T(8,128)(2,1)} %wk_ref.1, bf16[256,128]{1,0:T(8,128)(2,1)} %wv_ref.1, ...), custom_call_target="tpu_custom_call" | custom-call | tf_op jit(solution)/shard_map/project/pallas_call | solution.py:353
  77.3 2.7 collective-permute-start.9
  82.1 4.5 %collective-permute-done.10.refs_3_ = bf16[1152,128]{1,0:T(8,128)(2,1)S(1)} collective-permute-done((bf16[1152,128]{1,0:T(8,128)(2,1)}, bf16[1152,128]{1,0:T(8,128)(2,1)S(1)}, u32[]{:S(2)}, u32[]{:S(2)}) %collective-permute-start.10) | collective-permute-done | bytes 294944 | tf_op jit(solution)/shard_map/ppermute | solution.py:368
  87.8 4.6 %collective-permute-done.8.refs_1_ = bf16[1152,128]{1,0:T(8,128)(2,1)S(1)} collective-permute-done((bf16[1152,128]{1,0:T(8,128)(2,1)S(1)}, bf16[1152,128]{1,0:T(8,128)(2,1)S(1)}, u32[]{:S(2)}, u32[]{:S(2)}) %collective-permute-start.8) | collective-permute-done | bytes 294944 | tf_op jit(solution)/shard_map/ppermute | solution.py:368
  95.9 15.0 %near.1.refs_5_ = f32[3072,256]{1,0:T(8,128)} custom-call(bf16[1152,128]{1,0:T(8,128)(2,1)} %get-tuple-element.10.refs_0_, bf16[1152,128]{1,0:T(8,128)(2,1)} %copy-done.5, bf16[1152,128]{1,0:T(8,128)(2,1)} %copy-done.6, bf16[1152,128]{1,0:T(8,128)(2,1)} %copy-done.4, bf16[1920,128]{1,0:T(8,128)(2,1)} %get-tuple-element.11.refs_4_, ...), custom_call_target="tpu_custom_call" | custom-call | tf_op jit(solution)/shard_map/near/pallas_call | solution.py:371
  111.7 7.8 %far.1 = (bf16[784,128]{1,0:T(8,128)(2,1)}, bf16[784,128]{1,0:T(8,128)(2,1)}, bf16[784,128]{1,0:T(8,128)(2,1)}, bf16[784,128]{1,0:T(8,128)(2,1)}) custom-call(bf16[1152,128]{1,0:T(8,128)(2,1)} %get-tuple-element.10.refs_0_, bf16[1152,128]{1,0:T(8,128)(2,1)} %copy-done.5, bf16[1152,128]{1,0:T(8,128)(2,1)} %copy-done.6, bf16[1152,128]{1,0:T(8,128)(2,1)} %copy-done.4, ...), custom_call_target="tpu_custom_call" | custom-call | tf_op jit(solution)/shard_map/far/pallas_call | solution.py:382
  120.1 6.2 %collective-permute-done.14.refs_1_ = bf16[784,128]{1,0:T(8,128)(2,1)S(1)} collective-permute-done((bf16[784,128]{1,0:T(8,128)(2,1)}, bf16[784,128]{1,0:T(8,128)(2,1)S(1)}, u32[]{:S(2)}, u32[]{:S(2)}) %collective-permute-start.14) | collective-permute-done | bytes 200736 | tf_op jit(solution)/shard_map/ppermute | solution.py:395
  126.3 7.2 %collective-permute-done.15.refs_2_ = bf16[784,128]{1,0:T(8,128)(2,1)S(1)} collective-permute-done((bf16[784,128]{1,0:T(8,128)(2,1)}, bf16[784,128]{1,0:T(8,128)(2,1)S(1)}, u32[]{:S(2)}, u32[]{:S(2)}) %collective-permute-start.15) | collective-permute-done | bytes 200736 | tf_op jit(solution)/shard_map/ppermute | solution.py:395
  133.8 7.0 %collective-permute-done.16.refs_3_ = bf16[784,128]{1,0:T(8,128)(2,1)S(1)} collective-permute-done((bf16[784,128]{1,0:T(8,128)(2,1)}, bf16[784,128]{1,0:T(8,128)(2,1)S(1)}, u32[]{:S(2)}, u32[]{:S(2)}) %collective-permute-start.16) | collective-permute-done | bytes 200736 | tf_op jit(solution)/shard_map/ppermute | solution.py:395
  145.4 11.6 %experts.1._ = bf16[8,176,2048]{2,1,0:T(8,128)(2,1)} custom-call(s32[1]{0:T(128)} %bitcast.4.core_ref, bf16[8,128,2048]{2,1,0:T(8,128)(2,1)} %all-gather.2.cloned.1.call-done.x_ref, bf16[2,2048,256]{2,1,0:T(8,128)(2,1)} %refs_0_.1, bf16[2,2048,256]{2,1,0:T(8,128)(2,1)} %refs_1_.1, bf16[2,256,2048]{2,1,0:T(8,128)(2,1)} %refs_2_.1, ...), custom_call_target="tpu_custom_call" | custom-call | tf_op jit(solution)/shard_map/experts/pallas_call | solution.py:407
  157.7 3.2 %mix.1 = bf16[8,176,2048]{2,1,0:T(8,128)(2,1)} custom-call(s32[1]{0:T(128)} %bitcast.chip_ref, bf16[384,128]{1,0:T(8,128)(2,1)} %get-tuple-element.16.own_ref, bf16[384,128]{1,0:T(8,128)(2,1)} %copy-done.18, bf16[128,2048]{1,0:T(8,128)(2,1)} %w_own_ref.1, bf16[128,2048]{1,0:T(8,128)(2,1)} %collective-permute-done.18.w_twin_ref, ...), custom_call_target="tpu_custom_call", output_to_operand_aliasing={{}: (5, {})} | custom-call | tf_op jit(solution)/shard_map/mix/pallas_call | solution.py:435
  161.0 78.2 %reduce-scatter.2.cloned.1.call-done = bf16[176,2048]{1,0:T(8,128)(2,1)} async-done(((bf16[1408,2048]{1,0:T(8,128)(2,1)}), bf16[176,2048]{1,0:T(8,128)(2,1)}) %reduce-scatter.2.cloned.1.call-update) | async-done | bytes 720912 | tf_op jit(solution)/shard_map/reduce_scatter | solution.py:451
  241.3 7.4 %all-to-all-start.1 = ((bf16[32,4,2048]{2,1,0:T(4,128)(2,1)}), bf16[32,4,2048]{2,1,0:T(4,128)(2,1)S(1)}, u32[]{:S(2)}, u32[]{:S(2)}) async-start(bf16[32,4,2048]{2,1,0:T(4,128)(2,1)} %reshape.71), calls=%async_computation.2 | async-start | bytes 1048576 | tf_op jit(solution)/shard_map/all_to_all | solution.py:459
  250.3 8.8 %all-to-all-done.1 = bf16[32,4,2048]{2,1,0:T(4,128)(2,1)S(1)} async-done(((bf16[32,4,2048]{2,1,0:T(4,128)(2,1)}), bf16[32,4,2048]{2,1,0:T(4,128)(2,1)S(1)}, u32[]{:S(2)}, u32[]{:S(2)}) %all-to-all-start.1) | async-done | bytes 524320 | tf_op jit(solution)/shard_map/all_to_all | solution.py:459
  260.0 2.4 collect.1
  (108 shorter events, 36.3 us)
Async XLA Ops:
  7.2 136.5 %all-gather.2.cloned.1.call-start = ((), (), s32[]{:S(2)}) async-start(), calls=%async_computation.3 | async-start | bytes 4718592 | tf_op jit(solution)/shard_map/all_gather | solution.py:324
  29.4 209.8 %reduce-scatter.2.cloned.1.call-start = ((), (), s32[]{:S(2)}) async-start(), calls=%async_computation.4 | async-start | bytes 6488064 | tf_op jit(solution)/shard_map/reduce_scatter | solution.py:451
  31.6 14.7 %collective-permute-start = (bf16[288,128]{1,0:T(8,128)(2,1)}, bf16[288,128]{1,0:T(8,128)(2,1)S(1)}, u32[]{:S(2)}, u32[]{:S(2)}) collective-permute-start(bf16[288,128]{1,0:T(8,128)(2,1)} %latents.1.refs_0_), channel_id=1, source_target_pairs={{0,2},{1,3},{2,4},{3,5},{4,6},{5,7},{6,8},{7,9},{8,10},{9,11},{10,... | collective-permute-start | bytes 221192 | tf_op jit(solution)/shard_map/ppermute | solution.py:329
  33.5 15.5 %collective-permute-start.1 = (bf16[288,128]{1,0:T(8,128)(2,1)}, bf16[288,128]{1,0:T(8,128)(2,1)S(1)}, u32[]{:S(2)}, u32[]{:S(2)}) collective-permute-start(bf16[288,128]{1,0:T(8,128)(2,1)} %latents.1.refs_0_), channel_id=1, source_target_pairs={{0,4},{1,5},{2,6},{3,7},{4,8},{5,9},{6,10},{7,11},{8,12},{9,13},{1... | collective-permute-start | bytes 221192 | tf_op jit(solution)/shard_map/ppermute | solution.py:329
  36.8 16.8 %collective-permute-start.2 = (bf16[288,128]{1,0:T(8,128)(2,1)}, bf16[288,128]{1,0:T(8,128)(2,1)S(1)}, u32[]{:S(2)}, u32[]{:S(2)}) collective-permute-start(bf16[288,128]{1,0:T(8,128)(2,1)} %latents.1.refs_0_), channel_id=1, source_target_pairs={{0,6},{1,7},{2,8},{3,9},{4,10},{5,11},{6,12},{7,13},{8,14},{9,15},... | collective-permute-start | bytes 221192 | tf_op jit(solution)/shard_map/ppermute | solution.py:329
  40.8 13.0 %collective-permute-start.3 = (bf16[288,128]{1,0:T(8,128)(2,1)}, bf16[288,128]{1,0:T(8,128)(2,1)S(1)}, u32[]{:S(2)}, u32[]{:S(2)}) collective-permute-start(bf16[288,128]{1,0:T(8,128)(2,1)} %latents.1.refs_0_), channel_id=1, source_target_pairs={{0,8},{1,9},{2,10},{3,11},{4,12},{5,13},{6,14},{7,15},{8,0},{9,1},... | collective-permute-start | bytes 221192 | tf_op jit(solution)/shard_map/ppermute | solution.py:329
  41.4 18.9 %collective-permute-start.4 = (bf16[288,128]{1,0:T(8,128)(2,1)}, bf16[288,128]{1,0:T(8,128)(2,1)S(1)}, u32[]{:S(2)}, u32[]{:S(2)}) collective-permute-start(bf16[288,128]{1,0:T(8,128)(2,1)} %latents.1.refs_0_), channel_id=1, source_target_pairs={{0,10},{1,11},{2,12},{3,13},{4,14},{5,15},{6,0},{7,1},{8,2},{9,3},... | collective-permute-start | bytes 221192 | tf_op jit(solution)/shard_map/ppermute | solution.py:329
  46.3 14.4 %collective-permute-start.5 = (bf16[288,128]{1,0:T(8,128)(2,1)}, bf16[288,128]{1,0:T(8,128)(2,1)S(1)}, u32[]{:S(2)}, u32[]{:S(2)}) collective-permute-start(bf16[288,128]{1,0:T(8,128)(2,1)} %latents.1.refs_0_), channel_id=1, source_target_pairs={{0,12},{1,13},{2,14},{3,15},{4,0},{5,1},{6,2},{7,3},{8,4},{9,5},{1... | collective-permute-start | bytes 221192 | tf_op jit(solution)/shard_map/ppermute | solution.py:329
  49.0 14.5 %collective-permute-start.6 = (bf16[288,128]{1,0:T(8,128)(2,1)}, bf16[288,128]{1,0:T(8,128)(2,1)S(1)}, u32[]{:S(2)}, u32[]{:S(2)}) collective-permute-start(bf16[288,128]{1,0:T(8,128)(2,1)} %latents.1.refs_0_), channel_id=1, source_target_pairs={{0,14},{1,15},{2,0},{3,1},{4,2},{5,3},{6,4},{7,5},{8,6},{9,7},{10,... | collective-permute-start | bytes 221192 | tf_op jit(solution)/shard_map/ppermute | solution.py:329
  74.9 11.7 %collective-permute-start.10 = (bf16[1152,128]{1,0:T(8,128)(2,1)}, bf16[1152,128]{1,0:T(8,128)(2,1)S(1)}, u32[]{:S(2)}, u32[]{:S(2)}) collective-permute-start(bf16[1152,128]{1,0:T(8,128)(2,1)} %get-tuple-element.10.refs_0_), channel_id=1, source_target_pairs={{0,128},{16,144},{32,160},{48,176},{64,192},{80,208},{96,224},{112... | collective-permute-start | bytes 884744 | tf_op jit(solution)/shard_map/ppermute | solution.py:368
  76.7 15.7 %collective-permute-start.8 = (bf16[1152,128]{1,0:T(8,128)(2,1)S(1)}, bf16[1152,128]{1,0:T(8,128)(2,1)S(1)}, u32[]{:S(2)}, u32[]{:S(2)}) collective-permute-start(bf16[1152,128]{1,0:T(8,128)(2,1)S(1)} %copy-done.3), channel_id=1, source_target_pairs={{0,64},{16,80},{32,96},{48,112},{64,128},{80,144},{96,160},{112,17... | collective-permute-start | bytes 884744 | tf_op jit(solution)/shard_map/ppermute | solution.py:368
  77.3 15.3 %collective-permute-start.9 = (bf16[1152,128]{1,0:T(8,128)(2,1)S(1)}, bf16[1152,128]{1,0:T(8,128)(2,1)S(1)}, u32[]{:S(2)}, u32[]{:S(2)}) collective-permute-start(bf16[1152,128]{1,0:T(8,128)(2,1)S(1)} %copy-done.3), channel_id=1, source_target_pairs={{0,192},{16,208},{32,224},{48,240},{64,0},{80,16},{96,32},{112,48}... | collective-permute-start | bytes 884744 | tf_op jit(solution)/shard_map/ppermute | solution.py:368
  80.0 14.3 %collective-permute-start.12 = (bf16[1920,128]{1,0:T(8,128)(2,1)}, bf16[1920,128]{1,0:T(8,128)(2,1)S(1)}, u32[]{:S(2)}, u32[]{:S(2)}) collective-permute-start(bf16[1920,128]{1,0:T(8,128)(2,1)} %get-tuple-element.11.refs_4_), channel_id=1, source_target_pairs={{0,16},{16,32},{32,48},{48,0},{64,80},{80,96},{96,112},{112,64},{1... | collective-permute-start | bytes 1474568 | tf_op jit(solution)/shard_map/ppermute | solution.py:367
  80.1 15.0 %collective-permute-start.13 = (bf16[1920,128]{1,0:T(8,128)(2,1)}, bf16[1920,128]{1,0:T(8,128)(2,1)S(1)}, u32[]{:S(2)}, u32[]{:S(2)}) collective-permute-start(bf16[1920,128]{1,0:T(8,128)(2,1)} %get-tuple-element.11.refs_4_), channel_id=1, source_target_pairs={{0,48},{16,0},{32,16},{48,32},{64,112},{80,64},{96,80},{112,96},{1... | collective-permute-start | bytes 1474568 | tf_op jit(solution)/shard_map/ppermute | solution.py:367
  86.6 24.3 %collective-permute-start.11 = (bf16[1920,128]{1,0:T(8,128)(2,1)}, bf16[1920,128]{1,0:T(8,128)(2,1)S(1)}, u32[]{:S(2)}, u32[]{:S(2)}) collective-permute-start(bf16[1920,128]{1,0:T(8,128)(2,1)} %get-tuple-element.11.refs_4_), channel_id=1, source_target_pairs={{0,32},{16,48},{32,0},{48,16},{64,96},{80,112},{96,64},{112,80},{1... | collective-permute-start | bytes 1474568 | tf_op jit(solution)/shard_map/ppermute | solution.py:369
  92.4 51.2 %collective-permute-start.19 = (bf16[2048,256]{1,0:T(8,128)(2,1)}, bf16[2048,256]{1,0:T(8,128)(2,1)S(1)}, u32[]{:S(2)}, u32[]{:S(2)}) collective-permute-start(bf16[2048,256]{1,0:T(8,128)(2,1)} %dynamic-slice_bitcast_fusion.2), channel_id=1, source_target_pairs={{0,1},{1,0},{2,3},{3,2},{4,5},{5,4},{6,7},{7,6},{8,9},{9,8},{10,11... | collective-permute-start | bytes 3145736 | tf_op jit(solution)/shard_map/ppermute | solution.py:399
  92.5 51.1 %collective-permute-start.20 = (bf16[2048,256]{1,0:T(8,128)(2,1)S(1)}, bf16[2048,256]{1,0:T(8,128)(2,1)S(1)}, u32[]{:S(2)}, u32[]{:S(2)}) collective-permute-start(bf16[2048,256]{1,0:T(8,128)(2,1)S(1)} %dynamic-slice_bitcast_fusion.1), channel_id=1, source_target_pairs={{0,1},{1,0},{2,3},{3,2},{4,5},{5,4},{6,7},{7,6},{8,9},{9,8},{10,11... | collective-permute-start | bytes 3145736 | tf_op jit(solution)/shard_map/ppermute | solution.py:399
  94.3 49.4 %collective-permute-start.21 = (bf16[256,2048]{1,0:T(8,128)(2,1)S(1)}, bf16[256,2048]{1,0:T(8,128)(2,1)S(1)}, u32[]{:S(2)}, u32[]{:S(2)}) collective-permute-start(bf16[256,2048]{1,0:T(8,128)(2,1)S(1)} %dynamic-slice_bitcast_fusion), channel_id=1, source_target_pairs={{0,1},{1,0},{2,3},{3,2},{4,5},{5,4},{6,7},{7,6},{8,9},{9,8},{10,11... | collective-permute-start | bytes 3145736 | tf_op jit(solution)/shard_map/ppermute | solution.py:399
  119.5 6.8 %collective-permute-start.14 = (bf16[784,128]{1,0:T(8,128)(2,1)}, bf16[784,128]{1,0:T(8,128)(2,1)S(1)}, u32[]{:S(2)}, u32[]{:S(2)}) collective-permute-start(bf16[784,128]{1,0:T(8,128)(2,1)} %get-tuple-element.13), channel_id=1, source_target_pairs={{0,192},{16,208},{32,224},{48,240},{64,0},{80,16},{96,32},{112,48}... | collective-permute-start | bytes 602120 | tf_op jit(solution)/shard_map/ppermute | solution.py:395
  120.1 37.0 %collective-permute-start.18 = (bf16[128,2048]{1,0:T(8,128)(2,1)}, bf16[128,2048]{1,0:T(8,128)(2,1)}, u32[]{:S(2)}, u32[]{:S(2)}) collective-permute-start(bf16[128,2048]{1,0:T(8,128)(2,1)} %w_own_ref.1), channel_id=1, source_target_pairs={{0,1},{1,0},{2,3},{3,2},{4,5},{5,4},{6,7},{7,6},{8,9},{9,8},{10,11... | collective-permute-start | bytes 1572872 | tf_op jit(solution)/shard_map/ppermute | solution.py:402
  126.3 7.2 %collective-permute-start.15 = (bf16[784,128]{1,0:T(8,128)(2,1)}, bf16[784,128]{1,0:T(8,128)(2,1)S(1)}, u32[]{:S(2)}, u32[]{:S(2)}) collective-permute-start(bf16[784,128]{1,0:T(8,128)(2,1)} %get-tuple-element.14), channel_id=1, source_target_pairs={{0,64},{16,80},{32,96},{48,112},{64,128},{80,144},{96,160},{112,17... | collective-permute-start | bytes 602120 | tf_op jit(solution)/shard_map/ppermute | solution.py:395
  133.5 7.4 %collective-permute-start.16 = (bf16[784,128]{1,0:T(8,128)(2,1)}, bf16[784,128]{1,0:T(8,128)(2,1)S(1)}, u32[]{:S(2)}, u32[]{:S(2)}) collective-permute-start(bf16[784,128]{1,0:T(8,128)(2,1)} %get-tuple-element.15), channel_id=1, source_target_pairs={{0,128},{16,144},{32,160},{48,176},{64,192},{80,208},{96,224},{112... | collective-permute-start | bytes 602120 | tf_op jit(solution)/shard_map/ppermute | solution.py:395
  143.6 13.4 %collective-permute-start.17 = (bf16[384,128]{1,0:T(8,128)(2,1)}, bf16[384,128]{1,0:T(8,128)(2,1)S(1)}, u32[]{:S(2)}, u32[]{:S(2)}) collective-permute-start(bf16[384,128]{1,0:T(8,128)(2,1)} %get-tuple-element.17), channel_id=1, source_target_pairs={{0,1},{1,0},{2,3},{3,2},{4,5},{5,4},{6,7},{7,6},{8,9},{9,8},{10,11... | collective-permute-start | bytes 294920 | tf_op jit(solution)/shard_map/ppermute | solution.py:434
  241.3 17.8 %all-to-all-start.1 = ((bf16[32,4,2048]{2,1,0:T(4,128)(2,1)}), bf16[32,4,2048]{2,1,0:T(4,128)(2,1)S(1)}, u32[]{:S(2)}, u32[]{:S(2)}) async-start(bf16[32,4,2048]{2,1,0:T(4,128)(2,1)} %reshape.71), calls=%async_computation.2 | async-start | bytes 1048576 | tf_op jit(solution)/shard_map/all_to_all | solution.py:459
  (28 other events, 200.8 us)
Sparse Core Ops, SparseCore 0:
  29.5 65.8 all-gather.1
  161.1 78.0 reduce-scatter.1

commit v3 on v2

--- a/solution.py
+++ b/solution.py
@@ -40,7 +40,8 @@
     parts = [p[:, j : j + LANES] for p in (q, kv) for j in range(0, p.shape[1], LANES)]
     parts.append(jnp.concatenate([rope, jnp.zeros_like(rope)], axis=1))
     for n, part in enumerate(parts):
-        out_ref[n * rows : (n + 1) * rows, :] = part
+        for peer in range(out_ref.shape[0]):
+            out_ref[peer, n * rows : (n + 1) * rows, :] = part
 
 
 def square(row):
@@ -136,28 +137,30 @@
     kv_ref[4 * half :, :] = jnp.concatenate([k_rope[:half], k_rope[half:]], axis=1)
 
 
-def attend(q_refs, kv_refs, start, finish, qs, ks, vs):
+def attend_body(*refs):
+    q_refs, kv_refs, out_refs = refs[:SIDE], refs[SIDE : 2 * SIDE], refs[2 * SIDE : 3 * SIDE]
+    qs, ks, vs, acc_ref = refs[3 * SIDE :]
     rows = qs.shape[0] // SIDE
     half = rows // 2
     zero = jnp.zeros((half, ROPE_DIM), BF16)
     ones = jnp.ones((rows, LANES), BF16)
-    staged = [(r, qs, b, rows) for b, r in enumerate(q_refs)]
-    staged += [(r, ks, b, 2 * rows) for b, r in enumerate(kv_refs)]
-    for src, dst, b, off in staged:
+    for b in range(SIDE):
         at = b * rows
-        dst[at : at + rows, :NOPE_DIM] = src[:rows, :]
-        packed = src[off : off + half, :]
-        dst[at : at + half, NOPE_DIM:] = jnp.concatenate([packed[:, :ROPE_DIM], zero], axis=1)
-        dst[at + half : at + rows, NOPE_DIM:] = jnp.concatenate([packed[:, ROPE_DIM:], zero], axis=1)
-    for b, src in enumerate(kv_refs):
-        vs[b * rows : (b + 1) * rows, :VALUE_DIM] = src[rows : 2 * rows, :]
-        vs[b * rows : (b + 1) * rows, VALUE_DIM:] = ones
+        for src, dst, off in ((q_refs[b], qs, rows), (kv_refs[b], ks, 2 * rows)):
+            dst[at : at + rows, :NOPE_DIM] = src[:rows, :]
+            packed = src[off : off + half, :]
+            dst[at : at + half, NOPE_DIM:] = jnp.concatenate([packed[:, :ROPE_DIM], zero], axis=1)
+            dst[at + half : at + rows, NOPE_DIM:] = jnp.concatenate(
+                [packed[:, ROPE_DIM:], zero], axis=1
+            )
+        vs[at : at + rows, :VALUE_DIM] = kv_refs[b][rows : 2 * rows, :]
+        vs[at : at + rows, VALUE_DIM:] = ones
 
     def block(i, carry):
         here = pl.ds(pl.multiple_of(i * rows, rows), rows)
         q = qs[here, :]
-        acc = start(here)
-        for b in range(len(kv_refs)):
+        acc = None
+        for b in range(SIDE):
             there = slice(b * rows, (b + 1) * rows)
             scores = lax.dot_general(
                 q, ks[there, :], (((1,), (1,)), ((), ())), preferred_element_type=F32
@@ -165,30 +168,10 @@
             probs = jnp.exp2(scores).astype(BF16)
             term = jnp.dot(probs, vs[there, :], preferred_element_type=F32)
             acc = term if acc is None else acc + term
-        finish(here, acc)
+        acc_ref[here, :] = acc
         return carry
 
     lax.fori_loop(0, SIDE, block, 0)
-
-
-def near_body(*refs):
-    q_refs, kv_refs, (acc_ref, qs, ks, vs) = refs[:SIDE], refs[SIDE:-4], refs[-4:]
-
-    def finish(here, acc):
-        acc_ref[here, :] = acc
-
-    attend(q_refs, kv_refs, lambda here: None, finish, qs, ks, vs)
-
-
-def far_body(*refs):
-    q_refs, (kv_ref, in_ref), rest = refs[:SIDE], refs[SIDE : SIDE + 2], refs[SIDE + 2 :]
-    out_refs, (qs, ks, vs, acc_ref) = rest[:SIDE], rest[SIDE:]
-    rows = qs.shape[0] // SIDE
-
-    def finish(here, acc):
-        acc_ref[here, :] = acc
-
-    attend(q_refs, (kv_ref,), lambda here: in_ref[here, :], finish, qs, ks, vs)
     for b in range(SIDE):
         at = b * rows
         out_refs[b][:rows, :] = acc_ref[at : at + rows, :VALUE_DIM].astype(BF16)
@@ -200,11 +183,6 @@
             out_refs[b][rows + 8 + j : rows + 8 + j + 1, :] = low
 
 
-def stack_body(*refs):
-    for n, ref in enumerate(refs[:-1]):
-        refs[-1][n, :, :] = ref[...]
-
-
 def join_body(*refs):
     parts, outs = refs[:SIDE], refs[SIDE:]
     half = outs[0].shape[0]
@@ -221,7 +199,7 @@
         outs[j * LANES // half][at : at + LANES, :] = (head * scale).astype(BF16)
 
 
-def mix_body(chip_ref, own_ref, twin_ref, w_own_ref, w_twin_ref, _, out_ref, term_ref, sems):
+def mix_body(own_ref, twin_ref, w_own_ref, w_twin_ref, _, out_ref, term_ref, sems):
     owners, span, _ = out_ref.shape
     each = own_ref.shape[0] // owners
     step = owners // 2
@@ -234,7 +212,7 @@
         for i in range(c * step, (c + 1) * step):
             copy = pltpu.make_async_copy(
                 term_ref.at[pl.ds(i * each, each), :],
-                out_ref.at[(chip_ref[0] + owners - i) % owners, pl.ds(span - each, each), :],
+                out_ref.at[i, pl.ds(span - each, each), :],
                 sems.at[i],
             )
             copy.start()
@@ -295,7 +273,7 @@
     width = tokens_b.shape[1]
     slots = EXPERTS * CAP
     tp_at = lax.axis_index("tp")
-    core, chip = tp_at % 2, tp_at // 2
+    core = tp_at % 2
     same_core = [[z * 2 + c for z in range(chips)] for c in range(2)]
     plane = [
         [e * tp_count + z * 2 + c for e in range(ep_count) for c in range(2)] for z in range(chips)
@@ -305,11 +283,12 @@
     height = own * ((q_latent.shape[1] + kv_latent.shape[1]) // LANES + 1)
     latent = pl.pallas_call(
         latent_body,
-        out_shape=jax.ShapeDtypeStruct((height, LANES), BF16),
+        out_shape=jax.ShapeDtypeStruct((chips, height, LANES), BF16),
         compiler_params=params(),
         name="latents",
     )(q_latent, kv_latent, rope_key, q_latent_gain[None], kv_latent_gain[None])
 
+    latent, tokens_b = lax.optimization_barrier((latent, tokens_b))
     id_rows = expert_ids.T
     outgoing = pl.pallas_call(
         dispatch_body,
@@ -325,23 +304,14 @@
         arrived.reshape(slots, width), "tp", axis=0, axis_index_groups=same_core
     )
 
-    mine = [latent] + [
-        lax.ppermute(latent, "tp", [(i, (i + 2 * k) % tp_count) for i in range(tp_count)])
-        for k in range(1, chips)
-    ]
-    mine = pl.pallas_call(
-        stack_body,
-        out_shape=jax.ShapeDtypeStruct((chips, height, LANES), BF16),
-        compiler_params=params(),
-        name="stack",
-    )(*mine)
+    mine = lax.all_to_all(latent, "tp", 0, 0, axis_index_groups=same_core)
     other = lax.ppermute(mine, "tp", swap)
 
     block = jnp.arange(rows, dtype=jnp.int32) // own
     side = jnp.where(block < chips, core, 1 - core)
     positions = (
         lax.axis_index("ep") * rows
-        + (((chip - block) % chips) * 2 + side) * own
+        + ((block % chips) * 2 + side) * own
         + jnp.arange(rows, dtype=jnp.int32) % own
     )
     inverse = THETA ** (-jnp.arange(0, ROPE_DIM, 2, dtype=F32) / ROPE_DIM)
@@ -350,7 +320,7 @@
     cosine = jnp.concatenate([cosine, cosine], axis=1)
     sine = jnp.concatenate([-sine, sine], axis=1)
 
-    q_own, kv_own = pl.pallas_call(
+    project = pl.pallas_call(
         project_body,
         out_shape=(
             jax.ShapeDtypeStruct((rows + rows // 2, LANES), BF16),
@@ -362,43 +332,29 @@
         ],
         compiler_params=params(),
         name="project",
-    )(mine, other, w_query, w_key, w_value, query_gain[None], key_gain[None], cosine, sine)
-
-    kv_near = [kv_own] + [lax.ppermute(kv_own, "ep", shift(d, 0)) for d in (1, 3)]
+    )
+    q_own, kv_own = project(
+        mine, other, w_query, w_key, w_value, query_gain[None], key_gain[None], cosine, sine
+    )
+
+    kv_all = [kv_own] + [lax.ppermute(kv_own, "ep", shift(d, 0)) for d in (1, 3, 2)]
     q_all = [q_own] + [lax.ppermute(q_own, "ep", shift(0, d)) for d in (1, 3, 2)]
-    kv_far = lax.ppermute(kv_own, "ep", shift(2, 0))
-    wide = 2 * LANES
-    acc = pl.pallas_call(
-        near_body,
-        out_shape=jax.ShapeDtypeStruct((SIDE * rows, wide), F32),
-        scratch_shapes=[
-            pltpu.VMEM((SIDE * rows, wide), BF16),
-            pltpu.VMEM((3 * rows, wide), BF16),
-            pltpu.VMEM((3 * rows, wide), BF16),
-        ],
-        compiler_params=params(),
-        name="near",
-    )(*q_all, *kv_near)
     partial = pl.pallas_call(
-        far_body,
+        attend_body,
         out_shape=[jax.ShapeDtypeStruct((rows + 16, LANES), BF16)] * SIDE,
-        scratch_shapes=[
-            pltpu.VMEM((SIDE * rows, wide), BF16),
-            pltpu.VMEM((rows, wide), BF16),
-            pltpu.VMEM((rows, wide), BF16),
-            pltpu.VMEM((SIDE * rows, wide), F32),
-        ],
-        compiler_params=params(),
-        name="far",
-    )(*q_all, kv_far, acc)
+        scratch_shapes=[pltpu.VMEM((SIDE * rows, 2 * LANES), BF16)] * 3
+        + [pltpu.VMEM((SIDE * rows, 2 * LANES), F32)],
+        compiler_params=params(),
+        name="attend",
+    )(*q_all, *kv_all)
     parts = [partial[0]] + [
         lax.ppermute(p, "ep", shift(0, -d)) for p, d in zip(partial[1:], (1, 3, 2))
     ]
 
-    twin = [
-        lax.ppermute(lax.dynamic_index_in_dim(w, 1 - core, 0, False), "tp", swap)
-        for w in (w_gate, w_up, w_down)
-    ]
+    picked = []
+    for w in (w_down, w_gate, w_up):
+        picked.append(lax.dynamic_index_in_dim(w, 1 - core, 0, False))
+    down_twin, *twin = [lax.ppermute(w, "tp", swap) for w in picked]
     mix_twin = lax.ppermute(w_mix, "tp", swap)
 
     span = slots + own
@@ -423,7 +379,7 @@
         ),
         compiler_params=params(),
         name="experts",
-    )(core.reshape(1), everyone, w_gate, w_up, w_down, *twin)
+    )(core.reshape(1), everyone, w_gate, w_up, w_down, *twin, down_twin)
 
     own_head, twin_head = pl.pallas_call(
         join_body,
@@ -435,18 +391,17 @@
     terms = pl.pallas_call(
         mix_body,
         out_shape=jax.ShapeDtypeStruct((chips, span, width), BF16),
-        in_specs=[pl.BlockSpec(memory_space=pltpu.SMEM)]
-        + [pl.BlockSpec(memory_space=pltpu.VMEM)] * 4
+        in_specs=[pl.BlockSpec(memory_space=pltpu.VMEM)] * 4
         + [pl.BlockSpec(memory_space=pl.ANY)],
         out_specs=pl.BlockSpec(memory_space=pl.ANY),
         scratch_shapes=[
             pltpu.VMEM((half, width), BF16),
             pltpu.SemaphoreType.DMA((chips,)),
         ],
-        input_output_aliases={5: 0},
+        input_output_aliases={4: 0},
         compiler_params=params(),
         name="mix",
-    )(chip.reshape(1), own_head, twin_head, w_mix, mix_twin, terms)
+    )(own_head, twin_head, w_mix, mix_twin, terms)
 
     summed = lax.psum_scatter(
         terms.reshape(chips * span, width),
@@ -457,7 +412,7 @@
     )
     mix_out = summed[slots:]
     returned = lax.all_to_all(
-        summed[:slots].reshape(EXPERTS, CAP, width), ("ep", "tp"), 0, 0, axis_index_groups=plane
+        summed.reshape(span // CAP, CAP, width)[:EXPERTS], ("ep", "tp"), 0, 0, axis_index_groups=plane
     )
     expert_out = pl.pallas_call(
         collect_body,

time: 272 us -> 265 us (0.974)
  waiting for transfers between devices: 130 us -> 143 us
  starting transfers between devices: 34.7 us -> 23.8 us
  Pallas kernels: 53.1 us -> 45.9 us
    all_to_all x1 -> x2, waiting for transfers between devices: 8.76 us -> 33.6 us  [the longest x1 24.9 us: on_device(): mine = lax.all_to_all(latent, 'tp', 0, 0, axis_index_groups=same_core)]
    ppermute x11 -> x3, starting transfers between devices: 20.1 us -> 0.86 us  [on_device(): down_twin, *twin = [lax.ppermute(w, 'tp', swap) for w in picked]]
    ppermute x11 -> x3, waiting for transfers between devices: 12.7 us -> 0.01 us  [on_device(): down_twin, *twin = [lax.ppermute(w, 'tp', swap) for w in picked]]
    reduce_scatter x1, waiting for transfers between devices: 78.2 us -> 66.7 us  [on_device(): lax.psum_scatter(terms.reshape(chips * span, width), 'tp', scatter_dimens...]
    ppermute x2 -> x3, waiting for transfers between devices: 1.35 us -> 11.3 us  [on_device(): lax.ppermute(kv_own, 'ep', shift(d, 0))]
    all_to_all x1 -> x2, starting transfers between devices: 7.41 us -> 15.9 us  [the longest x1 8.47 us: on_device(): mine = lax.all_to_all(latent, 'tp', 0, 0, axis_index_groups=same_core)]
    pallas_call x5 -> x3, Pallas kernels: 31.6 us -> 24.4 us  [the longest x1 17.4 us: on_device(): pl.pallas_call(attend_body, out_shape=[jax.ShapeDtypeStruct((rows + 16, L...]
    unnamed x55 -> x39, local copies, waits for them, and re-layouts: 7.71 us -> 6 us
  transfers between devices with their start and end apart: 25 -> 19, of which waited for: 13 -> 8; matrix products, arithmetic and copies ran while one was open for 3% -> 2% of each run, Pallas kernels for 17% -> 14%
where the time goes in v3:
time: 265 us; the launch traced here: 263 us
  waiting for transfers between devices  143 us (54%)
  Pallas kernels  45.9 us (17%)
  starting transfers between devices  23.8 us (9%)
  blocking collectives  17.9 us (7%)
  local copies, waits for them, and re-layouts  15.3 us (6%)
  between operations  14.3 us (5%)
    reduce_scatter x1, waiting for transfers between devices, on_device(): lax.psum_scatter(terms.reshape(chips * span, width), 'tp', scatter_dimens...  66.7 us
    all_to_all x1, waiting for transfers between devices, on_device(): mine = lax.all_to_all(latent, 'tp', 0, 0, axis_index_groups=same_core)  24.9 us
    ppermute x3, waiting for transfers between devices, on_device(): lax.ppermute(p, 'ep', shift(0, -d))  20.5 us
    all_to_all x1, blocking collectives, on_device(): lax.all_to_all(outgoing.reshape(EXPERTS, CAP, width), ('ep', 'tp'), 0, 0,...  17.9 us
    pallas_call x1, Pallas kernels, on_device(): pl.pallas_call(attend_body, out_shape=[jax.ShapeDtypeStruct((rows + 16, L...  17.4 us
    pallas_call x1, Pallas kernels, on_device(): pl.pallas_call(expert_body, out_shape=jax.ShapeDtypeStruct((chips, span,...  11.6 us
    ppermute x3, waiting for transfers between devices, on_device(): lax.ppermute(kv_own, 'ep', shift(d, 0))  11.3 us
    ppermute x3, waiting for transfers between devices, on_device(): lax.ppermute(q_own, 'ep', shift(0, d))  10.7 us
  transfers between devices with their start and end apart: 19, of which 8 were waited for; matrix products, arithmetic and copies ran while one was open for 2% of the time, Pallas kernels for 14%

profile of v3, /device:TPU:2, one launch (start us, length us, event | category | flops | bytes accessed | tf_op | source)
XLA Modules:
  0.0 262.9 jit_solution(16879981590351819573)
XLA Ops:
  8.5 1.7 latents.1
  10.2 2.2 dispatch.1
  13.7 17.9 %all_to_all.15 = bf16[32,4,2048]{2,1,0:T(4,128)(2,1)S(1)} all-to-all(bf16[32,4,2048]{2,1,0:T(4,128)(2,1)S(1)} %reshape.63), channel_id=1, replica_groups={{0,1,16,17,32,33,48,49,64,65,80,81,96,97,112,113,128,129,144,145,160,16..., dimensions={0} | all-to-all | bytes 1048576 | tf_op jit(solution)/shard_map/all_to_all | solution.py:300
  32.5 8.5 %all-to-all-start = ((bf16[8,288,128]{2,1,0:T(8,128)(2,1)}), bf16[8,288,128]{2,1,0:T(8,128)(2,1)S(1)}, u32[]{:S(2)}, u32[]{:S(2)}) async-start(bf16[8,288,128]{2,1,0:T(8,128)(2,1)} %latents.1), calls=%async_computation | async-start | bytes 1179648 | tf_op jit(solution)/shard_map/all_to_all | solution.py:307
  41.9 24.9 %all-to-all-done.mine_ref = bf16[8,288,128]{2,1,0:T(8,128)(2,1)S(1)} async-done(((bf16[8,288,128]{2,1,0:T(8,128)(2,1)}), bf16[8,288,128]{2,1,0:T(8,128)(2,1)S(1)}, u32[]{:S(2)}, u32[]{:S(2)}) %all-to-all-start) | async-done | bytes 589856 | tf_op jit(solution)/shard_map/all_to_all | solution.py:307
  66.8 1.4 fusion
  70.3 5.3 %project.1 = (bf16[1152,128]{1,0:T(8,128)(2,1)}, bf16[1920,128]{1,0:T(8,128)(2,1)}) custom-call(bf16[8,288,128]{2,1,0:T(8,128)(2,1)} %copy-done.3, bf16[8,288,128]{2,1,0:T(8,128)(2,1)} %copy-done.7, bf16[384,192]{1,0:T(8,128)(2,1)} %copy.24.wq_ref, bf16[256,128]{1,0:T(8,128)(2,1)} %wk_ref.1, bf16[256,128]{1,0:T(8,128)(2,1)} %wv_ref.1, f32[1,192]{1,0:T(1,128)} %bitcast.19, ...), custom_call_target="tpu_custom_call" | custom-call | tf_op jit(solution)/shard_map/project/pallas_call | solution.py:336
  76.8 3.2 %collective-permute-start.2 = (bf16[1152,128]{1,0:T(8,128)(2,1)S(1)}, bf16[1152,128]{1,0:T(8,128)(2,1)}, u32[]{:S(2)}, u32[]{:S(2)}) collective-permute-start(bf16[1152,128]{1,0:T(8,128)(2,1)S(1)} %copy-done.12), channel_id=1, source_target_pairs={{0,192},{16,208},{32,224},{48,240},{64,0},{80,16},{96,32},{112,48}... | collective-permute-start | bytes 884744 | tf_op jit(solution)/shard_map/ppermute | solution.py:341
  80.1 2.1 collective-permute-start.5
  82.2 10.7 %collective-permute-done.1.refs_1_ = bf16[1152,128]{1,0:T(8,128)(2,1)S(1)} collective-permute-done((bf16[1152,128]{1,0:T(8,128)(2,1)}, bf16[1152,128]{1,0:T(8,128)(2,1)S(1)}, u32[]{:S(2)}, u32[]{:S(2)}) %collective-permute-start.1) | collective-permute-done | bytes 294944 | tf_op jit(solution)/shard_map/ppermute | solution.py:341
  92.9 1.6 collective-permute-start.6
  95.9 11.3 %collective-permute-done.6.refs_7_ = bf16[1920,128]{1,0:T(8,128)(2,1)S(1)} collective-permute-done((bf16[1920,128]{1,0:T(8,128)(2,1)S(1)}, bf16[1920,128]{1,0:T(8,128)(2,1)S(1)}, u32[]{:S(2)}, u32[]{:S(2)}) %collective-permute-start.6) | collective-permute-done | bytes 491552 | tf_op jit(solution)/shard_map/ppermute | solution.py:340
  108.1 17.4 %attend.1 = (bf16[784,128]{1,0:T(8,128)(2,1)}, bf16[784,128]{1,0:T(8,128)(2,1)}, bf16[784,128]{1,0:T(8,128)(2,1)}, bf16[784,128]{1,0:T(8,128)(2,1)}) custom-call(bf16[1152,128]{1,0:T(8,128)(2,1)} %get-tuple-element.13.refs_0_, bf16[1152,128]{1,0:T(8,128)(2,1)} %copy-done.13, bf16[1152,128]{1,0:T(8,128)(2,1)} %collective-permute-done.2.refs_2_, ...), custom_call_target="tpu_custom_call" | custom-call | tf_op jit(solution)/shard_map/attend/pallas_call | solution.py:342
  125.5 6.0 %collective-permute-done.7.refs_1_ = bf16[784,128]{1,0:T(8,128)(2,1)S(1)} collective-permute-done((bf16[784,128]{1,0:T(8,128)(2,1)}, bf16[784,128]{1,0:T(8,128)(2,1)S(1)}, u32[]{:S(2)}, u32[]{:S(2)}) %collective-permute-start.7) | collective-permute-done | bytes 200736 | tf_op jit(solution)/shard_map/ppermute | solution.py:351
  131.5 7.1 %collective-permute-done.8.refs_2_ = bf16[784,128]{1,0:T(8,128)(2,1)S(1)} collective-permute-done((bf16[784,128]{1,0:T(8,128)(2,1)}, bf16[784,128]{1,0:T(8,128)(2,1)S(1)}, u32[]{:S(2)}, u32[]{:S(2)}) %collective-permute-start.8) | collective-permute-done | bytes 200736 | tf_op jit(solution)/shard_map/ppermute | solution.py:351
  138.6 7.4 %collective-permute-done.9.refs_3_ = bf16[784,128]{1,0:T(8,128)(2,1)S(1)} collective-permute-done((bf16[784,128]{1,0:T(8,128)(2,1)}, bf16[784,128]{1,0:T(8,128)(2,1)S(1)}, u32[]{:S(2)}, u32[]{:S(2)}) %collective-permute-start.9) | collective-permute-done | bytes 200736 | tf_op jit(solution)/shard_map/ppermute | solution.py:351
  146.7 2.0 join.1
  150.5 11.6 %experts.1._ = bf16[8,176,2048]{2,1,0:T(8,128)(2,1)} custom-call(s32[1]{0:T(128)} %bitcast.3.core_ref, bf16[8,128,2048]{2,1,0:T(8,128)(2,1)} %all-gather.2.cloned.1.call-done.x_ref, bf16[2,2048,256]{2,1,0:T(8,128)(2,1)} %refs_0_.1, bf16[2,2048,256]{2,1,0:T(8,128)(2,1)} %refs_1_.1, bf16[2,256,2048]{2,1,0:T(8,128)(2,1)} %refs_2_.1, ...), custom_call_target="tpu_custom_call" | custom-call | tf_op jit(solution)/shard_map/experts/pallas_call | solution.py:363
  162.8 3.3 %mix.1 = bf16[8,176,2048]{2,1,0:T(8,128)(2,1)} custom-call(bf16[384,128]{1,0:T(8,128)(2,1)} %get-tuple-element.19.own_ref, bf16[384,128]{1,0:T(8,128)(2,1)} %copy-done.18, bf16[128,2048]{1,0:T(8,128)(2,1)} %w_own_ref.1, bf16[128,2048]{1,0:T(8,128)(2,1)} %collective-permute-done.11.w_twin_ref, ...), custom_call_target="tpu_custom_call", output_to_operand_aliasing={{}: (4, {})} | custom-call | tf_op jit(solution)/shard_map/mix/pallas_call | solution.py:391
  166.1 66.7 %reduce-scatter.2.cloned.1.call-done = bf16[176,2048]{1,0:T(8,128)(2,1)} async-done(((bf16[1408,2048]{1,0:T(8,128)(2,1)}), bf16[176,2048]{1,0:T(8,128)(2,1)}) %reduce-scatter.2.cloned.1.call-update) | async-done | bytes 720912 | tf_op jit(solution)/shard_map/reduce_scatter | solution.py:406
  234.9 7.4 %all-to-all-start.2 = ((bf16[32,4,2048]{2,1,0:T(4,128)(2,1)}), bf16[32,4,2048]{2,1,0:T(4,128)(2,1)S(1)}, u32[]{:S(2)}, u32[]{:S(2)}) async-start(bf16[32,4,2048]{2,1,0:T(4,128)(2,1)} %slice.11), calls=%async_computation.3 | async-start | bytes 1048576 | tf_op jit(solution)/shard_map/all_to_all | solution.py:414
  242.4 1.6 slice.12
  244.0 8.8 %all-to-all-done.2 = bf16[32,4,2048]{2,1,0:T(4,128)(2,1)S(1)} async-done(((bf16[32,4,2048]{2,1,0:T(4,128)(2,1)}), bf16[32,4,2048]{2,1,0:T(4,128)(2,1)S(1)}, u32[]{:S(2)}, u32[]{:S(2)}) %all-to-all-start.2) | async-done | bytes 524320 | tf_op jit(solution)/shard_map/all_to_all | solution.py:414
  253.7 2.4 collect.1
  (78 shorter events, 16.0 us)
Async XLA Ops:
  7.2 141.7 %all-gather.2.cloned.1.call-start = ((), (), s32[]{:S(2)}) async-start(), calls=%async_computation.4 | async-start | bytes 4718592 | tf_op jit(solution)/shard_map/all_gather | solution.py:303
  13.6 27.4 %copy-start.17 = (bf16[384,192]{0,1:T(8,128)(2,1)S(1)}, bf16[384,192]{0,1:T(8,128)(2,1)}, u32[]{:S(2)}) copy-start(bf16[384,192]{0,1:T(8,128)(2,1)} %param.23) | copy-start | bytes 442372
  32.5 34.3 %all-to-all-start = ((bf16[8,288,128]{2,1,0:T(8,128)(2,1)}), bf16[8,288,128]{2,1,0:T(8,128)(2,1)S(1)}, u32[]{:S(2)}, u32[]{:S(2)}) async-start(bf16[8,288,128]{2,1,0:T(8,128)(2,1)} %latents.1), calls=%async_computation | async-start | bytes 1179648 | tf_op jit(solution)/shard_map/all_to_all | solution.py:307
  41.0 191.8 %reduce-scatter.2.cloned.1.call-start = ((), (), s32[]{:S(2)}) async-start(), calls=%async_computation.5 | async-start | bytes 6488064 | tf_op jit(solution)/shard_map/reduce_scatter | solution.py:406
  66.8 2.7 %collective-permute-start = (bf16[8,288,128]{2,1,0:T(8,128)(2,1)S(1)}, bf16[8,288,128]{2,1,0:T(8,128)(2,1)S(1)}, u32[]{:S(2)}, u32[]{:S(2)}) collective-permute-start(bf16[8,288,128]{2,1,0:T(8,128)(2,1)S(1)} %all-to-all-done.mine_ref), channel_id=1, source_target_pairs={{0,1},{1,0},{2,3},{3,2},{4,5},{5,4},{6,7},{7,6},{8,9},{9,8},{10,11... | collective-permute-start | bytes 1769480 | tf_op jit(solution)/shard_map/ppermute | solution.py:308
  70.3 9.7 %copy-start.1 = (bf16[2,2048,256]{2,1,0:T(8,128)(2,1)S(1)}, bf16[2,2048,256]{2,1,0:T(8,128)(2,1)}, u32[]{:S(2)}) copy-start(bf16[2,2048,256]{2,1,0:T(8,128)(2,1)} %refs_1_.1) | copy-start | bytes 6291460
  75.6 18.8 %copy-start.2 = (bf16[2,256,2048]{2,1,0:T(8,128)(2,1)S(1)}, bf16[2,256,2048]{2,1,0:T(8,128)(2,1)}, u32[]{:S(2)}) copy-start(bf16[2,256,2048]{2,1,0:T(8,128)(2,1)} %refs_2_.1) | copy-start | bytes 6291460
  75.6 17.3 %collective-permute-start.1 = (bf16[1152,128]{1,0:T(8,128)(2,1)}, bf16[1152,128]{1,0:T(8,128)(2,1)S(1)}, u32[]{:S(2)}, u32[]{:S(2)}) collective-permute-start(bf16[1152,128]{1,0:T(8,128)(2,1)} %get-tuple-element.13.refs_0_), channel_id=1, source_target_pairs={{0,64},{16,80},{32,96},{48,112},{64,128},{80,144},{96,160},{112,17... | collective-permute-start | bytes 884744 | tf_op jit(solution)/shard_map/ppermute | solution.py:341
  76.8 17.7 %collective-permute-start.2 = (bf16[1152,128]{1,0:T(8,128)(2,1)S(1)}, bf16[1152,128]{1,0:T(8,128)(2,1)}, u32[]{:S(2)}, u32[]{:S(2)}) collective-permute-start(bf16[1152,128]{1,0:T(8,128)(2,1)S(1)} %copy-done.12), channel_id=1, source_target_pairs={{0,192},{16,208},{32,224},{48,240},{64,0},{80,16},{96,32},{112,48}... | collective-permute-start | bytes 884744 | tf_op jit(solution)/shard_map/ppermute | solution.py:341
  80.0 14.6 %collective-permute-start.3 = (bf16[1152,128]{1,0:T(8,128)(2,1)S(1)}, bf16[1152,128]{1,0:T(8,128)(2,1)}, u32[]{:S(2)}, u32[]{:S(2)}) collective-permute-start(bf16[1152,128]{1,0:T(8,128)(2,1)S(1)} %copy-done.12), channel_id=1, source_target_pairs={{0,128},{16,144},{32,160},{48,176},{64,192},{80,208},{96,224},{112... | collective-permute-start | bytes 884744 | tf_op jit(solution)/shard_map/ppermute | solution.py:341
  80.0 15.1 %collective-permute-start.4 = (bf16[1920,128]{1,0:T(8,128)(2,1)S(1)}, bf16[1920,128]{1,0:T(8,128)(2,1)S(1)}, u32[]{:S(2)}, u32[]{:S(2)}) collective-permute-start(bf16[1920,128]{1,0:T(8,128)(2,1)S(1)} %copy-done.8), channel_id=1, source_target_pairs={{0,16},{16,32},{32,48},{48,0},{64,80},{80,96},{96,112},{112,64},{1... | collective-permute-start | bytes 1474568 | tf_op jit(solution)/shard_map/ppermute | solution.py:340
  80.1 15.3 %collective-permute-start.5 = (bf16[1920,128]{1,0:T(8,128)(2,1)S(1)}, bf16[1920,128]{1,0:T(8,128)(2,1)S(1)}, u32[]{:S(2)}, u32[]{:S(2)}) collective-permute-start(bf16[1920,128]{1,0:T(8,128)(2,1)S(1)} %copy-done.8), channel_id=1, source_target_pairs={{0,48},{16,0},{32,16},{48,32},{64,112},{80,64},{96,80},{112,96},{1... | collective-permute-start | bytes 1474568 | tf_op jit(solution)/shard_map/ppermute | solution.py:340
  92.9 14.4 %collective-permute-start.6 = (bf16[1920,128]{1,0:T(8,128)(2,1)S(1)}, bf16[1920,128]{1,0:T(8,128)(2,1)S(1)}, u32[]{:S(2)}, u32[]{:S(2)}) collective-permute-start(bf16[1920,128]{1,0:T(8,128)(2,1)S(1)} %copy-done.8), channel_id=1, source_target_pairs={{0,32},{16,48},{32,0},{48,16},{64,96},{80,112},{96,64},{112,80},{1... | collective-permute-start | bytes 1474568 | tf_op jit(solution)/shard_map/ppermute | solution.py:340
  94.5 54.2 %collective-permute-start.12 = (bf16[2048,256]{1,0:T(8,128)(2,1)}, bf16[2048,256]{1,0:T(8,128)(2,1)S(1)}, u32[]{:S(2)}, u32[]{:S(2)}) collective-permute-start(bf16[2048,256]{1,0:T(8,128)(2,1)} %dynamic-slice_bitcast_fusion.2), channel_id=1, source_target_pairs={{0,1},{1,0},{2,3},{3,2},{4,5},{5,4},{6,7},{7,6},{8,9},{9,8},{10,11... | collective-permute-start | bytes 3145736 | tf_op jit(solution)/shard_map/ppermute | solution.py:357
  94.7 54.1 %collective-permute-start.13 = (bf16[2048,256]{1,0:T(8,128)(2,1)S(1)}, bf16[2048,256]{1,0:T(8,128)(2,1)S(1)}, u32[]{:S(2)}, u32[]{:S(2)}) collective-permute-start(bf16[2048,256]{1,0:T(8,128)(2,1)S(1)} %dynamic-slice_bitcast_fusion.1), channel_id=1, source_target_pairs={{0,1},{1,0},{2,3},{3,2},{4,5},{5,4},{6,7},{7,6},{8,9},{9,8},{10,11... | collective-permute-start | bytes 3145736 | tf_op jit(solution)/shard_map/ppermute | solution.py:357
  95.1 53.6 %collective-permute-start.14 = (bf16[256,2048]{1,0:T(8,128)(2,1)S(1)}, bf16[256,2048]{1,0:T(8,128)(2,1)S(1)}, u32[]{:S(2)}, u32[]{:S(2)}) collective-permute-start(bf16[256,2048]{1,0:T(8,128)(2,1)S(1)} %dynamic-slice_bitcast_fusion), channel_id=1, source_target_pairs={{0,1},{1,0},{2,3},{3,2},{4,5},{5,4},{6,7},{7,6},{8,9},{9,8},{10,11... | collective-permute-start | bytes 3145736 | tf_op jit(solution)/shard_map/ppermute | solution.py:357
  95.9 11.3 %copy-start.10 = (bf16[1920,128]{1,0:T(8,128)(2,1)}, bf16[1920,128]{1,0:T(8,128)(2,1)S(1)}, u32[]{:S(2)}) copy-start(bf16[1920,128]{1,0:T(8,128)(2,1)S(1)} %collective-permute-done.5.refs_6_) | copy-start | bytes 1474564
  125.4 6.0 %collective-permute-start.7 = (bf16[784,128]{1,0:T(8,128)(2,1)}, bf16[784,128]{1,0:T(8,128)(2,1)S(1)}, u32[]{:S(2)}, u32[]{:S(2)}) collective-permute-start(bf16[784,128]{1,0:T(8,128)(2,1)} %get-tuple-element.16), channel_id=1, source_target_pairs={{0,192},{16,208},{32,224},{48,240},{64,0},{80,16},{96,32},{112,48}... | collective-permute-start | bytes 602120 | tf_op jit(solution)/shard_map/ppermute | solution.py:351
  125.4 36.7 %collective-permute-start.11 = (bf16[128,2048]{1,0:T(8,128)(2,1)}, bf16[128,2048]{1,0:T(8,128)(2,1)}, u32[]{:S(2)}, u32[]{:S(2)}) collective-permute-start(bf16[128,2048]{1,0:T(8,128)(2,1)} %w_own_ref.1), channel_id=1, source_target_pairs={{0,1},{1,0},{2,3},{3,2},{4,5},{5,4},{6,7},{7,6},{8,9},{9,8},{10,11... | collective-permute-start | bytes 1572872 | tf_op jit(solution)/shard_map/ppermute | solution.py:358
  131.4 14.6 %copy-start.14 = (bf16[784,128]{1,0:T(8,128)(2,1)}, bf16[784,128]{1,0:T(8,128)(2,1)S(1)}, u32[]{:S(2)}) copy-start(bf16[784,128]{1,0:T(8,128)(2,1)S(1)} %collective-permute-done.7.refs_1_) | copy-start | bytes 602116
  131.4 7.1 %collective-permute-start.8 = (bf16[784,128]{1,0:T(8,128)(2,1)}, bf16[784,128]{1,0:T(8,128)(2,1)S(1)}, u32[]{:S(2)}, u32[]{:S(2)}) collective-permute-start(bf16[784,128]{1,0:T(8,128)(2,1)} %get-tuple-element.17), channel_id=1, source_target_pairs={{0,64},{16,80},{32,96},{48,112},{64,128},{80,144},{96,160},{112,17... | collective-permute-start | bytes 602120 | tf_op jit(solution)/shard_map/ppermute | solution.py:351
  138.6 7.4 %collective-permute-start.9 = (bf16[784,128]{1,0:T(8,128)(2,1)}, bf16[784,128]{1,0:T(8,128)(2,1)S(1)}, u32[]{:S(2)}, u32[]{:S(2)}) collective-permute-start(bf16[784,128]{1,0:T(8,128)(2,1)} %get-tuple-element.18), channel_id=1, source_target_pairs={{0,128},{16,144},{32,160},{48,176},{64,192},{80,208},{96,224},{112... | collective-permute-start | bytes 602120 | tf_op jit(solution)/shard_map/ppermute | solution.py:351
  148.8 13.4 %collective-permute-start.10 = (bf16[384,128]{1,0:T(8,128)(2,1)}, bf16[384,128]{1,0:T(8,128)(2,1)S(1)}, u32[]{:S(2)}, u32[]{:S(2)}) collective-permute-start(bf16[384,128]{1,0:T(8,128)(2,1)} %get-tuple-element.20), channel_id=1, source_target_pairs={{0,1},{1,0},{2,3},{3,2},{4,5},{5,4},{6,7},{7,6},{8,9},{9,8},{10,11... | collective-permute-start | bytes 294920 | tf_op jit(solution)/shard_map/ppermute | solution.py:390
  234.9 17.8 %all-to-all-start.2 = ((bf16[32,4,2048]{2,1,0:T(4,128)(2,1)}), bf16[32,4,2048]{2,1,0:T(4,128)(2,1)S(1)}, u32[]{:S(2)}, u32[]{:S(2)}) async-start(bf16[32,4,2048]{2,1,0:T(4,128)(2,1)} %slice.11), calls=%async_computation.3 | async-start | bytes 1048576 | tf_op jit(solution)/shard_map/all_to_all | solution.py:414
  (14 other events, 32.6 us)
Sparse Core Ops, SparseCore 0:
  32.7 65.0 all-gather.1
  166.3 66.5 reduce-scatter.1

commit v4 on v3

--- a/solution.py
+++ b/solution.py
@@ -34,7 +34,7 @@
 
 def latent_body(q_ref, kv_ref, rope_ref, qg_ref, kvg_ref, out_ref):
     rows = q_ref.shape[0]
-    q = rms(q_ref[...].astype(F32), qg_ref[...]).astype(BF16)
+    q = rms(q_ref[...].astype(F32), qg_ref[...][None, :]).astype(BF16)
     kv = rms(kv_ref[...].astype(F32), kvg_ref[...]).astype(BF16)
     rope = rope_ref[...]
     parts = [p[:, j : j + LANES] for p in (q, kv) for j in range(0, p.shape[1], LANES)]
@@ -69,23 +69,26 @@
 def dispatch_body(tok_ref, gain_ref, rows_ref, out_ref):
     normed = rms(tok_ref[...].astype(F32), gain_ref[...]).astype(BF16)
     first, second = slots_of(rows_ref[...], True)
-    shape = (out_ref.shape[0], normed.shape[0])
+    experts, cap, width = out_ref.shape
+    shape = (experts * cap, normed.shape[0])
     slot = lax.broadcasted_iota(jnp.int32, shape, 0)
     hot = jnp.where((slot == first) | (slot == second), 1.0, 0.0).astype(BF16)
-    out_ref[...] = jnp.dot(hot, normed, preferred_element_type=F32).astype(BF16)
+    picked = jnp.dot(hot, normed, preferred_element_type=F32)
+    out_ref[...] = picked.reshape(experts, cap, width).astype(BF16)
 
 
 def collect_body(back_ref, rows_ref, weight_ref, out_ref):
     first, second = slots_of(rows_ref[...], False)
     count = out_ref.shape[0]
-    slot = lax.broadcasted_iota(jnp.int32, (count, back_ref.shape[0]), 1)
+    slots = back_ref.shape[0] * back_ref.shape[1]
+    slot = lax.broadcasted_iota(jnp.int32, (count, slots), 1)
     weights = [square(weight_ref[k : k + 1, :]).T[:, :1] for k in range(TOP_K)]
     mixed = jnp.where(slot == first, weights[0], 0.0) + jnp.where(slot == second, weights[1], 0.0)
     high = mixed.astype(BF16)
     rest = mixed - high.astype(F32)
     low = rest.astype(BF16)
     last = (rest - low.astype(F32)).astype(BF16)
-    back = back_ref[...]
+    back = back_ref[...].astype(F32).reshape(slots, back_ref.shape[2]).astype(BF16)
     total = jnp.dot(high, back, preferred_element_type=F32)
     total += jnp.dot(low, back, preferred_element_type=F32)
     total += jnp.dot(last, back, preferred_element_type=F32)
@@ -116,7 +119,9 @@
         ropes.append(src[:, (q_parts + kv_parts) * own :, :].reshape(half, LANES)[:, :ROPE_DIM])
     rope = jnp.concatenate(ropes, axis=0).astype(F32)
     cosine, sine = cos_ref[...], sin_ref[...]
-    queries = jnp.dot(lat_q[...], wq_ref[...], preferred_element_type=F32)
+    queries = lax.dot_general(
+        lat_q[...], wq_ref[...], (((1,), (1,)), ((), ())), preferred_element_type=F32
+    )
     scale = HEAD_DIM**-0.5 * LOG2E
     queries = rms(queries, qg_ref[...] * scale)
     q_ref[: 2 * half, :] = queries[:, :NOPE_DIM].astype(BF16)
@@ -236,12 +241,14 @@
     out_ref[...] = out.astype(BF16).reshape(groups, rows, width)
 
 
-def shift(axis_x, axis_y):
-    return [
-        (y * SIDE + x, ((y + axis_y) % SIDE) * SIDE + (x + axis_x) % SIDE)
-        for y in range(SIDE)
-        for x in range(SIDE)
-    ]
+def shift(keys, queries, tp_count):
+    pairs = []
+    for e in range(SIDE * SIDE):
+        for t in range(tp_count):
+            step_x, step_y = (keys, queries) if t % 2 == 0 else (queries, keys)
+            there = (e // SIDE + step_y) % SIDE * SIDE + (e % SIDE + step_x) % SIDE
+            pairs.append((e * tp_count + t, there * tp_count + t))
+    return pairs
 
 
 def on_device(
@@ -280,25 +287,30 @@
     ]
     swap = [(i, i ^ 1) for i in range(tp_count)]
 
+    def move(x, keys, queries):
+        return lax.ppermute(x, ("ep", "tp"), shift(keys, queries, tp_count))
+
+
     height = own * ((q_latent.shape[1] + kv_latent.shape[1]) // LANES + 1)
     latent = pl.pallas_call(
         latent_body,
         out_shape=jax.ShapeDtypeStruct((chips, height, LANES), BF16),
         compiler_params=params(),
         name="latents",
-    )(q_latent, kv_latent, rope_key, q_latent_gain[None], kv_latent_gain[None])
+    )(q_latent, kv_latent, rope_key, q_latent_gain, kv_latent_gain[None])
 
     latent, tokens_b = lax.optimization_barrier((latent, tokens_b))
     id_rows = expert_ids.T
-    outgoing = pl.pallas_call(
+    dispatch = pl.pallas_call(
         dispatch_body,
-        out_shape=jax.ShapeDtypeStruct((slots, width), BF16),
+        out_shape=jax.ShapeDtypeStruct((EXPERTS, CAP, width), BF16),
         compiler_params=params(),
         name="dispatch",
-    )(tokens_b, norm_gain[None], id_rows)
+    )
+    outgoing = dispatch(tokens_b, norm_gain[None], id_rows)
 
     arrived = lax.all_to_all(
-        outgoing.reshape(EXPERTS, CAP, width), ("ep", "tp"), 0, 0, axis_index_groups=plane
+        outgoing, ("ep", "tp"), 0, 0, axis_index_groups=plane
     )
     everyone = lax.all_gather(
         arrived.reshape(slots, width), "tp", axis=0, axis_index_groups=same_core
@@ -334,11 +346,11 @@
         name="project",
     )
     q_own, kv_own = project(
-        mine, other, w_query, w_key, w_value, query_gain[None], key_gain[None], cosine, sine
-    )
-
-    kv_all = [kv_own] + [lax.ppermute(kv_own, "ep", shift(d, 0)) for d in (1, 3, 2)]
-    q_all = [q_own] + [lax.ppermute(q_own, "ep", shift(0, d)) for d in (1, 3, 2)]
+        mine, other, w_query.T, w_key, w_value, query_gain[None], key_gain[None], cosine, sine
+    )
+
+    kv_all = [kv_own] + [move(kv_own, d, 0) for d in (1, 3, 2)]
+    q_all = [q_own] + [move(q_own, 0, d) for d in (1, 3, 2)]
     partial = pl.pallas_call(
         attend_body,
         out_shape=[jax.ShapeDtypeStruct((rows + 16, LANES), BF16)] * SIDE,
@@ -348,7 +360,7 @@
         name="attend",
     )(*q_all, *kv_all)
     parts = [partial[0]] + [
-        lax.ppermute(p, "ep", shift(0, -d)) for p, d in zip(partial[1:], (1, 3, 2))
+        move(p, 0, -d) for p, d in zip(partial[1:], (1, 3, 2))
     ]
 
     picked = []
@@ -419,7 +431,7 @@
         out_shape=jax.ShapeDtypeStruct((own, width), BF16),
         compiler_params=params(),
         name="collect",
-    )(returned.reshape(slots, width), id_rows, route_weights.T)
+    )(returned, id_rows, route_weights.T)
     return (mix_out, expert_out)
 
 

time: 265 us -> 252 us (0.951)
  waiting for transfers between devices: 143 us -> 127 us
  starting transfers between devices: 23.8 us -> 30.8 us
  local copies, waits for them, and re-layouts: 15.3 us -> 11.6 us
    ppermute x9, waiting for transfers between devices: 42.5 us -> 26.8 us  [move(): return lax.ppermute(x, ('ep', 'tp'), shift(keys, queries, tp_count))]
    ppermute x3, starting transfers between devices: 0.86 us -> 5.92 us  [on_device(): down_twin, *twin = [lax.ppermute(w, 'tp', swap) for w in picked]]
    unnamed x39 -> x38, local copies, waits for them, and re-layouts: 6 us -> 5.71 us
  transfers between devices with their start and end apart: 19 -> 19, of which waited for: 8 -> 10; matrix products, arithmetic and copies ran while one was open for 2% -> 2% of each run, Pallas kernels for 14% -> 15%
where the time goes in v4:
time: 252 us; the launch traced here: 250 us
  waiting for transfers between devices  127 us (50%)
  Pallas kernels  45.9 us (18%)
  starting transfers between devices  30.8 us (12%)
  blocking collectives  18 us (7%)
  between operations  14.3 us (6%)
  local copies, waits for them, and re-layouts  11.6 us (5%)
  other arithmetic  2.64 us (1%)
    reduce_scatter x1, waiting for transfers between devices, on_device(): lax.psum_scatter(terms.reshape(chips * span, width), 'tp', scatter_dimens...  65.3 us
    ppermute x9, waiting for transfers between devices, move(): return lax.ppermute(x, ('ep', 'tp'), shift(keys, queries, tp_count))  26.8 us
    all_to_all x1, waiting for transfers between devices, on_device(): mine = lax.all_to_all(latent, 'tp', 0, 0, axis_index_groups=same_core)  25.7 us
    all_to_all x1, blocking collectives, on_device(): lax.all_to_all(outgoing, ('ep', 'tp'), 0, 0, axis_index_groups=plane)  18 us
    pallas_call x1, Pallas kernels, on_device(): pl.pallas_call(attend_body, out_shape=[jax.ShapeDtypeStruct((rows + 16, L...  17.4 us
    pallas_call x1, Pallas kernels, on_device(): pl.pallas_call(expert_body, out_shape=jax.ShapeDtypeStruct((chips, span,...  11.6 us
    all_to_all x1, waiting for transfers between devices, on_device(): lax.all_to_all(summed.reshape(span // CAP, CAP, width)[:EXPERTS], ('ep',...  8.76 us
    all_to_all x1, starting transfers between devices, on_device(): mine = lax.all_to_all(latent, 'tp', 0, 0, axis_index_groups=same_core)  8.48 us
  transfers between devices with their start and end apart: 19, of which 10 were waited for; matrix products, arithmetic and copies ran while one was open for 2% of the time, Pallas kernels for 15%

profile of v4, /device:TPU:2, one launch (start us, length us, event | category | flops | bytes accessed | tf_op | source)
XLA Modules:
  0.0 249.9 jit_solution(18323901194207810694)
XLA Ops:
  7.2 1.7 latents.1
  9.0 2.2 dispatch.1
  11.2 18.0 %all_to_all.15 = bf16[32,4,2048]{2,1,0:T(4,128)(2,1)S(1)} all-to-all(bf16[32,4,2048]{2,1,0:T(4,128)(2,1)} %dispatch.1), channel_id=1, replica_groups={{0,1,16,17,32,33,48,49,64,65,80,81,96,97,112,113,128,129,144,145,160,16..., dimensions={0} | all-to-all | bytes 1048576 | tf_op jit(solution)/shard_map/all_to_all | solution.py:312
  30.1 8.5 %all-to-all-start = ((bf16[8,288,128]{2,1,0:T(8,128)(2,1)}), bf16[8,288,128]{2,1,0:T(8,128)(2,1)S(1)}, u32[]{:S(2)}, u32[]{:S(2)}) async-start(bf16[8,288,128]{2,1,0:T(8,128)(2,1)} %latents.1), calls=%async_computation | async-start | bytes 1179648 | tf_op jit(solution)/shard_map/all_to_all | solution.py:319
  38.7 25.7 %all-to-all-done.mine_ref = bf16[8,288,128]{2,1,0:T(8,128)(2,1)S(1)} async-done(((bf16[8,288,128]{2,1,0:T(8,128)(2,1)}), bf16[8,288,128]{2,1,0:T(8,128)(2,1)S(1)}, u32[]{:S(2)}, u32[]{:S(2)}) %all-to-all-start) | async-done | bytes 589856 | tf_op jit(solution)/shard_map/all_to_all | solution.py:319
  67.9 5.3 %project.1 = (bf16[1152,128]{1,0:T(8,128)(2,1)}, bf16[1920,128]{1,0:T(8,128)(2,1)}) custom-call(bf16[8,288,128]{2,1,0:T(8,128)(2,1)} %copy-done.3, bf16[8,288,128]{2,1,0:T(8,128)(2,1)} %copy-done.8, bf16[192,384]{1,0:T(8,128)(2,1)} %bitcast.16, bf16[256,128]{1,0:T(8,128)(2,1)} %wk_ref.1, bf16[256,128]{1,0:T(8,128)(2,1)} %wv_ref.1, f32[1,192]{1,0:T(1,128)} %bitcast.20, ...), custom_call_target="tpu_custom_call" | custom-call | tf_op jit(solution)/shard_map/project/pallas_call | solution.py:348
  74.4 3.2 %collective-permute-start.2 = (bf16[1152,128]{1,0:T(8,128)(2,1)S(1)}, bf16[1152,128]{1,0:T(8,128)(2,1)}, u32[]{:S(2)}, u32[]{:S(2)}) collective-permute-start(bf16[1152,128]{1,0:T(8,128)(2,1)S(1)} %copy-done.13), channel_id=1, source_target_pairs={{0,192},{1,49},{2,194},{3,51},{4,196},{5,53},{6,198},{7,55},{8,200... | collective-permute-start | bytes 884744 | tf_op jit(solution)/shard_map/ppermute | solution.py:291
  77.7 2.1 collective-permute-start.5
  79.8 1.6 collective-permute-done.1.refs_1_
  81.4 1.6 collective-permute-start.6
  84.7 4.5 %collective-permute-done.3.refs_3_ = bf16[1152,128]{1,0:T(8,128)(2,1)} collective-permute-done((bf16[1152,128]{1,0:T(8,128)(2,1)S(1)}, bf16[1152,128]{1,0:T(8,128)(2,1)}, u32[]{:S(2)}, u32[]{:S(2)}) %collective-permute-start.3) | collective-permute-done | bytes 294944 | tf_op jit(solution)/shard_map/ppermute | solution.py:291
  89.2 5.9 %collective-permute-start.14 = (bf16[256,2048]{1,0:T(8,128)(2,1)S(1)}, bf16[256,2048]{1,0:T(8,128)(2,1)S(1)}, u32[]{:S(2)}, u32[]{:S(2)}) collective-permute-start(bf16[256,2048]{1,0:T(8,128)(2,1)S(1)} %dynamic-slice_bitcast_fusion), channel_id=1, source_target_pairs={{0,1},{1,0},{2,3},{3,2},{4,5},{5,4},{6,7},{7,6},{8,9},{9,8},{10,11... | collective-permute-start | bytes 3145736 | tf_op jit(solution)/shard_map/ppermute | solution.py:369
  96.7 17.4 %attend.1 = (bf16[784,128]{1,0:T(8,128)(2,1)}, bf16[784,128]{1,0:T(8,128)(2,1)}, bf16[784,128]{1,0:T(8,128)(2,1)}, bf16[784,128]{1,0:T(8,128)(2,1)}) custom-call(bf16[1152,128]{1,0:T(8,128)(2,1)} %get-tuple-element.13.refs_0_, bf16[1152,128]{1,0:T(8,128)(2,1)} %copy-done.14, bf16[1152,128]{1,0:T(8,128)(2,1)} %collective-permute-done.2.refs_2_, ...), custom_call_target="tpu_custom_call" | custom-call | tf_op jit(solution)/shard_map/attend/pallas_call | solution.py:354
  115.8 4.2 %collective-permute-done.7.refs_1_ = bf16[784,128]{1,0:T(8,128)(2,1)S(1)} collective-permute-done((bf16[784,128]{1,0:T(8,128)(2,1)}, bf16[784,128]{1,0:T(8,128)(2,1)S(1)}, u32[]{:S(2)}, u32[]{:S(2)}) %collective-permute-start.7) | collective-permute-done | bytes 200736 | tf_op jit(solution)/shard_map/ppermute | solution.py:291
  120.2 6.9 %collective-permute-done.8.refs_2_ = bf16[784,128]{1,0:T(8,128)(2,1)S(1)} collective-permute-done((bf16[784,128]{1,0:T(8,128)(2,1)}, bf16[784,128]{1,0:T(8,128)(2,1)S(1)}, u32[]{:S(2)}, u32[]{:S(2)}) %collective-permute-start.8) | collective-permute-done | bytes 200736 | tf_op jit(solution)/shard_map/ppermute | solution.py:291
  127.1 7.4 %collective-permute-done.9.refs_3_ = bf16[784,128]{1,0:T(8,128)(2,1)S(1)} collective-permute-done((bf16[784,128]{1,0:T(8,128)(2,1)}, bf16[784,128]{1,0:T(8,128)(2,1)S(1)}, u32[]{:S(2)}, u32[]{:S(2)}) %collective-permute-start.9) | collective-permute-done | bytes 200736 | tf_op jit(solution)/shard_map/ppermute | solution.py:291
  135.2 2.0 join.1
  139.1 11.6 %experts.1._ = bf16[8,176,2048]{2,1,0:T(8,128)(2,1)} custom-call(s32[1]{0:T(128)} %bitcast.4.core_ref, bf16[8,128,2048]{2,1,0:T(8,128)(2,1)} %all-gather.2.cloned.1.call-done.x_ref, bf16[2,2048,256]{2,1,0:T(8,128)(2,1)} %refs_0_.1, bf16[2,2048,256]{2,1,0:T(8,128)(2,1)} %refs_1_.1, bf16[2,256,2048]{2,1,0:T(8,128)(2,1)} %refs_2_.1, ...), custom_call_target="tpu_custom_call" | custom-call | tf_op jit(solution)/shard_map/experts/pallas_call | solution.py:375
  151.3 3.3 %mix.1 = bf16[8,176,2048]{2,1,0:T(8,128)(2,1)} custom-call(bf16[384,128]{1,0:T(8,128)(2,1)} %get-tuple-element.19.own_ref, bf16[384,128]{1,0:T(8,128)(2,1)} %copy-done.18, bf16[128,2048]{1,0:T(8,128)(2,1)} %w_own_ref.1, bf16[128,2048]{1,0:T(8,128)(2,1)} %collective-permute-done.11.w_twin_ref, ...), custom_call_target="tpu_custom_call", output_to_operand_aliasing={{}: (4, {})} | custom-call | tf_op jit(solution)/shard_map/mix/pallas_call | solution.py:403
  154.7 65.3 %reduce-scatter.2.cloned.1.call-done = bf16[176,2048]{1,0:T(8,128)(2,1)} async-done(((bf16[1408,2048]{1,0:T(8,128)(2,1)}), bf16[176,2048]{1,0:T(8,128)(2,1)}) %reduce-scatter.2.cloned.1.call-update) | async-done | bytes 720912 | tf_op jit(solution)/shard_map/reduce_scatter | solution.py:418
  222.1 7.4 %all-to-all-start.2 = ((bf16[32,4,2048]{2,1,0:T(4,128)(2,1)}), bf16[32,4,2048]{2,1,0:T(4,128)(2,1)S(1)}, u32[]{:S(2)}, u32[]{:S(2)}) async-start(bf16[32,4,2048]{2,1,0:T(4,128)(2,1)} %slice.11), calls=%async_computation.3 | async-start | bytes 1048576 | tf_op jit(solution)/shard_map/all_to_all | solution.py:426
  229.5 1.6 slice.12
  231.1 8.8 %all-to-all-done.2.back_ref = bf16[32,4,2048]{2,1,0:T(4,128)(2,1)S(1)} async-done(((bf16[32,4,2048]{2,1,0:T(4,128)(2,1)}), bf16[32,4,2048]{2,1,0:T(4,128)(2,1)S(1)}, u32[]{:S(2)}, u32[]{:S(2)}) %all-to-all-start.2) | async-done | bytes 524320 | tf_op jit(solution)/shard_map/all_to_all | solution.py:426
  240.7 2.4 collect.1
  (74 shorter events, 16.9 us)
Async XLA Ops:
  7.2 130.2 %all-gather.2.cloned.1.call-start = ((), (), s32[]{:S(2)}) async-start(), calls=%async_computation.4 | async-start | bytes 4718592 | tf_op jit(solution)/shard_map/all_gather | solution.py:315
  30.1 34.3 %all-to-all-start = ((bf16[8,288,128]{2,1,0:T(8,128)(2,1)}), bf16[8,288,128]{2,1,0:T(8,128)(2,1)S(1)}, u32[]{:S(2)}, u32[]{:S(2)}) async-start(bf16[8,288,128]{2,1,0:T(8,128)(2,1)} %latents.1), calls=%async_computation | async-start | bytes 1179648 | tf_op jit(solution)/shard_map/all_to_all | solution.py:319
  38.6 181.4 %reduce-scatter.2.cloned.1.call-start = ((), (), s32[]{:S(2)}) async-start(), calls=%async_computation.5 | async-start | bytes 6488064 | tf_op jit(solution)/shard_map/reduce_scatter | solution.py:418
  64.4 2.7 %collective-permute-start = (bf16[8,288,128]{2,1,0:T(8,128)(2,1)S(1)}, bf16[8,288,128]{2,1,0:T(8,128)(2,1)S(1)}, u32[]{:S(2)}, u32[]{:S(2)}) collective-permute-start(bf16[8,288,128]{2,1,0:T(8,128)(2,1)S(1)} %all-to-all-done.mine_ref), channel_id=1, source_target_pairs={{0,1},{1,0},{2,3},{3,2},{4,5},{5,4},{6,7},{7,6},{8,9},{9,8},{10,11... | collective-permute-start | bytes 1769480 | tf_op jit(solution)/shard_map/ppermute | solution.py:320
  65.9 7.4 %copy-start = (bf16[2,2048,256]{2,1,0:T(8,128)(2,1)S(1)}, bf16[2,2048,256]{2,1,0:T(8,128)(2,1)}, u32[]{:S(2)}) copy-start(bf16[2,2048,256]{2,1,0:T(8,128)(2,1)} %refs_0_.1) | copy-start | bytes 6291460
  67.9 9.7 %copy-start.1 = (bf16[2,2048,256]{2,1,0:T(8,128)(2,1)S(1)}, bf16[2,2048,256]{2,1,0:T(8,128)(2,1)}, u32[]{:S(2)}) copy-start(bf16[2,2048,256]{2,1,0:T(8,128)(2,1)} %refs_1_.1) | copy-start | bytes 6291460
  73.2 9.9 %copy-start.2 = (bf16[2,256,2048]{2,1,0:T(8,128)(2,1)S(1)}, bf16[2,256,2048]{2,1,0:T(8,128)(2,1)}, u32[]{:S(2)}) copy-start(bf16[2,256,2048]{2,1,0:T(8,128)(2,1)} %refs_2_.1) | copy-start | bytes 6291460
  73.2 8.2 %collective-permute-start.1 = (bf16[1152,128]{1,0:T(8,128)(2,1)}, bf16[1152,128]{1,0:T(8,128)(2,1)S(1)}, u32[]{:S(2)}, u32[]{:S(2)}) collective-permute-start(bf16[1152,128]{1,0:T(8,128)(2,1)} %get-tuple-element.13.refs_0_), channel_id=1, source_target_pairs={{0,64},{1,17},{2,66},{3,19},{4,68},{5,21},{6,70},{7,23},{8,72},{9,... | collective-permute-start | bytes 884744 | tf_op jit(solution)/shard_map/ppermute | solution.py:291
  74.4 10.3 %collective-permute-start.2 = (bf16[1152,128]{1,0:T(8,128)(2,1)S(1)}, bf16[1152,128]{1,0:T(8,128)(2,1)}, u32[]{:S(2)}, u32[]{:S(2)}) collective-permute-start(bf16[1152,128]{1,0:T(8,128)(2,1)S(1)} %copy-done.13), channel_id=1, source_target_pairs={{0,192},{1,49},{2,194},{3,51},{4,196},{5,53},{6,198},{7,55},{8,200... | collective-permute-start | bytes 884744 | tf_op jit(solution)/shard_map/ppermute | solution.py:291
  77.6 11.6 %collective-permute-start.3 = (bf16[1152,128]{1,0:T(8,128)(2,1)S(1)}, bf16[1152,128]{1,0:T(8,128)(2,1)}, u32[]{:S(2)}, u32[]{:S(2)}) collective-permute-start(bf16[1152,128]{1,0:T(8,128)(2,1)S(1)} %copy-done.13), channel_id=1, source_target_pairs={{0,128},{1,33},{2,130},{3,35},{4,132},{5,37},{6,134},{7,39},{8,136... | collective-permute-start | bytes 884744 | tf_op jit(solution)/shard_map/ppermute | solution.py:291
  77.6 11.6 %collective-permute-start.4 = (bf16[1920,128]{1,0:T(8,128)(2,1)S(1)}, bf16[1920,128]{1,0:T(8,128)(2,1)S(1)}, u32[]{:S(2)}, u32[]{:S(2)}) collective-permute-start(bf16[1920,128]{1,0:T(8,128)(2,1)S(1)} %copy-done.9), channel_id=1, source_target_pairs={{0,16},{1,65},{2,18},{3,67},{4,20},{5,69},{6,22},{7,71},{8,24},{9,... | collective-permute-start | bytes 1474568 | tf_op jit(solution)/shard_map/ppermute | solution.py:291
  77.7 17.4 %collective-permute-start.5 = (bf16[1920,128]{1,0:T(8,128)(2,1)S(1)}, bf16[1920,128]{1,0:T(8,128)(2,1)S(1)}, u32[]{:S(2)}, u32[]{:S(2)}) collective-permute-start(bf16[1920,128]{1,0:T(8,128)(2,1)S(1)} %copy-done.9), channel_id=1, source_target_pairs={{0,48},{1,193},{2,50},{3,195},{4,52},{5,197},{6,54},{7,199},{8,56}... | collective-permute-start | bytes 1474568 | tf_op jit(solution)/shard_map/ppermute | solution.py:291
  81.4 14.3 %collective-permute-start.6 = (bf16[1920,128]{1,0:T(8,128)(2,1)S(1)}, bf16[1920,128]{1,0:T(8,128)(2,1)S(1)}, u32[]{:S(2)}, u32[]{:S(2)}) collective-permute-start(bf16[1920,128]{1,0:T(8,128)(2,1)S(1)} %copy-done.9), channel_id=1, source_target_pairs={{0,32},{1,129},{2,34},{3,131},{4,36},{5,133},{6,38},{7,135},{8,40}... | collective-permute-start | bytes 1474568 | tf_op jit(solution)/shard_map/ppermute | solution.py:291
  84.7 52.6 %collective-permute-start.12 = (bf16[2048,256]{1,0:T(8,128)(2,1)}, bf16[2048,256]{1,0:T(8,128)(2,1)S(1)}, u32[]{:S(2)}, u32[]{:S(2)}) collective-permute-start(bf16[2048,256]{1,0:T(8,128)(2,1)} %dynamic-slice_bitcast_fusion.2), channel_id=1, source_target_pairs={{0,1},{1,0},{2,3},{3,2},{4,5},{5,4},{6,7},{7,6},{8,9},{9,8},{10,11... | collective-permute-start | bytes 3145736 | tf_op jit(solution)/shard_map/ppermute | solution.py:369
  89.2 48.1 %collective-permute-start.13 = (bf16[2048,256]{1,0:T(8,128)(2,1)S(1)}, bf16[2048,256]{1,0:T(8,128)(2,1)S(1)}, u32[]{:S(2)}, u32[]{:S(2)}) collective-permute-start(bf16[2048,256]{1,0:T(8,128)(2,1)S(1)} %dynamic-slice_bitcast_fusion.1), channel_id=1, source_target_pairs={{0,1},{1,0},{2,3},{3,2},{4,5},{5,4},{6,7},{7,6},{8,9},{9,8},{10,11... | collective-permute-start | bytes 3145736 | tf_op jit(solution)/shard_map/ppermute | solution.py:369
  89.2 48.1 %collective-permute-start.14 = (bf16[256,2048]{1,0:T(8,128)(2,1)S(1)}, bf16[256,2048]{1,0:T(8,128)(2,1)S(1)}, u32[]{:S(2)}, u32[]{:S(2)}) collective-permute-start(bf16[256,2048]{1,0:T(8,128)(2,1)S(1)} %dynamic-slice_bitcast_fusion), channel_id=1, source_target_pairs={{0,1},{1,0},{2,3},{3,2},{4,5},{5,4},{6,7},{7,6},{8,9},{9,8},{10,11... | collective-permute-start | bytes 3145736 | tf_op jit(solution)/shard_map/ppermute | solution.py:369
  114.1 5.9 %collective-permute-start.7 = (bf16[784,128]{1,0:T(8,128)(2,1)}, bf16[784,128]{1,0:T(8,128)(2,1)S(1)}, u32[]{:S(2)}, u32[]{:S(2)}) collective-permute-start(bf16[784,128]{1,0:T(8,128)(2,1)} %get-tuple-element.16), channel_id=1, source_target_pairs={{0,192},{1,49},{2,194},{3,51},{4,196},{5,53},{6,198},{7,55},{8,200... | collective-permute-start | bytes 602120 | tf_op jit(solution)/shard_map/ppermute | solution.py:291
  114.4 36.3 %collective-permute-start.11 = (bf16[128,2048]{1,0:T(8,128)(2,1)}, bf16[128,2048]{1,0:T(8,128)(2,1)}, u32[]{:S(2)}, u32[]{:S(2)}) collective-permute-start(bf16[128,2048]{1,0:T(8,128)(2,1)} %w_own_ref.1), channel_id=1, source_target_pairs={{0,1},{1,0},{2,3},{3,2},{4,5},{5,4},{6,7},{7,6},{8,9},{9,8},{10,11... | collective-permute-start | bytes 1572872 | tf_op jit(solution)/shard_map/ppermute | solution.py:370
  120.0 14.6 %copy-start.15 = (bf16[784,128]{1,0:T(8,128)(2,1)}, bf16[784,128]{1,0:T(8,128)(2,1)S(1)}, u32[]{:S(2)}) copy-start(bf16[784,128]{1,0:T(8,128)(2,1)S(1)} %collective-permute-done.7.refs_1_) | copy-start | bytes 602116
  120.0 7.1 %collective-permute-start.8 = (bf16[784,128]{1,0:T(8,128)(2,1)}, bf16[784,128]{1,0:T(8,128)(2,1)S(1)}, u32[]{:S(2)}, u32[]{:S(2)}) collective-permute-start(bf16[784,128]{1,0:T(8,128)(2,1)} %get-tuple-element.17), channel_id=1, source_target_pairs={{0,64},{1,17},{2,66},{3,19},{4,68},{5,21},{6,70},{7,23},{8,72},{9,... | collective-permute-start | bytes 602120 | tf_op jit(solution)/shard_map/ppermute | solution.py:291
  127.1 7.4 %copy-start.16 = (bf16[784,128]{1,0:T(8,128)(2,1)}, bf16[784,128]{1,0:T(8,128)(2,1)S(1)}, u32[]{:S(2)}) copy-start(bf16[784,128]{1,0:T(8,128)(2,1)S(1)} %collective-permute-done.8.refs_2_) | copy-start | bytes 602116
  127.1 7.4 %collective-permute-start.9 = (bf16[784,128]{1,0:T(8,128)(2,1)}, bf16[784,128]{1,0:T(8,128)(2,1)S(1)}, u32[]{:S(2)}, u32[]{:S(2)}) collective-permute-start(bf16[784,128]{1,0:T(8,128)(2,1)} %get-tuple-element.18), channel_id=1, source_target_pairs={{0,128},{1,33},{2,130},{3,35},{4,132},{5,37},{6,134},{7,39},{8,136... | collective-permute-start | bytes 602120 | tf_op jit(solution)/shard_map/ppermute | solution.py:291
  137.3 13.4 %collective-permute-start.10 = (bf16[384,128]{1,0:T(8,128)(2,1)}, bf16[384,128]{1,0:T(8,128)(2,1)S(1)}, u32[]{:S(2)}, u32[]{:S(2)}) collective-permute-start(bf16[384,128]{1,0:T(8,128)(2,1)} %get-tuple-element.20), channel_id=1, source_target_pairs={{0,1},{1,0},{2,3},{3,2},{4,5},{5,4},{6,7},{7,6},{8,9},{9,8},{10,11... | collective-permute-start | bytes 294920 | tf_op jit(solution)/shard_map/ppermute | solution.py:402
  222.1 17.8 %all-to-all-start.2 = ((bf16[32,4,2048]{2,1,0:T(4,128)(2,1)}), bf16[32,4,2048]{2,1,0:T(4,128)(2,1)S(1)}, u32[]{:S(2)}, u32[]{:S(2)}) async-start(bf16[32,4,2048]{2,1,0:T(4,128)(2,1)} %slice.11), calls=%async_computation.3 | async-start | bytes 1048576 | tf_op jit(solution)/shard_map/all_to_all | solution.py:426
  (14 other events, 24.5 us)
Sparse Core Ops, SparseCore 0:
  30.3 65.0 all-gather.1
  154.8 65.1 reduce-scatter.1

commit v5 on v4

--- a/solution.py
+++ b/solution.py
@@ -204,26 +204,10 @@
         outs[j * LANES // half][at : at + LANES, :] = (head * scale).astype(BF16)
 
 
-def mix_body(own_ref, twin_ref, w_own_ref, w_twin_ref, _, out_ref, term_ref, sems):
-    owners, span, _ = out_ref.shape
-    each = own_ref.shape[0] // owners
-    step = owners // 2
-    copies = []
-    for c in range(2):
-        there = slice(c * step * each, (c + 1) * step * each)
-        term = jnp.dot(own_ref[there, :], w_own_ref[...], preferred_element_type=F32)
-        term += jnp.dot(twin_ref[there, :], w_twin_ref[...], preferred_element_type=F32)
-        term_ref[there, :] = term.astype(BF16)
-        for i in range(c * step, (c + 1) * step):
-            copy = pltpu.make_async_copy(
-                term_ref.at[pl.ds(i * each, each), :],
-                out_ref.at[i, pl.ds(span - each, each), :],
-                sems.at[i],
-            )
-            copy.start()
-            copies.append(copy)
-    for copy in copies:
-        copy.wait()
+def mix_body(own_ref, twin_ref, w_own_ref, w_twin_ref, out_ref):
+    term = jnp.dot(own_ref[...], w_own_ref[...], preferred_element_type=F32)
+    term += jnp.dot(twin_ref[...], w_twin_ref[...], preferred_element_type=F32)
+    out_ref[...] = term.astype(BF16)
 
 
 def expert_body(core_ref, x_ref, *refs):
@@ -292,14 +276,14 @@
 
 
     height = own * ((q_latent.shape[1] + kv_latent.shape[1]) // LANES + 1)
-    latent = pl.pallas_call(
+    latents = pl.pallas_call(
         latent_body,
         out_shape=jax.ShapeDtypeStruct((chips, height, LANES), BF16),
         compiler_params=params(),
         name="latents",
-    )(q_latent, kv_latent, rope_key, q_latent_gain, kv_latent_gain[None])
-
-    latent, tokens_b = lax.optimization_barrier((latent, tokens_b))
+    )
+    latent = latents(q_latent, kv_latent, rope_key, q_latent_gain, kv_latent_gain[None])
+
     id_rows = expert_ids.T
     dispatch = pl.pallas_call(
         dispatch_body,
@@ -369,12 +353,11 @@
     down_twin, *twin = [lax.ppermute(w, "tp", swap) for w in picked]
     mix_twin = lax.ppermute(w_mix, "tp", swap)
 
-    span = slots + own
     step = chips // 2
     hidden = w_gate.shape[2]
     terms = pl.pallas_call(
         expert_body,
-        out_shape=jax.ShapeDtypeStruct((chips, span, width), BF16),
+        out_shape=jax.ShapeDtypeStruct((chips, slots, width), BF16),
         grid_spec=pltpu.PrefetchScalarGridSpec(
             num_scalar_prefetch=1,
             grid=(chips // step,),
@@ -400,31 +383,26 @@
         name="join",
     )(*parts)
     twin_head = lax.ppermute(twin_head, "tp", swap)
-    terms = pl.pallas_call(
+    mixed = pl.pallas_call(
         mix_body,
-        out_shape=jax.ShapeDtypeStruct((chips, span, width), BF16),
-        in_specs=[pl.BlockSpec(memory_space=pltpu.VMEM)] * 4
-        + [pl.BlockSpec(memory_space=pl.ANY)],
-        out_specs=pl.BlockSpec(memory_space=pl.ANY),
-        scratch_shapes=[
-            pltpu.VMEM((half, width), BF16),
-            pltpu.SemaphoreType.DMA((chips,)),
-        ],
-        input_output_aliases={4: 0},
+        out_shape=jax.ShapeDtypeStruct((half, width), BF16),
+        grid=(2,),
+        in_specs=[pl.BlockSpec((half // 2, VALUE_DIM), lambda i: (i, 0))] * 2
+        + [pl.BlockSpec((VALUE_DIM, width), lambda i: (0, 0))] * 2,
+        out_specs=pl.BlockSpec((half // 2, width), lambda i: (i, 0)),
         compiler_params=params(),
         name="mix",
-    )(own_head, twin_head, w_mix, mix_twin, terms)
-
-    summed = lax.psum_scatter(
-        terms.reshape(chips * span, width),
-        "tp",
-        scatter_dimension=0,
-        tiled=True,
-        axis_index_groups=same_core,
-    )
-    mix_out = summed[slots:]
+    )(own_head, twin_head, w_mix, mix_twin)
+
+    def summed(x):
+        return lax.psum_scatter(
+            x, "tp", scatter_dimension=0, tiled=True, axis_index_groups=same_core
+        )
+
+    done = summed(terms.reshape(chips * slots, width))
+    mix_out = summed(mixed)
     returned = lax.all_to_all(
-        summed.reshape(span // CAP, CAP, width)[:EXPERTS], ("ep", "tp"), 0, 0, axis_index_groups=plane
+        done.reshape(EXPERTS, CAP, width), ("ep", "tp"), 0, 0, axis_index_groups=plane
     )
     expert_out = pl.pallas_call(
         collect_body,

time: 252 us -> 237 us (0.940)
  blocking collectives: 18 us -> 34.1 us
  waiting for transfers between devices: 127 us -> 114 us
  starting transfers between devices: 30.8 us -> 19.3 us
  local copies, waits for them, and re-layouts: 11.6 us -> 6.6 us
    reduce_scatter x1 -> x2, waiting for transfers between devices: 65.3 us -> 16.3 us  [summed(): lax.psum_scatter(x, 'tp', scatter_dimension=0, tiled=True, axis_index_gro...]
    all_gather x1, waiting for transfers between devices: 0.02 us -> 49.1 us  [on_device(): lax.all_gather(arrived.reshape(slots, width), 'tp', axis=0, axis_index_gr...]
    all_to_all x0 -> x1, blocking collectives: none -> 16.2 us  [on_device(): lax.all_to_all(done.reshape(EXPERTS, CAP, width), ('ep', 'tp'), 0, 0, axi...]
    all_to_all x1 -> x0, waiting for transfers between devices: 8.76 us -> none  [on_device(): lax.all_to_all(summed.reshape(span // CAP, CAP, width)[:EXPERTS], ('ep',...]
    all_to_all x1 -> x0, starting transfers between devices: 7.39 us -> none  [on_device(): lax.all_to_all(summed.reshape(span // CAP, CAP, width)[:EXPERTS], ('ep',...]
    ppermute x9, waiting for transfers between devices: 26.8 us -> 20.5 us  [move(): return lax.ppermute(x, ('ep', 'tp'), shift(keys, queries, tp_count))]
    ppermute x9, starting transfers between devices: 7.61 us -> 13.2 us  [move(): return lax.ppermute(x, ('ep', 'tp'), shift(keys, queries, tp_count))]
    ppermute x3, starting transfers between devices: 5.92 us -> 1.62 us  [on_device(): down_twin, *twin = [lax.ppermute(w, 'tp', swap) for w in picked]]
  transfers between devices with their start and end apart: 19 -> 19, of which waited for: 10 -> 12; matrix products, arithmetic and copies ran while one was open for 2% -> 2% of each run, Pallas kernels for 15% -> 14%
where the time goes in v5:
time: 237 us; the launch traced here: 236 us
  waiting for transfers between devices  114 us (48%)
  Pallas kernels  46.1 us (19%)
  blocking collectives  34.1 us (14%)
  starting transfers between devices  19.3 us (8%)
  between operations  13.9 us (6%)
  local copies, waits for them, and re-layouts  6.6 us (3%)
  other arithmetic  2.64 us (1%)
    all_gather x1, waiting for transfers between devices, on_device(): lax.all_gather(arrived.reshape(slots, width), 'tp', axis=0, axis_index_gr...  49.1 us
    all_to_all x1, waiting for transfers between devices, on_device(): mine = lax.all_to_all(latent, 'tp', 0, 0, axis_index_groups=same_core)  23.1 us
    ppermute x9, waiting for transfers between devices, move(): return lax.ppermute(x, ('ep', 'tp'), shift(keys, queries, tp_count))  20.5 us
    all_to_all x1, blocking collectives, on_device(): lax.all_to_all(outgoing, ('ep', 'tp'), 0, 0, axis_index_groups=plane)  18 us
    pallas_call x1, Pallas kernels, on_device(): pl.pallas_call(attend_body, out_shape=[jax.ShapeDtypeStruct((rows + 16, L...  17.4 us
    reduce_scatter x2, waiting for transfers between devices, summed(): lax.psum_scatter(x, 'tp', scatter_dimension=0, tiled=True, axis_index_gro...  16.3 us
    all_to_all x1, blocking collectives, on_device(): lax.all_to_all(done.reshape(EXPERTS, CAP, width), ('ep', 'tp'), 0, 0, axi...  16.2 us
    ppermute x9, starting transfers between devices, move(): return lax.ppermute(x, ('ep', 'tp'), shift(keys, queries, tp_count))  13.2 us
  transfers between devices with their start and end apart: 19, of which 12 were waited for; matrix products, arithmetic and copies ran while one was open for 2% of the time, Pallas kernels for 14%

profile of v5, /device:TPU:2, one launch (start us, length us, event | category | flops | bytes accessed | tf_op | source)
XLA Modules:
  0.0 236.4 jit_solution(2513269174447328310)
XLA Ops:
  7.2 2.3 dispatch.1
  9.6 18.0 %all_to_all.15 = bf16[32,4,2048]{2,1,0:T(4,128)(2,1)S(1)} all-to-all(bf16[32,4,2048]{2,1,0:T(4,128)(2,1)} %dispatch.1), channel_id=1, replica_groups={{0,1,16,17,32,33,48,49,64,65,80,81,96,97,112,113,128,129,144,145,160,16..., dimensions={0} | all-to-all | bytes 1048576 | tf_op jit(solution)/shard_map/all_to_all | solution.py:296
  31.5 1.6 collective-permute-done.13.refs_4_
  34.6 49.1 %all-gather.2.cloned.1.call-done.x_ref = bf16[8,128,2048]{2,1,0:T(8,128)(2,1)} async-done(((bf16[1,128,2048]{2,1,0:T(8,128)(2,1)}), bf16[8,128,2048]{2,1,0:T(8,128)(2,1)}) %all-gather.2.cloned.1.call-update) | async-done | bytes 4194320 | tf_op jit(solution)/shard_map/all_gather | solution.py:299
  83.6 11.7 %experts.1 = bf16[8,128,2048]{2,1,0:T(8,128)(2,1)} custom-call(s32[1]{0:T(128)} %bitcast.4.core_ref, bf16[8,128,2048]{2,1,0:T(8,128)(2,1)} %all-gather.2.cloned.1.call-done.x_ref, bf16[2,2048,256]{2,1,0:T(8,128)(2,1)} %refs_0_.1, bf16[2,2048,256]{2,1,0:T(8,128)(2,1)} %refs_1_.1, bf16[2,256,2048]{2,1,0:T(8,128)(2,1)} %refs_2_.1, bf16[2048,256]{1,0:T(8,128)(2,1)} %copy-done.4, ...), custom_call_target="tpu_custom_call" | custom-call | tf_op jit(solution)/shard_map/experts/pallas_call | solution.py:358
  95.4 1.8 latents.1
  97.2 4.3 %all-to-all-start = ((bf16[8,288,128]{2,1,0:T(8,128)(2,1)}), bf16[8,288,128]{2,1,0:T(8,128)(2,1)S(1)}, u32[]{:S(2)}, u32[]{:S(2)}) async-start(bf16[8,288,128]{2,1,0:T(8,128)(2,1)} %latents.1), calls=%async_computation | async-start | bytes 1179648 | tf_op jit(solution)/shard_map/all_to_all | solution.py:303
  101.5 23.1 %all-to-all-done.mine_ref = bf16[8,288,128]{2,1,0:T(8,128)(2,1)S(1)} async-done(((bf16[8,288,128]{2,1,0:T(8,128)(2,1)}), bf16[8,288,128]{2,1,0:T(8,128)(2,1)S(1)}, u32[]{:S(2)}, u32[]{:S(2)}) %all-to-all-start) | async-done | bytes 589856 | tf_op jit(solution)/shard_map/all_to_all | solution.py:303
  128.2 5.1 %project.1 = (bf16[1152,128]{1,0:T(8,128)(2,1)}, bf16[1920,128]{1,0:T(8,128)(2,1)}) custom-call(bf16[8,288,128]{2,1,0:T(8,128)(2,1)} %copy-done.3, bf16[8,288,128]{2,1,0:T(8,128)(2,1)} %copy-done.7, bf16[192,384]{1,0:T(8,128)(2,1)} %bitcast.16, bf16[256,128]{1,0:T(8,128)(2,1)} %wk_ref.1, bf16[256,128]{1,0:T(8,128)(2,1)} %wv_ref.1, f32[1,192]{1,0:T(1,128)} %bitcast.20, ...), custom_call_target="tpu_custom_call" | custom-call | tf_op jit(solution)/shard_map/project/pallas_call | solution.py:332
  134.8 1.8 collective-permute-start.2
  138.6 2.1 collective-permute-start.6
  140.7 3.0 %collective-permute-done.1.refs_1_ = bf16[1152,128]{1,0:T(8,128)(2,1)S(1)} collective-permute-done((bf16[1152,128]{1,0:T(8,128)(2,1)}, bf16[1152,128]{1,0:T(8,128)(2,1)S(1)}, u32[]{:S(2)}, u32[]{:S(2)}) %collective-permute-start.1) | collective-permute-done | bytes 294944 | tf_op jit(solution)/shard_map/ppermute | solution.py:275
  143.6 1.8 collective-permute-start.3
  145.5 9.7 %collective-permute-done.3.refs_3_ = bf16[1152,128]{1,0:T(8,128)(2,1)S(1)} collective-permute-done((bf16[1152,128]{1,0:T(8,128)(2,1)}, bf16[1152,128]{1,0:T(8,128)(2,1)S(1)}, u32[]{:S(2)}, u32[]{:S(2)}) %collective-permute-start.3) | collective-permute-done | bytes 294944 | tf_op jit(solution)/shard_map/ppermute | solution.py:275
  157.1 17.4 %attend.1 = (bf16[784,128]{1,0:T(8,128)(2,1)}, bf16[784,128]{1,0:T(8,128)(2,1)}, bf16[784,128]{1,0:T(8,128)(2,1)}, bf16[784,128]{1,0:T(8,128)(2,1)}) custom-call(bf16[1152,128]{1,0:T(8,128)(2,1)} %get-tuple-element.10.refs_0_, bf16[1152,128]{1,0:T(8,128)(2,1)} %copy-done.13, bf16[1152,128]{1,0:T(8,128)(2,1)} %copy-done.14, bf16[1152,128]{1,0:T(8,128)(2,1)} %copy-done.15, ...), custom_call_target="tpu_custom_call" | custom-call | tf_op jit(solution)/shard_map/attend/pallas_call | solution.py:338
  174.5 1.7 collective-permute-start.7
  176.5 2.0 collective-permute-start.9
  178.5 1.9 collective-permute-done.7.refs_1_
  180.4 5.1 %collective-permute-done.8.refs_2_ = bf16[784,128]{1,0:T(8,128)(2,1)S(1)} collective-permute-done((bf16[784,128]{1,0:T(8,128)(2,1)}, bf16[784,128]{1,0:T(8,128)(2,1)S(1)}, u32[]{:S(2)}, u32[]{:S(2)}) %collective-permute-start.8) | collective-permute-done | bytes 200736 | tf_op jit(solution)/shard_map/ppermute | solution.py:275
  186.3 2.0 join.1
  190.5 3.3 %mix.1 = bf16[384,2048]{1,0:T(8,128)(2,1)} custom-call(bf16[384,128]{1,0:T(8,128)(2,1)} %get-tuple-element.16.own_ref, bf16[384,128]{1,0:T(8,128)(2,1)} %copy-done.19, bf16[128,2048]{1,0:T(8,128)(2,1)} %w_own_ref.1, bf16[128,2048]{1,0:T(8,128)(2,1)} %copy-done.9), custom_call_target="tpu_custom_call" | custom-call | tf_op jit(solution)/shard_map/mix/pallas_call | solution.py:386
  195.1 16.2 %all_to_all.16.back_ref = bf16[32,4,2048]{2,1,0:T(4,128)(2,1)} all-to-all(bf16[32,4,2048]{2,1,0:T(4,128)(2,1)S(1)} %reshape.59), channel_id=1, replica_groups={{0,1,16,17,32,33,48,49,64,65,80,81,96,97,112,113,128,129,144,145,160,16..., dimensions={0} | all-to-all | bytes 1048576 | tf_op jit(solution)/shard_map/all_to_all | solution.py:404
  211.2 2.4 collect.1
  213.6 16.3 %reduce-scatter.3.cloned.1.call-done = bf16[48,2048]{1,0:T(8,128)(2,1)} async-done(((bf16[384,2048]{1,0:T(8,128)(2,1)}), bf16[48,2048]{1,0:T(8,128)(2,1)}) %reduce-scatter.3.cloned.1.call-update) | async-done | bytes 196624 | tf_op jit(solution)/shard_map/reduce_scatter | solution.py:398
  (76 shorter events, 18.9 us)
Async XLA Ops:
  7.2 21.4 %copy-start = (bf16[2,2048,256]{2,1,0:T(8,128)(2,1)S(1)}, bf16[2,2048,256]{2,1,0:T(8,128)(2,1)}, u32[]{:S(2)}) copy-start(bf16[2,2048,256]{2,1,0:T(8,128)(2,1)} %refs_0_.1) | copy-start | bytes 6291460
  7.2 76.5 %all-gather.2.cloned.1.call-start = ((), (), s32[]{:S(2)}) async-start(), calls=%async_computation.6 | async-start | bytes 4718592 | tf_op jit(solution)/shard_map/all_gather | solution.py:299
  28.5 165.3 %reduce-scatter.5.cloned.1.call-start = ((), (), s32[]{:S(2)}) async-start(), calls=%async_computation.7 | async-start | bytes 4718592 | tf_op jit(solution)/shard_map/reduce_scatter | solution.py:398
  28.7 2.8 %collective-permute-start.12 = (bf16[2048,256]{1,0:T(8,128)(2,1)S(1)}, bf16[2048,256]{1,0:T(8,128)(2,1)S(1)}, u32[]{:S(2)}, u32[]{:S(2)}) collective-permute-start(bf16[2048,256]{1,0:T(8,128)(2,1)S(1)} %dynamic-slice_bitcast_fusion.2), channel_id=1, source_target_pairs={{0,1},{1,0},{2,3},{3,2},{4,5},{5,4},{6,7},{7,6},{8,9},{9,8},{10,11... | collective-permute-start | bytes 3145736 | tf_op jit(solution)/shard_map/ppermute | solution.py:353
  30.2 2.8 %collective-permute-start.13 = (bf16[2048,256]{1,0:T(8,128)(2,1)S(1)}, bf16[2048,256]{1,0:T(8,128)(2,1)S(1)}, u32[]{:S(2)}, u32[]{:S(2)}) collective-permute-start(bf16[2048,256]{1,0:T(8,128)(2,1)S(1)} %dynamic-slice_bitcast_fusion.1), channel_id=1, source_target_pairs={{0,1},{1,0},{2,3},{3,2},{4,5},{5,4},{6,7},{7,6},{8,9},{9,8},{10,11... | collective-permute-start | bytes 3145736 | tf_op jit(solution)/shard_map/ppermute | solution.py:353
  30.9 3.7 %collective-permute-start.14 = (bf16[256,2048]{1,0:T(8,128)(2,1)S(1)}, bf16[256,2048]{1,0:T(8,128)(2,1)S(1)}, u32[]{:S(2)}, u32[]{:S(2)}) collective-permute-start(bf16[256,2048]{1,0:T(8,128)(2,1)S(1)} %dynamic-slice_bitcast_fusion), channel_id=1, source_target_pairs={{0,1},{1,0},{2,3},{3,2},{4,5},{5,4},{6,7},{7,6},{8,9},{9,8},{10,11... | collective-permute-start | bytes 3145736 | tf_op jit(solution)/shard_map/ppermute | solution.py:353
  31.5 52.1 %copy-start.4 = (bf16[2048,256]{1,0:T(8,128)(2,1)}, bf16[2048,256]{1,0:T(8,128)(2,1)S(1)}, u32[]{:S(2)}) copy-start(bf16[2048,256]{1,0:T(8,128)(2,1)S(1)} %collective-permute-done.12.refs_3_) | copy-start | bytes 3145732
  33.1 50.6 %copy-start.5 = (bf16[2048,256]{1,0:T(8,128)(2,1)}, bf16[2048,256]{1,0:T(8,128)(2,1)S(1)}, u32[]{:S(2)}) copy-start(bf16[2048,256]{1,0:T(8,128)(2,1)S(1)} %collective-permute-done.13.refs_4_) | copy-start | bytes 3145732
  34.6 49.1 %copy-start.6 = (bf16[256,2048]{1,0:T(8,128)(2,1)}, bf16[256,2048]{1,0:T(8,128)(2,1)S(1)}, u32[]{:S(2)}) copy-start(bf16[256,2048]{1,0:T(8,128)(2,1)S(1)} %collective-permute-done.14.refs_5_) | copy-start | bytes 3145732
  97.2 27.5 %all-to-all-start = ((bf16[8,288,128]{2,1,0:T(8,128)(2,1)}), bf16[8,288,128]{2,1,0:T(8,128)(2,1)S(1)}, u32[]{:S(2)}, u32[]{:S(2)}) async-start(bf16[8,288,128]{2,1,0:T(8,128)(2,1)} %latents.1), calls=%async_computation | async-start | bytes 1179648 | tf_op jit(solution)/shard_map/all_to_all | solution.py:303
  101.5 128.4 %reduce-scatter.3.cloned.1.call-start = ((), (), s32[]{:S(2)}) async-start(), calls=%async_computation.5 | async-start | bytes 1769472 | tf_op jit(solution)/shard_map/reduce_scatter | solution.py:398
  124.6 2.7 %collective-permute-start = (bf16[8,288,128]{2,1,0:T(8,128)(2,1)S(1)}, bf16[8,288,128]{2,1,0:T(8,128)(2,1)S(1)}, u32[]{:S(2)}, u32[]{:S(2)}) collective-permute-start(bf16[8,288,128]{2,1,0:T(8,128)(2,1)S(1)} %all-to-all-done.mine_ref), channel_id=1, source_target_pairs={{0,1},{1,0},{2,3},{3,2},{4,5},{5,4},{6,7},{7,6},{8,9},{9,8},{10,11... | collective-permute-start | bytes 1769480 | tf_op jit(solution)/shard_map/ppermute | solution.py:304
  126.1 19.3 %copy-start.8 = (bf16[128,2048]{1,0:T(8,128)(2,1)S(1)}, bf16[128,2048]{1,0:T(8,128)(2,1)}, u32[]{:S(2)}) copy-start(bf16[128,2048]{1,0:T(8,128)(2,1)} %w_own_ref.1) | copy-start | bytes 1572868
  133.3 10.3 %collective-permute-start.1 = (bf16[1152,128]{1,0:T(8,128)(2,1)}, bf16[1152,128]{1,0:T(8,128)(2,1)S(1)}, u32[]{:S(2)}, u32[]{:S(2)}) collective-permute-start(bf16[1152,128]{1,0:T(8,128)(2,1)} %get-tuple-element.10.refs_0_), channel_id=1, source_target_pairs={{0,64},{1,17},{2,66},{3,19},{4,68},{5,21},{6,70},{7,23},{8,72},{9,... | collective-permute-start | bytes 884744 | tf_op jit(solution)/shard_map/ppermute | solution.py:275
  134.8 10.6 %collective-permute-start.2 = (bf16[1152,128]{1,0:T(8,128)(2,1)}, bf16[1152,128]{1,0:T(8,128)(2,1)S(1)}, u32[]{:S(2)}, u32[]{:S(2)}) collective-permute-start(bf16[1152,128]{1,0:T(8,128)(2,1)} %get-tuple-element.10.refs_0_), channel_id=1, source_target_pairs={{0,192},{1,49},{2,194},{3,51},{4,196},{5,53},{6,198},{7,55},{8,200... | collective-permute-start | bytes 884744 | tf_op jit(solution)/shard_map/ppermute | solution.py:275
  136.5 18.7 %collective-permute-start.4 = (bf16[1920,128]{1,0:T(8,128)(2,1)}, bf16[1920,128]{1,0:T(8,128)(2,1)S(1)}, u32[]{:S(2)}, u32[]{:S(2)}) collective-permute-start(bf16[1920,128]{1,0:T(8,128)(2,1)} %get-tuple-element.11.refs_4_), channel_id=1, source_target_pairs={{0,16},{1,65},{2,18},{3,67},{4,20},{5,69},{6,22},{7,71},{8,24},{9,... | collective-permute-start | bytes 1474568 | tf_op jit(solution)/shard_map/ppermute | solution.py:275
  138.0 17.2 %collective-permute-start.5 = (bf16[1920,128]{1,0:T(8,128)(2,1)}, bf16[1920,128]{1,0:T(8,128)(2,1)S(1)}, u32[]{:S(2)}, u32[]{:S(2)}) collective-permute-start(bf16[1920,128]{1,0:T(8,128)(2,1)} %get-tuple-element.11.refs_4_), channel_id=1, source_target_pairs={{0,48},{1,193},{2,50},{3,195},{4,52},{5,197},{6,54},{7,199},{8,56}... | collective-permute-start | bytes 1474568 | tf_op jit(solution)/shard_map/ppermute | solution.py:275
  138.6 17.5 %collective-permute-start.6 = (bf16[1920,128]{1,0:T(8,128)(2,1)}, bf16[1920,128]{1,0:T(8,128)(2,1)S(1)}, u32[]{:S(2)}, u32[]{:S(2)}) collective-permute-start(bf16[1920,128]{1,0:T(8,128)(2,1)} %get-tuple-element.11.refs_4_), channel_id=1, source_target_pairs={{0,32},{1,129},{2,34},{3,131},{4,36},{5,133},{6,38},{7,135},{8,40}... | collective-permute-start | bytes 1474568 | tf_op jit(solution)/shard_map/ppermute | solution.py:275
  143.6 11.6 %collective-permute-start.3 = (bf16[1152,128]{1,0:T(8,128)(2,1)}, bf16[1152,128]{1,0:T(8,128)(2,1)S(1)}, u32[]{:S(2)}, u32[]{:S(2)}) collective-permute-start(bf16[1152,128]{1,0:T(8,128)(2,1)} %get-tuple-element.10.refs_0_), channel_id=1, source_target_pairs={{0,128},{1,33},{2,130},{3,35},{4,132},{5,37},{6,134},{7,39},{8,136... | collective-permute-start | bytes 884744 | tf_op jit(solution)/shard_map/ppermute | solution.py:275
  145.4 42.9 %collective-permute-start.11 = (bf16[128,2048]{1,0:T(8,128)(2,1)S(1)}, bf16[128,2048]{1,0:T(8,128)(2,1)S(1)}, u32[]{:S(2)}, u32[]{:S(2)}) collective-permute-start(bf16[128,2048]{1,0:T(8,128)(2,1)S(1)} %copy-done.8), channel_id=1, source_target_pairs={{0,1},{1,0},{2,3},{3,2},{4,5},{5,4},{6,7},{7,6},{8,9},{9,8},{10,11... | collective-permute-start | bytes 1572872 | tf_op jit(solution)/shard_map/ppermute | solution.py:354
  174.5 5.9 %collective-permute-start.7 = (bf16[784,128]{1,0:T(8,128)(2,1)}, bf16[784,128]{1,0:T(8,128)(2,1)S(1)}, u32[]{:S(2)}, u32[]{:S(2)}) collective-permute-start(bf16[784,128]{1,0:T(8,128)(2,1)} %get-tuple-element.13), channel_id=1, source_target_pairs={{0,192},{1,49},{2,194},{3,51},{4,196},{5,53},{6,198},{7,55},{8,200... | collective-permute-start | bytes 602120 | tf_op jit(solution)/shard_map/ppermute | solution.py:275
  176.2 9.3 %collective-permute-start.8 = (bf16[784,128]{1,0:T(8,128)(2,1)}, bf16[784,128]{1,0:T(8,128)(2,1)S(1)}, u32[]{:S(2)}, u32[]{:S(2)}) collective-permute-start(bf16[784,128]{1,0:T(8,128)(2,1)} %get-tuple-element.14), channel_id=1, source_target_pairs={{0,64},{1,17},{2,66},{3,19},{4,68},{5,21},{6,70},{7,23},{8,72},{9,... | collective-permute-start | bytes 602120 | tf_op jit(solution)/shard_map/ppermute | solution.py:275
  176.5 9.0 %collective-permute-start.9 = (bf16[784,128]{1,0:T(8,128)(2,1)}, bf16[784,128]{1,0:T(8,128)(2,1)S(1)}, u32[]{:S(2)}, u32[]{:S(2)}) collective-permute-start(bf16[784,128]{1,0:T(8,128)(2,1)} %get-tuple-element.15), channel_id=1, source_target_pairs={{0,128},{1,33},{2,130},{3,35},{4,132},{5,37},{6,134},{7,39},{8,136... | collective-permute-start | bytes 602120 | tf_op jit(solution)/shard_map/ppermute | solution.py:275
  188.3 1.5 collective-permute-start.10
  (15 other events, 42.8 us)
Sparse Core Ops, SparseCore 0:
  28.6 54.9 all-gather.1
  95.5 62.3 reduce-scatter.4
  193.9 35.8 reduce-scatter.2

commit v6 on v5

--- a/solution.py
+++ b/solution.py
@@ -32,16 +32,16 @@
     return values * lax.rsqrt(jnp.mean(values * values, axis=-1, keepdims=True) + EPSILON) * gains
 
 
-def latent_body(q_ref, kv_ref, rope_ref, qg_ref, kvg_ref, out_ref):
+def latent_body(q_ref, kv_ref, rope_ref, qg_ref, kvg_ref, out_ref, turn_ref):
     rows = q_ref.shape[0]
     q = rms(q_ref[...].astype(F32), qg_ref[...][None, :]).astype(BF16)
     kv = rms(kv_ref[...].astype(F32), kvg_ref[...]).astype(BF16)
-    rope = rope_ref[...]
     parts = [p[:, j : j + LANES] for p in (q, kv) for j in range(0, p.shape[1], LANES)]
-    parts.append(jnp.concatenate([rope, jnp.zeros_like(rope)], axis=1))
     for n, part in enumerate(parts):
-        for peer in range(out_ref.shape[0]):
-            out_ref[peer, n * rows : (n + 1) * rows, :] = part
+        out_ref[n * rows : (n + 1) * rows, :] = part
+    rope = rope_ref[...].astype(F32)
+    packed = jnp.concatenate([rope[: rows // 2, :], rope[rows // 2 :, :]], axis=1)
+    turn_ref[...] = packed.astype(BF16)
 
 
 def square(row):
@@ -102,22 +102,24 @@
 
 
 def project_body(
-    mine_ref, other_ref, wq_ref, wk_ref, wv_ref, qg_ref, kg_ref, cos_ref, sin_ref,
-    q_ref, kv_ref, lat_q, lat_kv,
+    lat_ref, turn_ref, wq_ref, wk_ref, wv_ref, qg_ref, kg_ref, cos_ref, sin_ref,
+    q_ref, kv_ref, lat_q, lat_kv, turns,
 ):
-    groups, height, _ = mine_ref.shape
+    peers, height, _ = lat_ref.shape
     q_parts = lat_q.shape[1] // LANES
     kv_parts = lat_kv.shape[1] // LANES
-    own = height // (q_parts + kv_parts + 1)
-    half = groups * own
-    ropes = []
-    for n, src in enumerate((mine_ref, other_ref)):
+    own = height // (q_parts + kv_parts)
+    half = peers * own // 2
+    for t in range(peers):
+        at = (t % 2) * half + t // 2 * own
         for j in range(q_parts + kv_parts):
-            piece = src[:, j * own : (j + 1) * own, :].reshape(half, LANES)
+            piece = lat_ref[t, j * own : (j + 1) * own, :]
             dst, col = (lat_q, j) if j < q_parts else (lat_kv, j - q_parts)
-            dst[n * half : (n + 1) * half, col * LANES : (col + 1) * LANES] = piece
-        ropes.append(src[:, (q_parts + kv_parts) * own :, :].reshape(half, LANES)[:, :ROPE_DIM])
-    rope = jnp.concatenate(ropes, axis=0).astype(F32)
+            dst[at : at + own, col * LANES : (col + 1) * LANES] = piece
+        packed = turn_ref[t, :, :].astype(F32)
+        turns[at : at + own // 2, :] = packed[:, :ROPE_DIM]
+        turns[at + own // 2 : at + own, :] = packed[:, ROPE_DIM:]
+    rope = turns[...]
     cosine, sine = cos_ref[...], sin_ref[...]
     queries = lax.dot_general(
         lat_q[...], wq_ref[...], (((1,), (1,)), ((), ())), preferred_element_type=F32
@@ -188,9 +190,9 @@
             out_refs[b][rows + 8 + j : rows + 8 + j + 1, :] = low
 
 
-def join_body(*refs):
-    parts, outs = refs[:SIDE], refs[SIDE:]
-    half = outs[0].shape[0]
+def join_body(core_ref, *refs):
+    parts, (own_ref, twin_ref, head_ref) = refs[:SIDE], refs[SIDE:]
+    half = own_ref.shape[0]
     rows = 2 * half
     total = sum(
         p[rows : rows + 8, :].astype(F32) + p[rows + 8 : rows + 16, :].astype(F32) for p in parts
@@ -200,8 +202,10 @@
         there = slice(j * LANES, (j + 1) * LANES)
         scale = jnp.broadcast_to(inverse[j : j + 1, :], (LANES, LANES)).T
         head = sum(p[there, :].astype(F32) for p in parts)
-        at = j * LANES % half
-        outs[j * LANES // half][at : at + LANES, :] = (head * scale).astype(BF16)
+        head_ref[there, :] = (head * scale).astype(BF16)
+    core = core_ref[0]
+    own_ref[...] = head_ref[pl.ds(pl.multiple_of(core * half, half), half), :]
+    twin_ref[...] = head_ref[pl.ds(pl.multiple_of((1 - core) * half, half), half), :]
 
 
 def mix_body(own_ref, twin_ref, w_own_ref, w_twin_ref, out_ref):
@@ -275,14 +279,17 @@
         return lax.ppermute(x, ("ep", "tp"), shift(keys, queries, tp_count))
 
 
-    height = own * ((q_latent.shape[1] + kv_latent.shape[1]) // LANES + 1)
+    height = own * ((q_latent.shape[1] + kv_latent.shape[1]) // LANES)
     latents = pl.pallas_call(
         latent_body,
-        out_shape=jax.ShapeDtypeStruct((chips, height, LANES), BF16),
+        out_shape=[
+            jax.ShapeDtypeStruct((height, LANES), BF16),
+            jax.ShapeDtypeStruct((own // 2, LANES), BF16),
+        ],
         compiler_params=params(),
         name="latents",
     )
-    latent = latents(q_latent, kv_latent, rope_key, q_latent_gain, kv_latent_gain[None])
+    latent, turn = latents(q_latent, kv_latent, rope_key, q_latent_gain, kv_latent_gain[None])
 
     id_rows = expert_ids.T
     dispatch = pl.pallas_call(
@@ -296,18 +303,15 @@
     arrived = lax.all_to_all(
         outgoing, ("ep", "tp"), 0, 0, axis_index_groups=plane
     )
-    everyone = lax.all_gather(
-        arrived.reshape(slots, width), "tp", axis=0, axis_index_groups=same_core
-    )
-
-    mine = lax.all_to_all(latent, "tp", 0, 0, axis_index_groups=same_core)
-    other = lax.ppermute(mine, "tp", swap)
+    latent = lax.all_gather(latent, "tp", axis=0)
+    arrived, turn = lax.optimization_barrier((arrived.reshape(slots, width), turn))
+    everyone = lax.all_gather(arrived, "tp", axis=0, axis_index_groups=same_core)
+    turn = lax.all_gather(turn, "tp", axis=0)
 
     block = jnp.arange(rows, dtype=jnp.int32) // own
-    side = jnp.where(block < chips, core, 1 - core)
     positions = (
         lax.axis_index("ep") * rows
-        + ((block % chips) * 2 + side) * own
+        + ((block % chips) * 2 + block // chips) * own
         + jnp.arange(rows, dtype=jnp.int32) % own
     )
     inverse = THETA ** (-jnp.arange(0, ROPE_DIM, 2, dtype=F32) / ROPE_DIM)
@@ -325,12 +329,13 @@
         scratch_shapes=[
             pltpu.VMEM((rows, q_latent.shape[1]), BF16),
             pltpu.VMEM((rows, kv_latent.shape[1]), BF16),
+            pltpu.VMEM((rows, ROPE_DIM), F32),
         ],
         compiler_params=params(),
         name="project",
     )
     q_own, kv_own = project(
-        mine, other, w_query.T, w_key, w_value, query_gain[None], key_gain[None], cosine, sine
+        latent, turn, w_query.T, w_key, w_value, query_gain[None], key_gain[None], cosine, sine
     )
 
     kv_all = [kv_own] + [move(kv_own, d, 0) for d in (1, 3, 2)]
@@ -379,9 +384,12 @@
     own_head, twin_head = pl.pallas_call(
         join_body,
         out_shape=[jax.ShapeDtypeStruct((half, VALUE_DIM), BF16)] * 2,
+        in_specs=[pl.BlockSpec(memory_space=pltpu.SMEM)]
+        + [pl.BlockSpec(memory_space=pltpu.VMEM)] * SIDE,
+        scratch_shapes=[pltpu.VMEM((rows, VALUE_DIM), BF16)],
         compiler_params=params(),
         name="join",
-    )(*parts)
+    )(core.reshape(1), *parts)
     twin_head = lax.ppermute(twin_head, "tp", swap)
     mixed = pl.pallas_call(
         mix_body,

time: 237 us -> 251 us (1.059)
  blocking collectives: 34.1 us -> 57.3 us
  waiting for transfers between devices: 114 us -> 103 us
  starting transfers between devices: 19.3 us -> 22.2 us
    all_gather x0 -> x2, blocking collectives: none -> 41.3 us  [the longest x1 23 us: on_device(): latent = lax.all_gather(latent, 'tp', axis=0)]
    all_to_all x1 -> x0, blocking collectives: 18 us -> none  [on_device(): lax.all_to_all(outgoing, ('ep', 'tp'), 0, 0, axis_index_groups=plane)]
    all_to_all x1, waiting for transfers between devices: 23.1 us -> 8.79 us  [on_device(): lax.all_to_all(outgoing, ('ep', 'tp'), 0, 0, axis_index_groups=plane)]
    all_to_all x1, starting transfers between devices: 4.32 us -> 7.62 us  [on_device(): lax.all_to_all(outgoing, ('ep', 'tp'), 0, 0, axis_index_groups=plane)]
    reduce_scatter x2, waiting for transfers between devices: 16.3 us -> 19.2 us  [summed(): lax.psum_scatter(x, 'tp', scatter_dimension=0, tiled=True, axis_index_gro...]
  transfers between devices with their start and end apart: 19 -> 18, of which waited for: 12 -> 12; matrix products, arithmetic and copies ran while one was open for 2% -> 2% of each run, Pallas kernels for 14% -> 13%
where the time goes in v6:
time: 251 us; the launch traced here: 250 us
  waiting for transfers between devices  103 us (41%)
  blocking collectives  57.3 us (23%)
  Pallas kernels  45.6 us (18%)
  starting transfers between devices  22.2 us (9%)
  between operations  13.9 us (6%)
  local copies, waits for them, and re-layouts  5.99 us (2%)
  other arithmetic  2.64 us (1%)
    all_gather x1, waiting for transfers between devices, on_device(): lax.all_gather(arrived, 'tp', axis=0, axis_index_groups=same_core)  49.1 us
    all_gather x1, blocking collectives, on_device(): latent = lax.all_gather(latent, 'tp', axis=0)  23 us
    ppermute x9, waiting for transfers between devices, move(): return lax.ppermute(x, ('ep', 'tp'), shift(keys, queries, tp_count))  20.8 us
    reduce_scatter x2, waiting for transfers between devices, summed(): lax.psum_scatter(x, 'tp', scatter_dimension=0, tiled=True, axis_index_gro...  19.2 us
    all_gather x1, blocking collectives, on_device(): turn = lax.all_gather(turn, 'tp', axis=0)  18.3 us
    pallas_call x1, Pallas kernels, on_device(): pl.pallas_call(attend_body, out_shape=[jax.ShapeDtypeStruct((rows + 16, L...  17.4 us
    all_to_all x1, blocking collectives, on_device(): lax.all_to_all(done.reshape(EXPERTS, CAP, width), ('ep', 'tp'), 0, 0, axi...  16 us
    ppermute x9, starting transfers between devices, move(): return lax.ppermute(x, ('ep', 'tp'), shift(keys, queries, tp_count))  12.8 us
  transfers between devices with their start and end apart: 18, of which 12 were waited for; matrix products, arithmetic and copies ran while one was open for 2% of the time, Pallas kernels for 13%

profile of v6, /device:TPU:2, one launch (start us, length us, event | category | flops | bytes accessed | tf_op | source)
XLA Modules:
  0.0 250.2 jit_solution(13872717924235869148)
XLA Ops:
  7.2 2.3 dispatch.1
  9.5 7.6 %all-to-all-start = ((bf16[32,4,2048]{2,1,0:T(4,128)(2,1)}), bf16[32,4,2048]{2,1,0:T(4,128)(2,1)S(1)}, u32[]{:S(2)}, u32[]{:S(2)}) async-start(bf16[32,4,2048]{2,1,0:T(4,128)(2,1)} %dispatch.1), calls=%async_computation | async-start | bytes 1048576 | tf_op jit(solution)/shard_map/all_to_all | solution.py:303
  18.7 8.8 %all-to-all-done = bf16[32,4,2048]{2,1,0:T(4,128)(2,1)S(1)} async-done(((bf16[32,4,2048]{2,1,0:T(4,128)(2,1)}), bf16[32,4,2048]{2,1,0:T(4,128)(2,1)S(1)}, u32[]{:S(2)}, u32[]{:S(2)}) %all-to-all-start) | async-done | bytes 524320 | tf_op jit(solution)/shard_map/all_to_all | solution.py:303
  31.5 1.6 collective-permute-done.12.refs_4_
  34.5 49.1 %all-gather.5.cloned.1.call-done = bf16[1024,2048]{1,0:T(8,128)(2,1)} async-done(((bf16[128,2048]{1,0:T(8,128)(2,1)}), bf16[1024,2048]{1,0:T(8,128)(2,1)}) %all-gather.5.cloned.1.call-update) | async-done | bytes 4194320 | tf_op jit(solution)/shard_map/all_gather | solution.py:308
  83.6 11.7 %experts.1 = bf16[8,128,2048]{2,1,0:T(8,128)(2,1)} custom-call(s32[1]{0:T(128)} %bitcast.core_ref, bf16[8,128,2048]{2,1,0:T(8,128)(2,1)} %bitcast.19, bf16[2,2048,256]{2,1,0:T(8,128)(2,1)} %refs_0_.1, bf16[2,2048,256]{2,1,0:T(8,128)(2,1)} %refs_1_.1, bf16[2,256,2048]{2,1,0:T(8,128)(2,1)} %refs_2_.1, bf16[2048,256]{1,0:T(8,128)(2,1)} %copy-done.3, ...), custom_call_target="tpu_custom_call" | custom-call | tf_op jit(solution)/shard_map/experts/pallas_call | solution.py:363
  98.1 23.0 %all-gather = bf16[3840,128]{1,0:T(8,128)(2,1)} all-gather(bf16[240,128]{1,0:T(8,128)(2,1)S(1)} %copy-done.18), channel_id=2, replica_groups=mesh['ep'=16,'tp'=16] {'tp'}, dimensions={0}, use_global_device_ids=true | all-gather | bytes 1044480 | tf_op jit(solution)/shard_map/all_gather | solution.py:306
  121.2 18.3 %all-gather.1 = bf16[384,128]{1,0:T(8,128)(2,1)} all-gather(bf16[24,128]{1,0:T(8,128)(2,1)S(1)} %copy-done.19), channel_id=3, replica_groups=mesh['ep'=16,'tp'=16] {'tp'}, dimensions={0}, use_global_device_ids=true | all-gather | bytes 104448 | tf_op jit(solution)/shard_map/all_gather | solution.py:309
  139.4 4.8 %project.1 = (bf16[1152,128]{1,0:T(8,128)(2,1)}, bf16[1920,128]{1,0:T(8,128)(2,1)}) custom-call(bf16[16,240,128]{2,1,0:T(8,128)(2,1)} %bitcast.20, bf16[16,24,128]{2,1,0:T(8,128)(2,1)} %bitcast.21, bf16[192,384]{1,0:T(8,128)(2,1)} %bitcast.22, bf16[256,128]{1,0:T(8,128)(2,1)} %wk_ref.1, bf16[256,128]{1,0:T(8,128)(2,1)} %wv_ref.1, f32[1,192]{1,0:T(1,128)} %bitcast.26, ...), custom_call_target="tpu_custom_call" | custom-call | tf_op jit(solution)/shard_map/project/pallas_call | solution.py:337
  145.7 1.8 collective-permute-start.1
  149.5 2.1 collective-permute-start.5
  151.6 3.2 %collective-permute-done.refs_1_ = bf16[1152,128]{1,0:T(8,128)(2,1)S(1)} collective-permute-done((bf16[1152,128]{1,0:T(8,128)(2,1)}, bf16[1152,128]{1,0:T(8,128)(2,1)S(1)}, u32[]{:S(2)}, u32[]{:S(2)}) %collective-permute-start) | collective-permute-done | bytes 294944 | tf_op jit(solution)/shard_map/ppermute | solution.py:279
  154.8 1.8 collective-permute-start.2
  156.6 9.7 %collective-permute-done.2.refs_3_ = bf16[1152,128]{1,0:T(8,128)(2,1)S(1)} collective-permute-done((bf16[1152,128]{1,0:T(8,128)(2,1)}, bf16[1152,128]{1,0:T(8,128)(2,1)S(1)}, u32[]{:S(2)}, u32[]{:S(2)}) %collective-permute-start.2) | collective-permute-done | bytes 294944 | tf_op jit(solution)/shard_map/ppermute | solution.py:279
  168.2 17.4 %attend.1 = (bf16[784,128]{1,0:T(8,128)(2,1)}, bf16[784,128]{1,0:T(8,128)(2,1)}, bf16[784,128]{1,0:T(8,128)(2,1)}, bf16[784,128]{1,0:T(8,128)(2,1)}) custom-call(bf16[1152,128]{1,0:T(8,128)(2,1)} %get-tuple-element.17.refs_0_, bf16[1152,128]{1,0:T(8,128)(2,1)} %copy-done.11, bf16[1152,128]{1,0:T(8,128)(2,1)} %copy-done.12, bf16[1152,128]{1,0:T(8,128)(2,1)} %copy-done.13, ...), custom_call_target="tpu_custom_call" | custom-call | tf_op jit(solution)/shard_map/attend/pallas_call | solution.py:343
  185.7 1.6 collective-permute-start.6
  187.7 1.6 collective-permute-start.8
  189.3 2.3 collective-permute-done.6.refs_1_
  191.6 5.0 %collective-permute-done.7.refs_2_ = bf16[784,128]{1,0:T(8,128)(2,1)S(1)} collective-permute-done((bf16[784,128]{1,0:T(8,128)(2,1)}, bf16[784,128]{1,0:T(8,128)(2,1)S(1)}, u32[]{:S(2)}, u32[]{:S(2)}) %collective-permute-start.7) | collective-permute-done | bytes 200736 | tf_op jit(solution)/shard_map/ppermute | solution.py:279
  197.3 2.1 join.1
  201.6 3.3 %mix.1 = bf16[384,2048]{1,0:T(8,128)(2,1)} custom-call(bf16[384,128]{1,0:T(8,128)(2,1)} %get-tuple-element.23.own_ref, bf16[384,128]{1,0:T(8,128)(2,1)} %copy-done.17, bf16[128,2048]{1,0:T(8,128)(2,1)} %w_own_ref.1, bf16[128,2048]{1,0:T(8,128)(2,1)} %copy-done.7), custom_call_target="tpu_custom_call" | custom-call | tf_op jit(solution)/shard_map/mix/pallas_call | solution.py:394
  206.1 16.0 %all_to_all.10.back_ref = bf16[32,4,2048]{2,1,0:T(4,128)(2,1)} all-to-all(bf16[32,4,2048]{2,1,0:T(4,128)(2,1)S(1)} %reshape.77), channel_id=1, replica_groups={{0,1,16,17,32,33,48,49,64,65,80,81,96,97,112,113,128,129,144,145,160,16..., dimensions={0} | all-to-all | bytes 1048576 | tf_op jit(solution)/shard_map/all_to_all | solution.py:412
  222.1 2.4 collect.1
  224.5 19.2 %reduce-scatter.3.cloned.1.call-done = bf16[48,2048]{1,0:T(8,128)(2,1)} async-done(((bf16[384,2048]{1,0:T(8,128)(2,1)}), bf16[48,2048]{1,0:T(8,128)(2,1)}) %reduce-scatter.3.cloned.1.call-update) | async-done | bytes 196624 | tf_op jit(solution)/shard_map/reduce_scatter | solution.py:406
  (75 shorter events, 19.7 us)
Async XLA Ops:
  7.2 21.4 %copy-start = (bf16[2,2048,256]{2,1,0:T(8,128)(2,1)S(1)}, bf16[2,2048,256]{2,1,0:T(8,128)(2,1)}, u32[]{:S(2)}) copy-start(bf16[2,2048,256]{2,1,0:T(8,128)(2,1)} %refs_0_.1) | copy-start | bytes 6291460
  9.5 18.0 %all-to-all-start = ((bf16[32,4,2048]{2,1,0:T(4,128)(2,1)}), bf16[32,4,2048]{2,1,0:T(4,128)(2,1)S(1)}, u32[]{:S(2)}, u32[]{:S(2)}) async-start(bf16[32,4,2048]{2,1,0:T(4,128)(2,1)} %dispatch.1), calls=%async_computation | async-start | bytes 1048576 | tf_op jit(solution)/shard_map/all_to_all | solution.py:303
  17.1 66.5 %all-gather.5.cloned.1.call-start = ((), (), s32[]{:S(2)}) async-start(), calls=%async_computation.6 | async-start | bytes 4718592 | tf_op jit(solution)/shard_map/all_gather | solution.py:308
  28.4 176.4 %reduce-scatter.5.cloned.1.call-start = ((), (), s32[]{:S(2)}) async-start(), calls=%async_computation.5 | async-start | bytes 4718592 | tf_op jit(solution)/shard_map/reduce_scatter | solution.py:406
  28.6 2.8 %collective-permute-start.11 = (bf16[2048,256]{1,0:T(8,128)(2,1)S(1)}, bf16[2048,256]{1,0:T(8,128)(2,1)S(1)}, u32[]{:S(2)}, u32[]{:S(2)}) collective-permute-start(bf16[2048,256]{1,0:T(8,128)(2,1)S(1)} %dynamic-slice_bitcast_fusion.2), channel_id=1, source_target_pairs={{0,1},{1,0},{2,3},{3,2},{4,5},{5,4},{6,7},{7,6},{8,9},{9,8},{10,11... | collective-permute-start | bytes 3145736 | tf_op jit(solution)/shard_map/ppermute | solution.py:358
  30.2 2.8 %collective-permute-start.12 = (bf16[2048,256]{1,0:T(8,128)(2,1)S(1)}, bf16[2048,256]{1,0:T(8,128)(2,1)S(1)}, u32[]{:S(2)}, u32[]{:S(2)}) collective-permute-start(bf16[2048,256]{1,0:T(8,128)(2,1)S(1)} %dynamic-slice_bitcast_fusion.1), channel_id=1, source_target_pairs={{0,1},{1,0},{2,3},{3,2},{4,5},{5,4},{6,7},{7,6},{8,9},{9,8},{10,11... | collective-permute-start | bytes 3145736 | tf_op jit(solution)/shard_map/ppermute | solution.py:358
  30.9 3.7 %collective-permute-start.13 = (bf16[256,2048]{1,0:T(8,128)(2,1)S(1)}, bf16[256,2048]{1,0:T(8,128)(2,1)S(1)}, u32[]{:S(2)}, u32[]{:S(2)}) collective-permute-start(bf16[256,2048]{1,0:T(8,128)(2,1)S(1)} %dynamic-slice_bitcast_fusion), channel_id=1, source_target_pairs={{0,1},{1,0},{2,3},{3,2},{4,5},{5,4},{6,7},{7,6},{8,9},{9,8},{10,11... | collective-permute-start | bytes 3145736 | tf_op jit(solution)/shard_map/ppermute | solution.py:358
  31.5 52.1 %copy-start.3 = (bf16[2048,256]{1,0:T(8,128)(2,1)}, bf16[2048,256]{1,0:T(8,128)(2,1)S(1)}, u32[]{:S(2)}) copy-start(bf16[2048,256]{1,0:T(8,128)(2,1)S(1)} %collective-permute-done.11.refs_3_) | copy-start | bytes 3145732
  33.0 50.6 %copy-start.4 = (bf16[2048,256]{1,0:T(8,128)(2,1)}, bf16[2048,256]{1,0:T(8,128)(2,1)S(1)}, u32[]{:S(2)}) copy-start(bf16[2048,256]{1,0:T(8,128)(2,1)S(1)} %collective-permute-done.12.refs_4_) | copy-start | bytes 3145732
  34.5 49.1 %copy-start.5 = (bf16[256,2048]{1,0:T(8,128)(2,1)}, bf16[256,2048]{1,0:T(8,128)(2,1)S(1)}, u32[]{:S(2)}) copy-start(bf16[256,2048]{1,0:T(8,128)(2,1)S(1)} %collective-permute-done.13.refs_5_) | copy-start | bytes 3145732
  95.4 148.3 %reduce-scatter.3.cloned.1.call-start = ((), (), s32[]{:S(2)}) async-start(), calls=%async_computation.4 | async-start | bytes 1769472 | tf_op jit(solution)/shard_map/reduce_scatter | solution.py:406
  95.5 25.7 %copy-start.19 = (bf16[24,128]{1,0:T(8,128)(2,1)S(1)}, bf16[24,128]{1,0:T(8,128)(2,1)}, u32[]{:S(2)}) copy-start(bf16[24,128]{1,0:T(8,128)(2,1)} %get-tuple-element.16) | copy-start | bytes 18436
  98.1 58.4 %copy-start.6 = (bf16[128,2048]{1,0:T(8,128)(2,1)S(1)}, bf16[128,2048]{1,0:T(8,128)(2,1)}, u32[]{:S(2)}) copy-start(bf16[128,2048]{1,0:T(8,128)(2,1)} %w_own_ref.1) | copy-start | bytes 1572868
  144.3 10.5 %collective-permute-start = (bf16[1152,128]{1,0:T(8,128)(2,1)}, bf16[1152,128]{1,0:T(8,128)(2,1)S(1)}, u32[]{:S(2)}, u32[]{:S(2)}) collective-permute-start(bf16[1152,128]{1,0:T(8,128)(2,1)} %get-tuple-element.17.refs_0_), channel_id=1, source_target_pairs={{0,64},{1,17},{2,66},{3,19},{4,68},{5,21},{6,70},{7,23},{8,72},{9,... | collective-permute-start | bytes 884744 | tf_op jit(solution)/shard_map/ppermute | solution.py:279
  145.7 10.8 %collective-permute-start.1 = (bf16[1152,128]{1,0:T(8,128)(2,1)}, bf16[1152,128]{1,0:T(8,128)(2,1)S(1)}, u32[]{:S(2)}, u32[]{:S(2)}) collective-permute-start(bf16[1152,128]{1,0:T(8,128)(2,1)} %get-tuple-element.17.refs_0_), channel_id=1, source_target_pairs={{0,192},{1,49},{2,194},{3,51},{4,196},{5,53},{6,198},{7,55},{8,200... | collective-permute-start | bytes 884744 | tf_op jit(solution)/shard_map/ppermute | solution.py:279
  147.5 18.9 %collective-permute-start.3 = (bf16[1920,128]{1,0:T(8,128)(2,1)}, bf16[1920,128]{1,0:T(8,128)(2,1)S(1)}, u32[]{:S(2)}, u32[]{:S(2)}) collective-permute-start(bf16[1920,128]{1,0:T(8,128)(2,1)} %get-tuple-element.18.refs_4_), channel_id=1, source_target_pairs={{0,16},{1,65},{2,18},{3,67},{4,20},{5,69},{6,22},{7,71},{8,24},{9,... | collective-permute-start | bytes 1474568 | tf_op jit(solution)/shard_map/ppermute | solution.py:279
  149.0 17.4 %collective-permute-start.4 = (bf16[1920,128]{1,0:T(8,128)(2,1)}, bf16[1920,128]{1,0:T(8,128)(2,1)S(1)}, u32[]{:S(2)}, u32[]{:S(2)}) collective-permute-start(bf16[1920,128]{1,0:T(8,128)(2,1)} %get-tuple-element.18.refs_4_), channel_id=1, source_target_pairs={{0,48},{1,193},{2,50},{3,195},{4,52},{5,197},{6,54},{7,199},{8,56}... | collective-permute-start | bytes 1474568 | tf_op jit(solution)/shard_map/ppermute | solution.py:279
  149.5 17.5 %collective-permute-start.5 = (bf16[1920,128]{1,0:T(8,128)(2,1)}, bf16[1920,128]{1,0:T(8,128)(2,1)S(1)}, u32[]{:S(2)}, u32[]{:S(2)}) collective-permute-start(bf16[1920,128]{1,0:T(8,128)(2,1)} %get-tuple-element.18.refs_4_), channel_id=1, source_target_pairs={{0,32},{1,129},{2,34},{3,131},{4,36},{5,133},{6,38},{7,135},{8,40}... | collective-permute-start | bytes 1474568 | tf_op jit(solution)/shard_map/ppermute | solution.py:279
  154.8 11.6 %collective-permute-start.2 = (bf16[1152,128]{1,0:T(8,128)(2,1)}, bf16[1152,128]{1,0:T(8,128)(2,1)S(1)}, u32[]{:S(2)}, u32[]{:S(2)}) collective-permute-start(bf16[1152,128]{1,0:T(8,128)(2,1)} %get-tuple-element.17.refs_0_), channel_id=1, source_target_pairs={{0,128},{1,33},{2,130},{3,35},{4,132},{5,37},{6,134},{7,39},{8,136... | collective-permute-start | bytes 884744 | tf_op jit(solution)/shard_map/ppermute | solution.py:279
  156.6 42.9 %collective-permute-start.10 = (bf16[128,2048]{1,0:T(8,128)(2,1)S(1)}, bf16[128,2048]{1,0:T(8,128)(2,1)S(1)}, u32[]{:S(2)}, u32[]{:S(2)}) collective-permute-start(bf16[128,2048]{1,0:T(8,128)(2,1)S(1)} %copy-done.6), channel_id=1, source_target_pairs={{0,1},{1,0},{2,3},{3,2},{4,5},{5,4},{6,7},{7,6},{8,9},{9,8},{10,11... | collective-permute-start | bytes 1572872 | tf_op jit(solution)/shard_map/ppermute | solution.py:359
  185.7 5.9 %collective-permute-start.6 = (bf16[784,128]{1,0:T(8,128)(2,1)}, bf16[784,128]{1,0:T(8,128)(2,1)S(1)}, u32[]{:S(2)}, u32[]{:S(2)}) collective-permute-start(bf16[784,128]{1,0:T(8,128)(2,1)} %get-tuple-element.20), channel_id=1, source_target_pairs={{0,192},{1,49},{2,194},{3,51},{4,196},{5,53},{6,198},{7,55},{8,200... | collective-permute-start | bytes 602120 | tf_op jit(solution)/shard_map/ppermute | solution.py:279
  187.3 9.3 %collective-permute-start.7 = (bf16[784,128]{1,0:T(8,128)(2,1)}, bf16[784,128]{1,0:T(8,128)(2,1)S(1)}, u32[]{:S(2)}, u32[]{:S(2)}) collective-permute-start(bf16[784,128]{1,0:T(8,128)(2,1)} %get-tuple-element.21), channel_id=1, source_target_pairs={{0,64},{1,17},{2,66},{3,19},{4,68},{5,21},{6,70},{7,23},{8,72},{9,... | collective-permute-start | bytes 602120 | tf_op jit(solution)/shard_map/ppermute | solution.py:279
  187.7 8.9 %collective-permute-start.8 = (bf16[784,128]{1,0:T(8,128)(2,1)}, bf16[784,128]{1,0:T(8,128)(2,1)S(1)}, u32[]{:S(2)}, u32[]{:S(2)}) collective-permute-start(bf16[784,128]{1,0:T(8,128)(2,1)} %get-tuple-element.22), channel_id=1, source_target_pairs={{0,128},{1,33},{2,130},{3,35},{4,132},{5,37},{6,134},{7,39},{8,136... | collective-permute-start | bytes 602120 | tf_op jit(solution)/shard_map/ppermute | solution.py:279
  199.4 1.5 collective-permute-start.9
  (14 other events, 41.4 us)
Sparse Core Ops, SparseCore 0:
  28.6 54.9 all-gather.4
  95.5 56.8 reduce-scatter.4
  205.0 38.6 reduce-scatter.2

commit v7 on v5

--- a/solution.py
+++ b/solution.py
@@ -36,12 +36,13 @@
     rows = q_ref.shape[0]
     q = rms(q_ref[...].astype(F32), qg_ref[...][None, :]).astype(BF16)
     kv = rms(kv_ref[...].astype(F32), kvg_ref[...]).astype(BF16)
-    rope = rope_ref[...]
+    rope = rope_ref[...].astype(F32)
     parts = [p[:, j : j + LANES] for p in (q, kv) for j in range(0, p.shape[1], LANES)]
-    parts.append(jnp.concatenate([rope, jnp.zeros_like(rope)], axis=1))
-    for n, part in enumerate(parts):
-        for peer in range(out_ref.shape[0]):
+    packed = jnp.concatenate([rope[: rows // 2, :], rope[rows // 2 :, :]], axis=1)
+    for peer in range(out_ref.shape[0]):
+        for n, part in enumerate(parts):
             out_ref[peer, n * rows : (n + 1) * rows, :] = part
+        out_ref[peer, len(parts) * rows :, :] = packed.astype(BF16)
 
 
 def square(row):
@@ -108,7 +109,7 @@
     groups, height, _ = mine_ref.shape
     q_parts = lat_q.shape[1] // LANES
     kv_parts = lat_kv.shape[1] // LANES
-    own = height // (q_parts + kv_parts + 1)
+    own = 2 * height // (2 * (q_parts + kv_parts) + 1)
     half = groups * own
     ropes = []
     for n, src in enumerate((mine_ref, other_ref)):
@@ -116,8 +117,10 @@
             piece = src[:, j * own : (j + 1) * own, :].reshape(half, LANES)
             dst, col = (lat_q, j) if j < q_parts else (lat_kv, j - q_parts)
             dst[n * half : (n + 1) * half, col * LANES : (col + 1) * LANES] = piece
-        ropes.append(src[:, (q_parts + kv_parts) * own :, :].reshape(half, LANES)[:, :ROPE_DIM])
-    rope = jnp.concatenate(ropes, axis=0).astype(F32)
+        packed = src[:, (q_parts + kv_parts) * own :, :].astype(F32)
+        pair = [packed[:, :, :ROPE_DIM], packed[:, :, ROPE_DIM:]]
+        ropes.append(jnp.concatenate(pair, axis=1).reshape(half, ROPE_DIM))
+    rope = jnp.concatenate(ropes, axis=0)
     cosine, sine = cos_ref[...], sin_ref[...]
     queries = lax.dot_general(
         lat_q[...], wq_ref[...], (((1,), (1,)), ((), ())), preferred_element_type=F32
@@ -211,16 +214,33 @@
 
 
 def expert_body(core_ref, x_ref, *refs):
-    del core_ref
-    sets, out_ref = (refs[:3], refs[3:6]), refs[6]
+    sources, out_ref, held, sems = refs[:6], refs[6], refs[7:13], refs[13]
     groups, rows, width = x_ref.shape
+    first = pl.program_id(0) == 0
+    views = [r.at[core_ref[0]] for r in sources[:3]] + list(sources[3:])
+    copies = [
+        pltpu.make_async_copy(view, dst, sems.at[n]) for n, (view, dst) in enumerate(zip(views, held))
+    ]
+
+    @pl.when(first)
+    def _():
+        for copy in copies:
+            copy.start()
+
+    def weights(n):
+        @pl.when(first)
+        def _():
+            copies[n].wait()
+
+        return held[n][...]
+
     x = x_ref[...].reshape(groups * rows, width)
     out = None
-    for gate_ref, up_ref, down_ref in sets:
-        gate = jnp.dot(x, gate_ref[...].reshape(width, -1), preferred_element_type=F32)
-        up = jnp.dot(x, up_ref[...].reshape(width, -1), preferred_element_type=F32)
+    for n in (0, 3):
+        gate = jnp.dot(x, weights(n), preferred_element_type=F32)
+        up = jnp.dot(x, weights(n + 1), preferred_element_type=F32)
         hidden = (gate / (1.0 + jnp.exp(-gate)) * up).astype(BF16)
-        term = jnp.dot(hidden, down_ref[...].reshape(-1, width), preferred_element_type=F32)
+        term = jnp.dot(hidden, weights(n + 2), preferred_element_type=F32)
         out = term if out is None else out + term
     out_ref[...] = out.astype(BF16).reshape(groups, rows, width)
 
@@ -275,7 +295,7 @@
         return lax.ppermute(x, ("ep", "tp"), shift(keys, queries, tp_count))
 
 
-    height = own * ((q_latent.shape[1] + kv_latent.shape[1]) // LANES + 1)
+    height = own * ((q_latent.shape[1] + kv_latent.shape[1]) // LANES) + own // 2
     latents = pl.pallas_call(
         latent_body,
         out_shape=jax.ShapeDtypeStruct((chips, height, LANES), BF16),
@@ -363,13 +383,13 @@
             grid=(chips // step,),
             in_specs=[
                 pl.BlockSpec((step, slots, width), lambda j, c: (j, 0, 0)),
-                pl.BlockSpec((1, width, hidden), lambda j, c: (c[0], 0, 0)),
-                pl.BlockSpec((1, width, hidden), lambda j, c: (c[0], 0, 0)),
-                pl.BlockSpec((1, hidden, width), lambda j, c: (c[0], 0, 0)),
-                pl.BlockSpec((width, hidden), lambda j, c: (0, 0)),
-                pl.BlockSpec((width, hidden), lambda j, c: (0, 0)),
-                pl.BlockSpec((hidden, width), lambda j, c: (0, 0)),
-            ],
+            ]
+            + [pl.BlockSpec(memory_space=pl.ANY)] * 6,
+            scratch_shapes=[
+                pltpu.VMEM(shape, BF16)
+                for shape in ((width, hidden), (width, hidden), (hidden, width)) * 2
+            ]
+            + [pltpu.SemaphoreType.DMA((6,))],
             out_specs=pl.BlockSpec((step, slots, width), lambda j, c: (j, 0, 0)),
         ),
         compiler_params=params(),

time: 237 us -> 241 us (1.017)
  blocking collectives: 34.1 us -> 60.7 us
  waiting for transfers between devices: 114 us -> 90.2 us
  Pallas kernels: 46.1 us -> 50.9 us
  starting transfers between devices: 19.3 us -> 15 us
    all_to_all x0 -> x1, blocking collectives: none -> 26.6 us  [on_device(): mine = lax.all_to_all(latent, 'tp', 0, 0, axis_index_groups=same_core)]
    all_to_all x1 -> x0, waiting for transfers between devices: 23.1 us -> none  [on_device(): mine = lax.all_to_all(latent, 'tp', 0, 0, axis_index_groups=same_core)]
    pallas_call x1, Pallas kernels: 11.7 us -> 17 us  [on_device(): pl.pallas_call(expert_body, out_shape=jax.ShapeDtypeStruct((chips, slots,...]
    all_to_all x1 -> x0, starting transfers between devices: 4.32 us -> none  [on_device(): mine = lax.all_to_all(latent, 'tp', 0, 0, axis_index_groups=same_core)]
  transfers between devices with their start and end apart: 19 -> 18, of which waited for: 12 -> 11; matrix products, arithmetic and copies ran while one was open for 2% -> 2% of each run, Pallas kernels for 14% -> 13%
where the time goes in v7:
time: 241 us; the launch traced here: 240 us
  waiting for transfers between devices  90.2 us (37%)
  blocking collectives  60.7 us (25%)
  Pallas kernels  50.9 us (21%)
  starting transfers between devices  15 us (6%)
  between operations  13.9 us (6%)
  local copies, waits for them, and re-layouts  6.65 us (3%)
  other arithmetic  2.65 us (1%)
    all_gather x1, waiting for transfers between devices, on_device(): lax.all_gather(arrived.reshape(slots, width), 'tp', axis=0, axis_index_gr...  49.1 us
    all_to_all x1, blocking collectives, on_device(): mine = lax.all_to_all(latent, 'tp', 0, 0, axis_index_groups=same_core)  26.6 us
    ppermute x9, waiting for transfers between devices, move(): return lax.ppermute(x, ('ep', 'tp'), shift(keys, queries, tp_count))  20.5 us
    all_to_all x1, blocking collectives, on_device(): lax.all_to_all(outgoing, ('ep', 'tp'), 0, 0, axis_index_groups=plane)  18 us
    pallas_call x1, Pallas kernels, on_device(): pl.pallas_call(attend_body, out_shape=[jax.ShapeDtypeStruct((rows + 16, L...  17.4 us
    pallas_call x1, Pallas kernels, on_device(): pl.pallas_call(expert_body, out_shape=jax.ShapeDtypeStruct((chips, slots,...  17 us
    all_to_all x1, blocking collectives, on_device(): lax.all_to_all(done.reshape(EXPERTS, CAP, width), ('ep', 'tp'), 0, 0, axi...  16.1 us
    reduce_scatter x2, waiting for transfers between devices, summed(): lax.psum_scatter(x, 'tp', scatter_dimension=0, tiled=True, axis_index_gro...  16 us
  transfers between devices with their start and end apart: 18, of which 11 were waited for; matrix products, arithmetic and copies ran while one was open for 2% of the time, Pallas kernels for 13%

profile of v7, /device:TPU:2, one launch (start us, length us, event | category | flops | bytes accessed | tf_op | source)
XLA Modules:
  0.0 240.1 jit_solution(18173699244796613163)
XLA Ops:
  7.2 2.3 dispatch.1
  9.5 18.0 %all_to_all.15 = bf16[32,4,2048]{2,1,0:T(4,128)(2,1)S(1)} all-to-all(bf16[32,4,2048]{2,1,0:T(4,128)(2,1)} %dispatch.1), channel_id=1, replica_groups={{0,1,16,17,32,33,48,49,64,65,80,81,96,97,112,113,128,129,144,145,160,16..., dimensions={0} | all-to-all | bytes 1048576 | tf_op jit(solution)/shard_map/all_to_all | solution.py:316
  31.5 1.6 collective-permute-done.13.refs_4_
  33.0 1.5 collective-permute-done.14.refs_5_
  34.5 49.1 %all-gather.2.cloned.1.call-done.x_ref = bf16[8,128,2048]{2,1,0:T(8,128)(2,1)} async-done(((bf16[1,128,2048]{2,1,0:T(8,128)(2,1)}), bf16[8,128,2048]{2,1,0:T(8,128)(2,1)}) %all-gather.2.cloned.1.call-update) | async-done | bytes 4194320 | tf_op jit(solution)/shard_map/all_gather | solution.py:319
  83.6 17.0 %experts.1 = bf16[8,128,2048]{2,1,0:T(8,128)(2,1)} custom-call(s32[1]{0:T(128)} %bitcast.4.core_ref, bf16[8,128,2048]{2,1,0:T(8,128)(2,1)} %all-gather.2.cloned.1.call-done.x_ref, bf16[2,2048,256]{2,1,0:T(8,128)(2,1)} %refs_0_.1, bf16[2,2048,256]{2,1,0:T(8,128)(2,1)} %refs_1_.1, bf16[2,256,2048]{2,1,0:T(8,128)(2,1)} %refs_2_.1, bf16[2048,256]{1,0:T(8,128)(2,1)} %copy-done.4, ...), custom_call_target="tpu_custom_call" | custom-call | tf_op jit(solution)/shard_map/experts/pallas_call | solution.py:378
  100.7 1.7 latents.1
  102.4 26.6 %all_to_all.16.mine_ref = bf16[8,264,128]{2,1,0:T(8,128)(2,1)S(1)} all-to-all(bf16[8,264,128]{2,1,0:T(8,128)(2,1)} %latents.1), channel_id=1, replica_groups={{0,2,4,6,8,10,12,14},{1,3,5,7,9,11,13,15},{16,18,20,22,24,26,28,30},{17..., dimensions={0} | all-to-all | bytes 1081344 | tf_op jit(solution)/shard_map/all_to_all | solution.py:323
  132.6 4.7 %project.1 = (bf16[1152,128]{1,0:T(8,128)(2,1)}, bf16[1920,128]{1,0:T(8,128)(2,1)}) custom-call(bf16[8,264,128]{2,1,0:T(8,128)(2,1)} %copy-done.3, bf16[8,264,128]{2,1,0:T(8,128)(2,1)} %copy-done.7, bf16[192,384]{1,0:T(8,128)(2,1)} %bitcast.16, bf16[256,128]{1,0:T(8,128)(2,1)} %wk_ref.1, bf16[256,128]{1,0:T(8,128)(2,1)} %wv_ref.1, f32[1,192]{1,0:T(1,128)} %bitcast.20, ...), custom_call_target="tpu_custom_call" | custom-call | tf_op jit(solution)/shard_map/project/pallas_call | solution.py:352
  138.8 1.8 collective-permute-start.2
  142.6 2.1 collective-permute-start.6
  144.7 3.0 %collective-permute-done.1.refs_1_ = bf16[1152,128]{1,0:T(8,128)(2,1)S(1)} collective-permute-done((bf16[1152,128]{1,0:T(8,128)(2,1)}, bf16[1152,128]{1,0:T(8,128)(2,1)S(1)}, u32[]{:S(2)}, u32[]{:S(2)}) %collective-permute-start.1) | collective-permute-done | bytes 294944 | tf_op jit(solution)/shard_map/ppermute | solution.py:295
  147.6 1.8 collective-permute-start.3
  149.5 9.7 %collective-permute-done.3.refs_3_ = bf16[1152,128]{1,0:T(8,128)(2,1)S(1)} collective-permute-done((bf16[1152,128]{1,0:T(8,128)(2,1)}, bf16[1152,128]{1,0:T(8,128)(2,1)S(1)}, u32[]{:S(2)}, u32[]{:S(2)}) %collective-permute-start.3) | collective-permute-done | bytes 294944 | tf_op jit(solution)/shard_map/ppermute | solution.py:295
  161.2 17.4 %attend.1 = (bf16[784,128]{1,0:T(8,128)(2,1)}, bf16[784,128]{1,0:T(8,128)(2,1)}, bf16[784,128]{1,0:T(8,128)(2,1)}, bf16[784,128]{1,0:T(8,128)(2,1)}) custom-call(bf16[1152,128]{1,0:T(8,128)(2,1)} %get-tuple-element.10.refs_0_, bf16[1152,128]{1,0:T(8,128)(2,1)} %copy-done.13, bf16[1152,128]{1,0:T(8,128)(2,1)} %copy-done.14, bf16[1152,128]{1,0:T(8,128)(2,1)} %copy-done.15, ...), custom_call_target="tpu_custom_call" | custom-call | tf_op jit(solution)/shard_map/attend/pallas_call | solution.py:358
  178.6 1.7 collective-permute-start.7
  180.6 2.0 collective-permute-start.9
  182.6 1.9 collective-permute-done.7.refs_1_
  184.5 5.1 %collective-permute-done.8.refs_2_ = bf16[784,128]{1,0:T(8,128)(2,1)S(1)} collective-permute-done((bf16[784,128]{1,0:T(8,128)(2,1)}, bf16[784,128]{1,0:T(8,128)(2,1)S(1)}, u32[]{:S(2)}, u32[]{:S(2)}) %collective-permute-start.8) | collective-permute-done | bytes 200736 | tf_op jit(solution)/shard_map/ppermute | solution.py:295
  190.3 2.0 join.1
  194.5 3.3 %mix.1 = bf16[384,2048]{1,0:T(8,128)(2,1)} custom-call(bf16[384,128]{1,0:T(8,128)(2,1)} %get-tuple-element.16.own_ref, bf16[384,128]{1,0:T(8,128)(2,1)} %copy-done.19, bf16[128,2048]{1,0:T(8,128)(2,1)} %w_own_ref.1, bf16[128,2048]{1,0:T(8,128)(2,1)} %copy-done.9), custom_call_target="tpu_custom_call" | custom-call | tf_op jit(solution)/shard_map/mix/pallas_call | solution.py:406
  199.1 16.1 %all_to_all.17.back_ref = bf16[32,4,2048]{2,1,0:T(4,128)(2,1)} all-to-all(bf16[32,4,2048]{2,1,0:T(4,128)(2,1)S(1)} %reshape.59), channel_id=1, replica_groups={{0,1,16,17,32,33,48,49,64,65,80,81,96,97,112,113,128,129,144,145,160,16..., dimensions={0} | all-to-all | bytes 1048576 | tf_op jit(solution)/shard_map/all_to_all | solution.py:424
  215.2 2.4 collect.1
  217.6 16.0 %reduce-scatter.3.cloned.1.call-done = bf16[48,2048]{1,0:T(8,128)(2,1)} async-done(((bf16[384,2048]{1,0:T(8,128)(2,1)}), bf16[48,2048]{1,0:T(8,128)(2,1)}) %reduce-scatter.3.cloned.1.call-update) | async-done | bytes 196624 | tf_op jit(solution)/shard_map/reduce_scatter | solution.py:418
  (75 shorter events, 17.4 us)
Async XLA Ops:
  7.2 21.4 %copy-start = (bf16[2,2048,256]{2,1,0:T(8,128)(2,1)S(1)}, bf16[2,2048,256]{2,1,0:T(8,128)(2,1)}, u32[]{:S(2)}) copy-start(bf16[2,2048,256]{2,1,0:T(8,128)(2,1)} %refs_0_.1) | copy-start | bytes 6291460
  7.2 76.4 %all-gather.2.cloned.1.call-start = ((), (), s32[]{:S(2)}) async-start(), calls=%async_computation.6 | async-start | bytes 4718592 | tf_op jit(solution)/shard_map/all_gather | solution.py:319
  28.5 169.4 %reduce-scatter.5.cloned.1.call-start = ((), (), s32[]{:S(2)}) async-start(), calls=%async_computation.7 | async-start | bytes 4718592 | tf_op jit(solution)/shard_map/reduce_scatter | solution.py:418
  28.7 2.8 %collective-permute-start.12 = (bf16[2048,256]{1,0:T(8,128)(2,1)S(1)}, bf16[2048,256]{1,0:T(8,128)(2,1)S(1)}, u32[]{:S(2)}, u32[]{:S(2)}) collective-permute-start(bf16[2048,256]{1,0:T(8,128)(2,1)S(1)} %dynamic-slice_bitcast_fusion.2), channel_id=1, source_target_pairs={{0,1},{1,0},{2,3},{3,2},{4,5},{5,4},{6,7},{7,6},{8,9},{9,8},{10,11... | collective-permute-start | bytes 3145736 | tf_op jit(solution)/shard_map/ppermute | solution.py:373
  30.2 2.8 %collective-permute-start.13 = (bf16[2048,256]{1,0:T(8,128)(2,1)S(1)}, bf16[2048,256]{1,0:T(8,128)(2,1)S(1)}, u32[]{:S(2)}, u32[]{:S(2)}) collective-permute-start(bf16[2048,256]{1,0:T(8,128)(2,1)S(1)} %dynamic-slice_bitcast_fusion.1), channel_id=1, source_target_pairs={{0,1},{1,0},{2,3},{3,2},{4,5},{5,4},{6,7},{7,6},{8,9},{9,8},{10,11... | collective-permute-start | bytes 3145736 | tf_op jit(solution)/shard_map/ppermute | solution.py:373
  30.9 3.7 %collective-permute-start.14 = (bf16[256,2048]{1,0:T(8,128)(2,1)S(1)}, bf16[256,2048]{1,0:T(8,128)(2,1)S(1)}, u32[]{:S(2)}, u32[]{:S(2)}) collective-permute-start(bf16[256,2048]{1,0:T(8,128)(2,1)S(1)} %dynamic-slice_bitcast_fusion), channel_id=1, source_target_pairs={{0,1},{1,0},{2,3},{3,2},{4,5},{5,4},{6,7},{7,6},{8,9},{9,8},{10,11... | collective-permute-start | bytes 3145736 | tf_op jit(solution)/shard_map/ppermute | solution.py:373
  31.5 52.1 %copy-start.4 = (bf16[2048,256]{1,0:T(8,128)(2,1)}, bf16[2048,256]{1,0:T(8,128)(2,1)S(1)}, u32[]{:S(2)}) copy-start(bf16[2048,256]{1,0:T(8,128)(2,1)S(1)} %collective-permute-done.12.refs_3_) | copy-start | bytes 3145732
  33.0 50.6 %copy-start.5 = (bf16[2048,256]{1,0:T(8,128)(2,1)}, bf16[2048,256]{1,0:T(8,128)(2,1)S(1)}, u32[]{:S(2)}) copy-start(bf16[2048,256]{1,0:T(8,128)(2,1)S(1)} %collective-permute-done.13.refs_4_) | copy-start | bytes 3145732
  34.5 49.1 %copy-start.6 = (bf16[256,2048]{1,0:T(8,128)(2,1)}, bf16[256,2048]{1,0:T(8,128)(2,1)S(1)}, u32[]{:S(2)}) copy-start(bf16[256,2048]{1,0:T(8,128)(2,1)S(1)} %collective-permute-done.14.refs_5_) | copy-start | bytes 3145732
  100.7 132.9 %reduce-scatter.3.cloned.1.call-start = ((), (), s32[]{:S(2)}) async-start(), calls=%async_computation.5 | async-start | bytes 1769472 | tf_op jit(solution)/shard_map/reduce_scatter | solution.py:418
  129.1 2.7 %collective-permute-start = (bf16[8,264,128]{2,1,0:T(8,128)(2,1)S(1)}, bf16[8,264,128]{2,1,0:T(8,128)(2,1)S(1)}, u32[]{:S(2)}, u32[]{:S(2)}) collective-permute-start(bf16[8,264,128]{2,1,0:T(8,128)(2,1)S(1)} %all_to_all.16.mine_ref), channel_id=1, source_target_pairs={{0,1},{1,0},{2,3},{3,2},{4,5},{5,4},{6,7},{7,6},{8,9},{9,8},{10,11... | collective-permute-start | bytes 1622024 | tf_op jit(solution)/shard_map/ppermute | solution.py:324
  130.6 18.9 %copy-start.8 = (bf16[128,2048]{1,0:T(8,128)(2,1)S(1)}, bf16[128,2048]{1,0:T(8,128)(2,1)}, u32[]{:S(2)}) copy-start(bf16[128,2048]{1,0:T(8,128)(2,1)} %w_own_ref.1) | copy-start | bytes 1572868
  137.4 10.3 %collective-permute-start.1 = (bf16[1152,128]{1,0:T(8,128)(2,1)}, bf16[1152,128]{1,0:T(8,128)(2,1)S(1)}, u32[]{:S(2)}, u32[]{:S(2)}) collective-permute-start(bf16[1152,128]{1,0:T(8,128)(2,1)} %get-tuple-element.10.refs_0_), channel_id=1, source_target_pairs={{0,64},{1,17},{2,66},{3,19},{4,68},{5,21},{6,70},{7,23},{8,72},{9,... | collective-permute-start | bytes 884744 | tf_op jit(solution)/shard_map/ppermute | solution.py:295
  138.8 10.6 %collective-permute-start.2 = (bf16[1152,128]{1,0:T(8,128)(2,1)}, bf16[1152,128]{1,0:T(8,128)(2,1)S(1)}, u32[]{:S(2)}, u32[]{:S(2)}) collective-permute-start(bf16[1152,128]{1,0:T(8,128)(2,1)} %get-tuple-element.10.refs_0_), channel_id=1, source_target_pairs={{0,192},{1,49},{2,194},{3,51},{4,196},{5,53},{6,198},{7,55},{8,200... | collective-permute-start | bytes 884744 | tf_op jit(solution)/shard_map/ppermute | solution.py:295
  140.6 18.7 %collective-permute-start.4 = (bf16[1920,128]{1,0:T(8,128)(2,1)}, bf16[1920,128]{1,0:T(8,128)(2,1)S(1)}, u32[]{:S(2)}, u32[]{:S(2)}) collective-permute-start(bf16[1920,128]{1,0:T(8,128)(2,1)} %get-tuple-element.11.refs_4_), channel_id=1, source_target_pairs={{0,16},{1,65},{2,18},{3,67},{4,20},{5,69},{6,22},{7,71},{8,24},{9,... | collective-permute-start | bytes 1474568 | tf_op jit(solution)/shard_map/ppermute | solution.py:295
  142.1 17.2 %collective-permute-start.5 = (bf16[1920,128]{1,0:T(8,128)(2,1)}, bf16[1920,128]{1,0:T(8,128)(2,1)S(1)}, u32[]{:S(2)}, u32[]{:S(2)}) collective-permute-start(bf16[1920,128]{1,0:T(8,128)(2,1)} %get-tuple-element.11.refs_4_), channel_id=1, source_target_pairs={{0,48},{1,193},{2,50},{3,195},{4,52},{5,197},{6,54},{7,199},{8,56}... | collective-permute-start | bytes 1474568 | tf_op jit(solution)/shard_map/ppermute | solution.py:295
  142.6 17.5 %collective-permute-start.6 = (bf16[1920,128]{1,0:T(8,128)(2,1)}, bf16[1920,128]{1,0:T(8,128)(2,1)S(1)}, u32[]{:S(2)}, u32[]{:S(2)}) collective-permute-start(bf16[1920,128]{1,0:T(8,128)(2,1)} %get-tuple-element.11.refs_4_), channel_id=1, source_target_pairs={{0,32},{1,129},{2,34},{3,131},{4,36},{5,133},{6,38},{7,135},{8,40}... | collective-permute-start | bytes 1474568 | tf_op jit(solution)/shard_map/ppermute | solution.py:295
  147.6 12.5 %copy-start.13 = (bf16[1152,128]{1,0:T(8,128)(2,1)}, bf16[1152,128]{1,0:T(8,128)(2,1)S(1)}, u32[]{:S(2)}) copy-start(bf16[1152,128]{1,0:T(8,128)(2,1)S(1)} %collective-permute-done.1.refs_1_) | copy-start | bytes 884740
  147.6 11.6 %collective-permute-start.3 = (bf16[1152,128]{1,0:T(8,128)(2,1)}, bf16[1152,128]{1,0:T(8,128)(2,1)S(1)}, u32[]{:S(2)}, u32[]{:S(2)}) collective-permute-start(bf16[1152,128]{1,0:T(8,128)(2,1)} %get-tuple-element.10.refs_0_), channel_id=1, source_target_pairs={{0,128},{1,33},{2,130},{3,35},{4,132},{5,37},{6,134},{7,39},{8,136... | collective-permute-start | bytes 884744 | tf_op jit(solution)/shard_map/ppermute | solution.py:295
  149.4 43.0 %collective-permute-start.11 = (bf16[128,2048]{1,0:T(8,128)(2,1)S(1)}, bf16[128,2048]{1,0:T(8,128)(2,1)S(1)}, u32[]{:S(2)}, u32[]{:S(2)}) collective-permute-start(bf16[128,2048]{1,0:T(8,128)(2,1)S(1)} %copy-done.8), channel_id=1, source_target_pairs={{0,1},{1,0},{2,3},{3,2},{4,5},{5,4},{6,7},{7,6},{8,9},{9,8},{10,11... | collective-permute-start | bytes 1572872 | tf_op jit(solution)/shard_map/ppermute | solution.py:374
  178.6 5.9 %collective-permute-start.7 = (bf16[784,128]{1,0:T(8,128)(2,1)}, bf16[784,128]{1,0:T(8,128)(2,1)S(1)}, u32[]{:S(2)}, u32[]{:S(2)}) collective-permute-start(bf16[784,128]{1,0:T(8,128)(2,1)} %get-tuple-element.13), channel_id=1, source_target_pairs={{0,192},{1,49},{2,194},{3,51},{4,196},{5,53},{6,198},{7,55},{8,200... | collective-permute-start | bytes 602120 | tf_op jit(solution)/shard_map/ppermute | solution.py:295
  180.3 9.3 %collective-permute-start.8 = (bf16[784,128]{1,0:T(8,128)(2,1)}, bf16[784,128]{1,0:T(8,128)(2,1)S(1)}, u32[]{:S(2)}, u32[]{:S(2)}) collective-permute-start(bf16[784,128]{1,0:T(8,128)(2,1)} %get-tuple-element.14), channel_id=1, source_target_pairs={{0,64},{1,17},{2,66},{3,19},{4,68},{5,21},{6,70},{7,23},{8,72},{9,... | collective-permute-start | bytes 602120 | tf_op jit(solution)/shard_map/ppermute | solution.py:295
  180.6 9.0 %collective-permute-start.9 = (bf16[784,128]{1,0:T(8,128)(2,1)}, bf16[784,128]{1,0:T(8,128)(2,1)S(1)}, u32[]{:S(2)}, u32[]{:S(2)}) collective-permute-start(bf16[784,128]{1,0:T(8,128)(2,1)} %get-tuple-element.15), channel_id=1, source_target_pairs={{0,128},{1,33},{2,130},{3,35},{4,132},{5,37},{6,134},{7,39},{8,136... | collective-permute-start | bytes 602120 | tf_op jit(solution)/shard_map/ppermute | solution.py:295
  192.4 1.5 collective-permute-start.10
  (14 other events, 30.4 us)
Sparse Core Ops, SparseCore 0:
  28.6 54.9 all-gather.1
  100.8 61.4 reduce-scatter.4
  198.0 35.5 reduce-scatter.2
